TPU v7x, 512 devices: a whole 4x8x8 slice. The times are simulated.
512 devices in a mesh: sp: 64 (over z, y), tp: 8 (over x, core).
Axes of the slice: x: 4, y: 8, z: 8, core: 2. Of those that a mesh axis runs over, the one named last changes fastest.
Arguments:
- inputs: bfloat16 [24576, 2048], P(('sp', 'tp')), may hold values from -6 to 6
- norm_gain: float32 [2048], replicated, may hold values from 0.1 to 1.9
- latent_down: bfloat16 [2048, 256], P('sp'), may hold values from -0.125 to 0.125
- rope_down: bfloat16 [2048, 64], P('sp'), may hold values from -0.125 to 0.125
- latent_gain: float32 [256], replicated, may hold values from 0.1 to 1.9
- mla_query: bfloat16 [2048, 1536], P(None, 'tp'), as said below
- key_up: bfloat16 [256, 1024], replicated, may hold values from -3.5 to 3.5
- value_up: bfloat16 [256, 1024], replicated, may hold values from -1.75 to 1.75
- swa_query: bfloat16 [2048, 1024], P(None, 'tp'), as said below
- swa_key: bfloat16 [2048, 512], P(None, 'tp'), may hold values from -0.125 to 0.125
- swa_value: bfloat16 [2048, 512], P(None, 'tp'), may hold values from -0.125 to 0.125
- sink_logits: float32 [16], replicated, may hold values from 1 to 6
- out_mla: bfloat16 [1024, 2048], P(None, 'tp'), may hold values from -0.875 to 0.875
- out_swa: bfloat16 [1024, 2048], P(None, 'tp'), may hold values from -0.875 to 0.875
Outputs:
- mixed: bfloat16 [24576, 2048], P('sp', 'tp')
Inputs may be any that keep to these rules, and one draw needn't show every extreme that they name: `mla_query`: entries lie within 360 / sqrt(2048) in magnitude. `swa_query`: entries lie within 900 / sqrt(2048) in magnitude.
All inputs are finite; a program needn't handle non-finite values.
Results may differ from a plain program's by a relative error of at most 0.02.
The roundings to bfloat16 on the way count: a program that leaves them out, or rounds other values in their place, can miss the bound.
Values may be sent and summed in bfloat16 or wider, within the bound.
No kernel may reach another device: no remote copies, remote signals or barrier semaphores. Data moves between devices by JAX's collectives and lax.ppermute only.
A program may use at most 64 MiB of HBM per device.

v0:
```python
import math

import jax
import jax.numpy as jnp
from jax import lax
from jax.sharding import Mesh
from jax.sharding import PartitionSpec as P

NOPE = 128
ROPE = 64
VDIM = 128
KV_RANK = 256
HEAD = 64
WINDOW = 128
SP = ("sp_0", "sp_1")
SP_TP = ("sp_0", "sp_1", "tp")


NORM_EPS = 1e-06
ROPE_BASE = 10000.0
MASKED_VALUE = -1e30
KEY_SPAN = 512


def joined_along(tiles, dim):
    tiles = jnp.moveaxis(tiles, 0, dim)
    lengths = tiles.shape
    return tiles.reshape(*lengths[:dim], lengths[dim] * lengths[dim + 1], *lengths[dim + 2 :])


def copy_for_each(array, axis):
    copies = jnp.broadcast_to(array, (lax.axis_size(axis), *array.shape))
    return lax.all_to_all(copies, axis, split_axis=0, concat_axis=0, tiled=True)


def gathered_copies(array, axis, dim):
    return joined_along(copy_for_each(array, axis), dim)


def in_one_piece(arrays, axis, dim, along):
    ends, at = ([], 0)
    for a in arrays[:-1]:
        at += a.shape[along]
        ends.append(at)
    both = jnp.concatenate(arrays, axis=along)
    return tuple(jnp.split(lax.all_gather(both, axis, axis=dim, tiled=True), ends, axis=along))


def stacked_from(array, axes, turns):
    tiles = array[None]
    for k in turns:
        tiles = lax.all_gather(tiles, axes[k], axis=0, tiled=True)
    held = [lax.axis_size(axes[k]) for k in reversed(turns)]
    tiles = tiles.reshape(*held, *array.shape)
    turned = sorted(range(len(turns)), key=lambda place: turns[len(turns) - 1 - place])
    return tiles.transpose(*turned, *range(len(turns), tiles.ndim)).reshape(-1, *array.shape)


def gather_axes(array, axes, turns, dim):
    return joined_along(stacked_from(array, axes, turns), dim)


def of_everyone(array, axis):
    everything = copy_for_each(array, axis)
    return jnp.max(everything, axis=0)


def in_one_piece_2(arrays, axis, dim, along):
    widths = [math.prod(a.shape[along:]) for a in arrays]
    both = jnp.concatenate(
        [a.reshape(*a.shape[:along], w) for a, w in zip(arrays, widths)], axis=along
    )
    result = lax.psum_scatter(both, axis, scatter_dimension=dim, tiled=True)
    tiles = jnp.split(result, [sum(widths[:k]) for k in range(1, len(widths))], axis=along)
    return tuple(
        (b.reshape(*result.shape[:along], *a.shape[along:]) for a, b in zip(arrays, tiles))
    )


def from_behind(value, axis, steps):
    count = lax.axis_size(axis)
    first, last = (max(0, -steps), min(count, count - steps))
    return lax.ppermute(value, axis, [(source, source + steps) for source in range(first, last)])


def to_float(values):
    return lax.optimization_barrier(values).astype(jnp.float32)


def norm_rows(values, gains):
    widened = to_float(values)
    scaled = widened * lax.rsqrt(jnp.mean(widened * widened, axis=-1, keepdims=True) + NORM_EPS)
    return (scaled * gains).astype(jnp.bfloat16)


def rotate(values, positions):
    full_width = values.shape[-1]
    half_width = full_width // 2
    inverse = ROPE_BASE ** (-jnp.arange(0, full_width, 2, dtype=jnp.float32) / full_width)
    angles = positions.astype(jnp.float32)[:, None] * inverse[None, :]
    shaped = (values.shape[0],) + (1,) * (values.ndim - 2) + (half_width,)
    cos_table = jnp.cos(angles).reshape(shaped)
    sin_table = jnp.sin(angles).reshape(shaped)
    widened = to_float(values)
    first_half = widened[..., :half_width]
    second_half = widened[..., half_width:]
    return jnp.concatenate(
        [
            first_half * cos_table - second_half * sin_table,
            first_half * sin_table + second_half * cos_table,
        ],
        axis=-1,
    ).astype(jnp.bfloat16)


def attend_latent(
    state_in, keys_latent, keys_rope, key_positions, query_latent, query_rope, query_pos, mla_scale
):
    key_count = keys_latent.shape[0]
    span_rows = math.gcd(key_count, KEY_SPAN)
    last_query = query_pos[-1]

    def update(step_index, state):
        span_pos = lax.dynamic_slice_in_dim(key_positions, step_index * span_rows, span_rows, 0)

        def compute(current):
            running_max, denom_sum, weighted = current
            lat_block = lax.dynamic_slice_in_dim(keys_latent, step_index * span_rows, span_rows, 0)
            rope_block = lax.dynamic_slice_in_dim(keys_rope, step_index * span_rows, span_rows, 0)
            scores = (
                jnp.einsum(
                    "htj,sj->hts", query_latent, lat_block, preferred_element_type=jnp.float32
                )
                + jnp.einsum(
                    "htd,sd->hts", query_rope, rope_block, preferred_element_type=jnp.float32
                )
            ) * mla_scale
            allowed = span_pos[None, None, :] <= query_pos[None, :, None]
            scores = jnp.where(allowed, scores, MASKED_VALUE)
            new_max = jnp.maximum(running_max, jnp.max(scores, axis=-1))
            weights_raw = jnp.where(allowed, jnp.exp(scores - new_max[..., None]), 0.0)
            rescale = jnp.exp(running_max - new_max)
            denom_sum = denom_sum * rescale + jnp.sum(weights_raw, axis=-1)
            weighted = weighted * rescale[..., None] + jnp.einsum(
                "hts,sj->htj",
                weights_raw.astype(jnp.bfloat16),
                lat_block,
                preferred_element_type=jnp.float32,
            )
            return (new_max, denom_sum, weighted)

        return lax.cond(span_pos[0] <= last_query, compute, lambda current: current, state)

    return lax.fori_loop(0, key_count // span_rows, update, state_in)


def shards(
    inputs,
    norm_gain,
    latent_down,
    rope_down,
    latent_gain,
    mla_query,
    key_up,
    value_up,
    swa_query,
    swa_key,
    swa_value,
    sink_logits,
    out_mla,
    out_swa,
):
    own_rows = inputs.shape[0]
    tp_count = lax.axis_size("tp")
    block_rows = own_rows * tp_count
    tp_rank = lax.axis_index("tp")
    offset = lax.axis_index(SP) * block_rows
    own_pos = offset + tp_rank * own_rows + jnp.arange(own_rows, dtype=jnp.int32)
    block_pos = offset + jnp.arange(block_rows, dtype=jnp.int32)
    width_mla = mla_query.shape[1]
    width_swa = swa_query.shape[1]
    width_kv = swa_key.shape[1]
    heads_mla = width_mla // (NOPE + ROPE)
    heads_swa = width_swa // HEAD
    groups_kv = width_kv // HEAD
    group = heads_swa // groups_kv
    normed = norm_rows(inputs, norm_gain)
    pieces = gathered_copies(normed, "tp", 0)
    projected = jnp.concatenate(
        [
            jnp.dot(pieces, mla_query, preferred_element_type=jnp.float32).astype(jnp.bfloat16),
            jnp.dot(pieces, swa_query, preferred_element_type=jnp.float32).astype(jnp.bfloat16),
            jnp.dot(pieces, swa_key, preferred_element_type=jnp.float32).astype(jnp.bfloat16),
            jnp.dot(pieces, swa_value, preferred_element_type=jnp.float32).astype(jnp.bfloat16),
        ],
        axis=1,
    )
    pieces = in_one_piece((latent_down, rope_down), SP, 0, 1)
    latent = jnp.dot(normed, pieces[0], preferred_element_type=jnp.float32)
    rope_raw = jnp.dot(normed, pieces[1], preferred_element_type=jnp.float32)
    keys_latent = norm_rows(latent.astype(jnp.bfloat16), latent_gain)
    keys_rope = rotate(rope_raw.astype(jnp.bfloat16), own_pos)
    queries = projected[:, :width_mla].reshape(block_rows, heads_mla, NOPE + ROPE)
    query_rope = jnp.transpose(rotate(queries[:, :, NOPE:], block_pos), (1, 0, 2))
    head_first = tp_rank * heads_mla
    up_keys = lax.dynamic_slice_in_dim(key_up, head_first * NOPE, heads_mla * NOPE, 1)
    up_keys = up_keys.reshape(KV_RANK, heads_mla, NOPE)
    query_latent = jnp.einsum(
        "thn,jhn->htj", queries[:, :, :NOPE], up_keys, preferred_element_type=jnp.float32
    ).astype(jnp.bfloat16)
    mla_scale = (NOPE + ROPE) ** (-0.5)
    every_latent, every_rope = in_one_piece((query_latent, query_rope), "tp", 0, 2)
    slice_latent, slice_rope = (
        gather_axes(keys_latent, SP, (0, 1), 0),
        gather_axes(keys_rope, SP, (0, 1), 0),
    )
    heads_all = every_latent.shape[0]
    row_index = jnp.arange(slice_latent.shape[0], dtype=jnp.int32)
    slice_pos = row_index // own_rows * block_rows + tp_rank * own_rows + row_index % own_rows
    slice_state = (
        jnp.full((heads_all, block_rows), MASKED_VALUE, jnp.float32),
        jnp.zeros((heads_all, block_rows), jnp.float32),
        jnp.zeros((heads_all, block_rows, KV_RANK), jnp.float32),
    )
    part_max, part_sum, part_weighted = attend_latent(
        slice_state,
        slice_latent,
        slice_rope,
        slice_pos,
        every_latent,
        every_rope,
        block_pos,
        mla_scale,
    )
    global_max = of_everyone(part_max, "tp")
    rescale = jnp.exp(part_max - global_max)
    denom_sum, weighted = tuple(
        (
            part.astype(jnp.float32)
            for part in in_one_piece_2(
                (
                    (part_sum * rescale).astype(jnp.bfloat16),
                    (part_weighted * rescale[..., None]).astype(jnp.bfloat16),
                ),
                "tp",
                0,
                2,
            )
        )
    )
    latent_out = (weighted / denom_sum[..., None]).astype(jnp.bfloat16)
    up_values = lax.dynamic_slice_in_dim(value_up, head_first * VDIM, heads_mla * VDIM, 1)
    up_values = up_values.reshape(KV_RANK, heads_mla, VDIM)
    mla_out = jnp.einsum(
        "htj,jhv->thv", latent_out, up_values, preferred_element_type=jnp.float32
    ).astype(jnp.bfloat16)
    mla_out = mla_out.reshape(block_rows, heads_mla * VDIM)
    swa_q = projected[:, width_mla : width_mla + width_swa].reshape(
        block_rows, groups_kv, group, HEAD
    )
    swa_k = projected[:, width_mla + width_swa : width_mla + width_swa + width_kv]
    swa_v = projected[:, width_mla + width_swa + width_kv : width_mla + width_swa + 2 * width_kv]
    prev_keys, prev_values = from_behind(
        (swa_k[block_rows - WINDOW :], swa_v[block_rows - WINDOW :]), SP, 1
    )
    window_keys_all = jnp.concatenate([prev_keys, swa_k], axis=0).reshape(
        WINDOW + block_rows, groups_kv, HEAD
    )
    window_values = jnp.concatenate([prev_values, swa_v], axis=0).reshape(
        WINDOW + block_rows, groups_kv, HEAD
    )
    scores = jnp.einsum(
        "tkgd,skd->kgts", swa_q, window_keys_all, preferred_element_type=jnp.float32
    ) * HEAD ** (-0.5)
    key_pos = offset - WINDOW + jnp.arange(WINDOW + block_rows, dtype=jnp.int32)
    distance = block_pos[:, None] - key_pos[None, :]
    allowed = (distance >= 0) & (distance < WINDOW) & (key_pos[None, :] >= 0)
    scores = jnp.where(allowed, scores, MASKED_VALUE)
    sink_table = lax.dynamic_slice_in_dim(sink_logits, tp_rank * heads_swa, heads_swa, 0)
    sink_table = sink_table.reshape(groups_kv, group, 1, 1)
    row_max = jnp.maximum(jnp.max(scores, axis=-1, keepdims=True), sink_table)
    weights_raw = jnp.exp(scores - row_max)
    weights = (
        weights_raw / (jnp.sum(weights_raw, axis=-1, keepdims=True) + jnp.exp(sink_table - row_max))
    ).astype(jnp.bfloat16)
    swa_out = jnp.einsum(
        "kgts,skd->tkgd", weights, window_values, preferred_element_type=jnp.float32
    ).astype(jnp.bfloat16)
    swa_out = swa_out.reshape(block_rows, heads_swa * HEAD)
    all_mla, all_swa = in_one_piece((mla_out, swa_out), "tp", 1, 0)
    mixed = jnp.dot(all_mla, out_mla, preferred_element_type=jnp.float32) + jnp.dot(
        all_swa, out_swa, preferred_element_type=jnp.float32
    )
    return mixed.astype(jnp.bfloat16)


def solution(mesh):
    split = Mesh(mesh.devices.reshape(8, 8, mesh.shape["tp"]), ("sp_0", "sp_1", "tp"))
    placed = (
        P(SP_TP, None),
        P(),
        P(SP, None),
        P(SP, None),
        P(),
        P(None, "tp"),
        P(),
        P(),
        P(None, "tp"),
        P(None, "tp"),
        P(None, "tp"),
        P(),
        P(None, "tp"),
        P(None, "tp"),
    )
    return jax.shard_map(
        shards, mesh=split, in_specs=placed, out_specs=P(SP, "tp"), check_vma=False
    )
```

profile of v0, /device:TPU:1, one launch (start us, length us, event | category | flops | bytes accessed | tf_op | source)
XLA Modules:
  0.0 359.5 jit_solution(10568069677121225495)
XLA Ops:
  6.5 1.4 pad_maximum_fusion.3
  8.0 1.1 fusion.35
  9.1 1.1 fusion.37
  10.1 1.4 broadcast_in_dim.68
  11.5 10.3 %all-to-all-start = ((bf16[8,48,2048]{2,1,0:T(8,128)(2,1)}), bf16[8,48,2048]{2,1,0:T(8,128)(2,1)S(1)}, u32[]{:S(2)}, u32[]{:S(2)}) async-start(bf16[8,48,2048]{2,1,0:T(8,128)(2,1)} %broadcast_in_dim.68), calls=%async_computation | async-start | bytes 3145728 | tf_op jit(solution)/shard_map/all_to_all | solution.py:33
  21.8 20.6 %all-to-all-done = bf16[8,48,2048]{2,1,0:T(8,128)(2,1)S(1)} async-done(((bf16[8,48,2048]{2,1,0:T(8,128)(2,1)}), bf16[8,48,2048]{2,1,0:T(8,128)(2,1)S(1)}, u32[]{:S(2)}, u32[]{:S(2)}) %all-to-all-start) | async-done | bytes 1572896 | tf_op jit(solution)/shard_map/all_to_all | solution.py:33
  42.4 0.7 fusion.25
  43.2 1.0 fusion.24
  44.5 0.7 pad_maximum_fusion.1
  45.3 48.9 %all-gather.6.cloned.1.call-done = bf16[2048,320]{1,0:T(8,128)(2,1)} async-done(((bf16[32,320]{1,0:T(8,128)(2,1)}), bf16[2048,320]{1,0:T(8,128)(2,1)}) %all-gather.6.cloned.1.call-update) | async-done | bytes 1310736 | tf_op jit(solution)/shard_map/all_gather | solution.py:46
  94.2 1.5 convolution_convert_fusion.7
  95.9 20.3 %all-gather = bf16[384,256]{1,0:T(8,128)(2,1)} all-gather(bf16[48,256]{1,0:T(8,128)(2,1)S(1)} %fusion.52), channel_id=2, replica_groups=mesh['sp_0'=8,'sp_1'=8,'tp'=8] {'sp_0'}, dimensions={0}, use_global_device_ids=true | all-gather | bytes 221184 | tf_op jit(solution)/shard_map/all_gather | solution.py:52
  116.3 0.7 slice.34
  117.0 1.3 convolution_convert_fusion.8
  118.6 18.9 %all_gather.25 = bf16[8,48,64]{2,1,0:T(8,128)(2,1)S(1)} all-gather(bf16[1,48,64]{2,1,0:T(8,128)(2,1)S(1)} %pad_maximum_fusion.4), channel_id=1, replica_groups=mesh['sp_0'=8,'sp_1'=8,'tp'=8] {'sp_0'}, dimensions={0}, use_global_device_ids=true | all-gather | bytes 55296 | tf_op jit(solution)/shard_map/all_gather | solution.py:52
  137.5 23.1 %all_gather.26 = bf16[64,48,64]{2,1,0:T(8,128)(2,1)S(1)} all-gather(bf16[8,48,64]{2,1,0:T(8,128)(2,1)S(1)} %all_gather.25), channel_id=1, replica_groups=mesh['sp_0'=8,'sp_1'=8,'tp'=8] {'sp_1'}, dimensions={0}, use_global_device_ids=true | all-gather | bytes 442368 | tf_op jit(solution)/shard_map/all_gather | solution.py:52
  160.5 1.6 copy.34
  162.2 2.0 reshape_reshape.7
  164.2 2.7 split.33
  166.9 1.7 copy.35
  168.7 1.0 split.35
  169.7 2.7 copy.33
  172.5 1.9 broadcast_in_dim.66
  174.4 22.4 %while.18 = (s32[]{:T(128)}, f32[8,384]{1,0:T(8,128)S(1)}, f32[8,384]{1,0:T(8,128)S(1)}, f32[8,384,256]{2,1,0:T(8,128)}, s32[3072]{0:T(1024)S(1)}, /*index=5*/s3...) while((s32[]{:T(128)}, f32[8,384]{1,0:T(8,128)S(1)}, ...), condition=%wide.region_7.8_spmd.clone, body=%wide.region_2.7_spmd.clone.sunk | while | flops 1829443968 | bytes 66466276 | solution.py:154
  176.4 10.4 %conditional.3 = ((f32[8,384]{1,0:T(8,128)S(1)}, f32[8,384]{1,0:T(8,128)S(1)}, f32[8,384,256]{2,1,0:T(8,128)})) conditional(s32[]{:T(128)} %convert_element_type.210, (f32[8,384]{1,0:T(8,128)S(1)}, f32[8,384]{1,0:T(8,128)S(1)}, f32[8,384,256]{2,1,0:T(8,128)}) %tuple.52, (s32[512]{0:T(512)S(1)}, s32[]{:T(128)}, s32[]{:T(128)}, ...), branch_computations={%region_3.3_spmd, %region_4.6_spmd} | conditional | flops 1829443968 | bytes 66460312 | solution.py:152
  176.6 1.0 fusion.15
  177.6 2.5 fusion.85
  180.2 1.1 fusion.3
  181.3 0.8 copy-done.1
  182.0 3.1 multiply_add_fusion
  185.1 1.6 copy-done.2
  188.8 0.5 slice.79
  192.9 0.5 slice.79
  196.8 29.9 %all_to_all.10 = f32[8,8,384]{2,1,0:T(8,128)S(1)} all-to-all(f32[8,8,384]{2,1,0:T(8,128)S(1)} %broadcast_in_dim.69), channel_id=1, replica_groups=mesh['sp_0'=8,'sp_1'=8,'tp'=8] {'tp'}, dimensions={0} | all-to-all | bytes 196608 | tf_op jit(solution)/shard_map/all_to_all | solution.py:33
  227.2 2.4 multiply_convert_fusion
  229.5 2.5 pad_maximum_fusion
  233.5 0.6 convolution_convert_fusion.5
  234.1 2.6 collective-permute-start.1
  236.7 0.6 convolution_convert_fusion.6
  237.4 3.1 collective-permute-start
  240.5 0.6 convolution_convert_fusion.3
  242.4 73.9 %reduce-scatter.2.cloned.1.call-done = bf16[1,384,257]{2,1,0:T(8,128)(2,1)} async-done(((bf16[8,384,257]{2,1,0:T(8,128)(2,1)}), bf16[1,384,257]{2,1,0:T(8,128)(2,1)}) %reduce-scatter.2.cloned.1.call-update) | async-done | bytes 197392 | tf_op jit(solution)/shard_map/reduce_scatter | solution.py:73
  316.2 1.0 convert_reduce_fusion
  317.3 1.3 fusion.26
  318.6 0.7 pad_maximum_fusion.2
  319.3 30.9 %all-gather.12.cloned.1.call-done = bf16[768,1024]{0,1:T(8,128)(2,1)} async-done(((bf16[768,128]{0,1:T(8,128)(2,1)}), bf16[768,1024]{0,1:T(8,128)(2,1)}) %all-gather.12.cloned.1.call-update) | async-done | bytes 1572880 | tf_op jit(solution)/shard_map/all_gather | solution.py:46
  350.2 1.7 fusion.29
  351.9 1.1 fusion.23
  (96 shorter events, 7.0 us)
Async XLA Ops:
  6.5 35.9 %copy-start = (bf16[2048,192]{0,1:T(8,128)(2,1)S(1)}, bf16[2048,192]{0,1:T(8,128)(2,1)}, u32[]{:S(2)}) copy-start(bf16[2048,192]{0,1:T(8,128)(2,1)} %param.23) | copy-start | bytes 2359300
  6.5 87.7 %all-gather.6.cloned.1.call-start = ((), (), s32[]{:S(2)}) async-start(), calls=%async_computation.3 | async-start | bytes 1597440 | tf_op jit(solution)/shard_map/all_gather | solution.py:46
  11.5 30.9 %all-to-all-start = ((bf16[8,48,2048]{2,1,0:T(8,128)(2,1)}), bf16[8,48,2048]{2,1,0:T(8,128)(2,1)S(1)}, u32[]{:S(2)}, u32[]{:S(2)}) async-start(bf16[8,48,2048]{2,1,0:T(8,128)(2,1)} %broadcast_in_dim.68), calls=%async_computation | async-start | bytes 3145728 | tf_op jit(solution)/shard_map/all_to_all | solution.py:33
  21.8 142.4 %all-gather.10.cloned.1.call-start = ((), (), s32[]{:S(2)}) async-start(), calls=%async_computation.5 | async-start | bytes 2211840 | tf_op jit(solution)/shard_map/all_gather | solution.py:46
  42.4 1.8 copy-start.3
  43.1 52.7 %copy-start.8 = (f32[256]{0:T(256)S(1)}, f32[256]{0:T(256)}, u32[]{:S(2)}) copy-start(f32[256]{0:T(256)} %param.22) | copy-start | bytes 3076
  45.2 124.5 %all-gather.8.cloned.1.call-start = ((), (), s32[]{:S(2)}) async-start(), calls=%async_computation.4 | async-start | bytes 1769472 | tf_op jit(solution)/shard_map/all_gather | solution.py:52
  116.3 200.0 %reduce-scatter.2.cloned.1.call-start = ((), (), s32[]{:S(2)}) async-start(), calls=%async_computation.6 | async-start | bytes 2654208 | tf_op jit(solution)/shard_map/reduce_scatter | solution.py:73
  180.1 1.9 copy-start.1
  185.1 1.6 copy-start.2
  232.0 0.7 copy-start.12
  232.0 1.4 copy-start.4
  232.0 1.4 copy-start.6
  232.1 4.7 %copy-start.7 = (bf16[2048,64]{0,1:T(8,128)(2,1)S(1)}, bf16[2048,64]{0,1:T(8,128)(2,1)}, u32[]{:S(2)}) copy-start(bf16[2048,64]{0,1:T(8,128)(2,1)} %param.28) | copy-start | bytes 786436
  232.1 118.1 %all-gather.12.cloned.1.call-start = ((), (), s32[]{:S(2)}) async-start(), calls=%async_computation.7 | async-start | bytes 1769472 | tf_op jit(solution)/shard_map/all_gather | solution.py:46
  233.5 7.0 %copy-start.5 = (bf16[2048,128]{1,0:T(8,128)(2,1)S(1)}, bf16[2048,128]{1,0:T(8,128)(2,1)}, u32[]{:S(2)}) copy-start(bf16[2048,128]{1,0:T(8,128)(2,1)} %param.26) | copy-start | bytes 1572868
  234.1 7.0 %collective-permute-start.1 = (bf16[128,64]{0,1:T(8,128)(2,1)S(1)}, bf16[128,64]{0,1:T(8,128)(2,1)S(1)}, u32[]{:S(2)}, u32[]{:S(2)}) collective-permute-start(bf16[128,64]{0,1:T(8,128)(2,1)S(1)} %slice.51), channel_id=1, source_target_pairs={{0,8},{8,16},{16,24},{24,32},{32,40},{40,48},{48,56},{56,64},{64,7... | collective-permute-start | bytes 49160 | tf_op jit(solution)/shard_map/ppermute | solution.py:83
  237.4 4.6 %collective-permute-start = (bf16[128,64]{0,1:T(8,128)(2,1)S(1)}, bf16[128,64]{0,1:T(8,128)(2,1)S(1)}, u32[]{:S(2)}, u32[]{:S(2)}) collective-permute-start(bf16[128,64]{0,1:T(8,128)(2,1)S(1)} %slice.50), channel_id=1, source_target_pairs={{0,8},{8,16},{16,24},{24,32},{32,40},{40,48},{48,56},{56,64},{64,7... | collective-permute-start | bytes 49160 | tf_op jit(solution)/shard_map/ppermute | solution.py:83
  242.4 107.8 %copy-start.10 = (bf16[1024,256]{1,0:T(8,128)(2,1)S(1)}, bf16[1024,256]{1,0:T(8,128)(2,1)}, u32[]{:S(2)}) copy-start(bf16[1024,256]{1,0:T(8,128)(2,1)} %param.30) | copy-start | bytes 1572868
  318.6 33.3 %copy-start.11 = (bf16[1024,256]{1,0:T(8,128)(2,1)S(1)}, bf16[1024,256]{1,0:T(8,128)(2,1)}, u32[]{:S(2)}) copy-start(bf16[1024,256]{1,0:T(8,128)(2,1)} %param.31) | copy-start | bytes 1572868
  350.2 1.7 copy-start.9
Sparse Core Ops, SparseCore 0:
  10.3 83.8 all-gather.5
  96.3 32.2 all-gather.9
  130.7 38.5 all-gather.7
  232.2 84.0 reduce-scatter.1
  319.5 30.6 all-gather.11
where the time goes:
time: 361 us; the launch traced here: 360 us
  waiting for transfers between devices  174 us (48%)
  blocking collectives  92.2 us (26%)
  local copies, waits for them, and re-layouts  23.2 us (6%)
  matrix products  17.9 us (5%)
  starting transfers between devices  16.4 us (5%)
  other arithmetic  13.6 us (4%)
  between operations  13.5 us (4%)
  loops' own time  8.35 us (2%)
    all_gather x3, waiting for transfers between devices, in_one_piece(): lax.all_gather(both, axis, axis=dim, tiled=True)  79.8 us
    reduce_scatter x1, waiting for transfers between devices, in_one_piece_2(): result = lax.psum_scatter(both, axis, scatter_dimension=dim, tiled=True)  73.9 us
    all_gather x3, blocking collectives, stacked_from(): tiles = lax.all_gather(tiles, axes[k], axis=0, tiled=True)  62.3 us
    all_to_all x1, blocking collectives, copy_for_each(): return lax.all_to_all(copies, axis, split_axis=0, concat_axis=0, tiled=True)  29.9 us
    all_to_all x1, waiting for transfers between devices, copy_for_each(): return lax.all_to_all(copies, axis, split_axis=0, concat_axis=0, tiled=True)  20.6 us
    all_to_all x1, starting transfers between devices, copy_for_each(): return lax.all_to_all(copies, axis, split_axis=0, concat_axis=0, tiled=True)  10.3 us
    another operation x1, loops' own time, attend_latent(): return lax.fori_loop(0, key_count // span_rows, update, state_in)  8.16 us
  transfers between devices with their start and end apart: 8, of which 4 were waited for; matrix products, arithmetic and copies ran while one was open for 6% of the time, Pallas kernels for 0%

commit v1 on v0

v1 whole, which is shorter than its diff:
```python
import functools
import math

import jax
import jax.numpy as jnp
from jax import lax
from jax.experimental import pallas as pl
from jax.experimental.pallas import tpu as pltpu
from jax.sharding import Mesh
from jax.sharding import PartitionSpec as P

NOPE = 128
ROPE = 64
VDIM = 128
KV_RANK = 256
HEAD = 64
WINDOW = 128
SP = ("z", "y")
TP = ("x", "c")
SP_TP = ("z", "y", "x", "c")

NORM_EPS = 1e-06
ROPE_BASE = 10000.0
MASKED_VALUE = -1e30
LANES = 128
OWN = 48
SOURCES = 64
ROWS = 384
CHUNK = 16
QTILE = 256
HEADS_CORE = 4
QROWS = HEADS_CORE * ROWS
TILES = QROWS // QTILE
STAT_ROWS = 16
EXP_SCALE = (NOPE + ROPE) ** (-0.5) * math.log2(math.e)


def exchange(array, axis):
    return lax.all_to_all(array, axis, split_axis=0, concat_axis=0, tiled=True)


def to_everyone(array, axis):
    copies = jnp.broadcast_to(array, (lax.axis_size(axis), *array.shape))
    return exchange(copies, axis)


def from_core(value):
    return lax.ppermute(value, "c", [(0, 1), (1, 0)])


def from_x(value, step):
    count = lax.axis_size("x")
    return lax.ppermute(value, "x", [(i, (i + step) % count) for i in range(count)])


def to_float(values):
    return lax.optimization_barrier(values).astype(jnp.float32)


def norm_rows(values, gains):
    widened = to_float(values)
    scaled = widened * lax.rsqrt(jnp.mean(widened * widened, axis=-1, keepdims=True) + NORM_EPS)
    return (scaled * gains).astype(jnp.bfloat16)


def rotate(values, positions):
    full_width = values.shape[-1]
    half_width = full_width // 2
    inverse = ROPE_BASE ** (-jnp.arange(0, full_width, 2, dtype=jnp.float32) / full_width)
    angles = positions.astype(jnp.float32)[:, None] * inverse[None, :]
    cos_table = jnp.cos(angles)
    sin_table = jnp.sin(angles)
    widened = to_float(values)
    first_half = widened[..., :half_width]
    second_half = widened[..., half_width:]
    return jnp.concatenate(
        [
            first_half * cos_table - second_half * sin_table,
            first_half * sin_table + second_half * cos_table,
        ],
        axis=-1,
    ).astype(jnp.bfloat16)


def attend_body(where_ref, keys_ref, q_ref, *refs, first, last):
    if first:
        (o_ref, m_ref, l_ref, kc_ref, vt_ref) = refs
    elif last:
        (o_in, m_in, l_in, out_ref, o_ref, m_ref, l_ref, kc_ref, vt_ref) = refs
    block = where_ref[0]
    key_rank = where_ref[1]
    if first:
        o_ref[...] = jnp.zeros_like(o_ref)
        m_ref[...] = jnp.full(m_ref.shape, MASKED_VALUE, jnp.float32)
        l_ref[...] = jnp.zeros_like(l_ref)
    else:
        o_ref[...] = o_in[...]
        m_ref[...] = m_in[...]
        l_ref[...] = l_in[...]
    n_keys = CHUNK * OWN

    def chunk_step(index, masked):
        part = keys_ref[pl.ds(index * CHUNK, CHUNK)]
        k0 = part[:, :OWN].reshape(n_keys, LANES)
        k1 = part[:, OWN : 2 * OWN].reshape(n_keys, LANES)
        t0 = part[:, 2 * OWN : 2 * OWN + 16]
        t1 = part[:, 2 * OWN + 16 :]
        t0s = jnp.concatenate([t0[..., ROPE:], t0[..., :ROPE]], axis=-1)
        kr = jnp.stack([t0, t0s, t1], axis=1).reshape(n_keys, LANES)
        kc_ref[:, :LANES] = k0
        kc_ref[:, LANES : 2 * LANES] = k1
        kc_ref[:, 2 * LANES :] = kr
        vt_ref[:LANES] = k0.T
        vt_ref[LANES:] = k1.T
        if masked:
            row = lax.broadcasted_iota(jnp.int32, (n_keys, 1), 0)
            key_pos = (index * CHUNK + row // OWN) * ROWS + key_rank * OWN + row % OWN

        def tile_step(tile):
            q = q_ref[pl.ds(tile * QTILE, QTILE)]
            s = lax.dot_general(
                kc_ref[...], q, (((1,), (1,)), ((), ())), preferred_element_type=jnp.float32
            )
            if masked:
                col = tile * QTILE + lax.broadcasted_iota(jnp.int32, (1, QTILE), 1)
                allowed = key_pos <= block * ROWS + col % ROWS
                s = jnp.where(allowed, s, MASKED_VALUE)
            old = m_ref[tile]
            new = jnp.maximum(old, jnp.max(s, axis=0, keepdims=True))
            p = jnp.exp2((s - new) * EXP_SCALE)
            if masked:
                p = jnp.where(allowed, p, 0.0)
            alpha = jnp.exp2((old - new) * EXP_SCALE)
            m_ref[tile] = new
            l_ref[tile] = l_ref[tile] * alpha + jnp.sum(p, axis=0, keepdims=True)
            o_ref[tile] = o_ref[tile] * alpha + jnp.dot(
                vt_ref[...], p.astype(jnp.bfloat16), preferred_element_type=jnp.float32
            )

        def pair_step(pair, carry):
            tile_step(2 * pair)
            tile_step(2 * pair + 1)
            return carry

        lax.fori_loop(0, TILES // 2, pair_step, 0)

    def full_step(index, carry):
        chunk_step(index, False)
        return carry

    n_full = block // CHUNK
    lax.fori_loop(0, n_full, full_step, 0)
    chunk_step(n_full, True)
    if last:
        whole = jnp.concatenate([o_ref[t] for t in range(TILES)], axis=1).astype(jnp.bfloat16)
        m = jnp.concatenate([m_ref[t] for t in range(TILES)], axis=1)
        l = jnp.concatenate([l_ref[t] for t in range(TILES)], axis=1)
        m0 = m.astype(jnp.bfloat16).astype(jnp.float32)
        m1 = (m - m0).astype(jnp.bfloat16).astype(jnp.float32)
        m2 = m - m0 - m1
        l0 = l.astype(jnp.bfloat16).astype(jnp.float32)
        l1 = l - l0
        pad = jnp.zeros((STAT_ROWS - 5, QROWS), jnp.float32)
        stats = jnp.concatenate([m0, m1, m2, l0, l1, pad], axis=0).astype(jnp.bfloat16)
        for h in range(HEADS_CORE):
            out_ref[h, :KV_RANK] = whole[:, h * ROWS : (h + 1) * ROWS]
            out_ref[h, KV_RANK:] = stats[:, h * ROWS : (h + 1) * ROWS]


def attend(where, keys, q, state):
    state_shapes = (
        jax.ShapeDtypeStruct((TILES, KV_RANK, QTILE), jnp.float32),
        jax.ShapeDtypeStruct((TILES, 1, QTILE), jnp.float32),
        jax.ShapeDtypeStruct((TILES, 1, QTILE), jnp.float32),
    )
    first = state is None
    smem = pl.BlockSpec(memory_space=pltpu.SMEM)
    vmem = pl.BlockSpec(memory_space=pltpu.VMEM)
    scratch = [
        pltpu.VMEM((CHUNK * OWN, 3 * LANES), jnp.bfloat16),
        pltpu.VMEM((KV_RANK, CHUNK * OWN), jnp.bfloat16),
    ]
    if not first:
        scratch = [pltpu.VMEM(s.shape, s.dtype) for s in state_shapes] + scratch
    out_shape = (
        state_shapes
        if first
        else jax.ShapeDtypeStruct((HEADS_CORE, KV_RANK + STAT_ROWS, ROWS), jnp.bfloat16)
    )
    operands = (where, keys, q) + (() if first else tuple(state))
    flops = 2 * QROWS * SOURCES * OWN * (3 * LANES + KV_RANK)
    return pl.pallas_call(
        functools.partial(attend_body, first=first, last=not first),
        out_shape=out_shape,
        in_specs=[smem] + [vmem] * (len(operands) - 1),
        out_specs=jax.tree.map(lambda _: vmem, out_shape),
        scratch_shapes=scratch,
        cost_estimate=pl.CostEstimate(
            flops=flops, transcendentals=QROWS * SOURCES * OWN, bytes_accessed=6000000
        ),
        name="attend_first" if first else "attend_last",
    )(*operands)


def shards(
    inputs,
    norm_gain,
    latent_down,
    rope_down,
    latent_gain,
    mla_query,
    key_up,
    value_up,
    swa_query,
    swa_key,
    swa_value,
    sink_logits,
    out_mla,
    out_swa,
):
    own_rows = inputs.shape[0]
    x_rank = lax.axis_index("x")
    c_rank = lax.axis_index("c")
    tp_rank = lax.axis_index(TP)
    block = lax.axis_index(SP)
    offset = block * ROWS
    own_pos = offset + tp_rank * own_rows + jnp.arange(own_rows, dtype=jnp.int32)
    block_pos = offset + jnp.arange(ROWS, dtype=jnp.int32)
    heads_swa = swa_query.shape[1] // HEAD

    down = jnp.concatenate([latent_down, rope_down], axis=1)
    width = down.shape[1] // lax.axis_size(TP)
    down = lax.dynamic_slice_in_dim(down, tp_rank * width, width, 1)
    half = down.shape[0] // 2
    fill = ((0, 0), (0, LANES // 2 - width))
    down = jnp.concatenate([jnp.pad(down[:half], fill), jnp.pad(down[half:], fill)], axis=1)
    down = to_everyone(down, SP)
    down = jnp.stack([down[:, :, :width], down[:, :, LANES // 2 : LANES // 2 + width]], axis=1)
    down = down.reshape(-1, width)

    normed = norm_rows(inputs, norm_gain)
    mine = to_everyone(normed, "x")
    other = from_core(mine)
    is_first = c_rank == 0
    pieces = jnp.stack([jnp.where(is_first, mine, other), jnp.where(is_first, other, mine)], axis=1)
    pieces = pieces.reshape(ROWS, -1)

    latent = jnp.dot(pieces, down, preferred_element_type=jnp.float32).astype(jnp.bfloat16)
    latent = exchange(latent.reshape(-1, own_rows, width), TP)
    latent = jnp.transpose(latent, (1, 0, 2)).reshape(own_rows, KV_RANK + ROPE)
    keys_latent = norm_rows(latent[:, :KV_RANK], latent_gain)
    keys_rope = rotate(latent[:, KV_RANK:], own_pos)
    packed = jnp.concatenate(
        [
            keys_latent[:, :LANES],
            keys_latent[:, LANES:],
            jnp.concatenate([keys_rope[:16], keys_rope[16:32]], axis=1),
            jnp.concatenate([keys_rope[32:], jnp.zeros((16, ROPE), jnp.bfloat16)], axis=1),
        ],
        axis=0,
    )
    packed, pieces = lax.optimization_barrier((packed, pieces))
    keys_own = to_everyone(packed, SP)

    queries = jnp.dot(pieces, mla_query, preferred_element_type=jnp.float32).astype(jnp.bfloat16)
    swa_q = jnp.dot(pieces, swa_query, preferred_element_type=jnp.float32).astype(jnp.bfloat16)
    swa_k = jnp.dot(pieces, swa_key, preferred_element_type=jnp.float32).astype(jnp.bfloat16)
    swa_v = jnp.dot(pieces, swa_value, preferred_element_type=jnp.float32).astype(jnp.bfloat16)
    query = jnp.concatenate(
        [
            queries[:, :NOPE],
            rotate(queries[:, NOPE:], block_pos),
            jnp.zeros((ROWS, LANES - ROPE), jnp.bfloat16),
        ],
        axis=1,
    )
    around = jnp.stack([query] + [from_x(query, k) for k in range(1, 4)], axis=0)
    q_heads = []
    for j in range(HEADS_CORE):
        q_j = lax.dynamic_index_in_dim(around, (x_rank - j) % HEADS_CORE, 0, keepdims=False)
        up = lax.dynamic_slice_in_dim(key_up, (2 * j + c_rank) * NOPE, NOPE, 1)
        lat = lax.dot_general(
            q_j[:, :NOPE], up, (((1,), (1,)), ((), ())), preferred_element_type=jnp.float32
        ).astype(jnp.bfloat16)
        q_heads.append(jnp.concatenate([lat, q_j[:, NOPE:]], axis=1))
    q_all = jnp.concatenate(q_heads, axis=0)

    tail = jnp.concatenate([swa_k[ROWS - WINDOW :], swa_v[ROWS - WINDOW :]], axis=1)
    count = lax.axis_size(SP)
    before = lax.ppermute(tail, SP, [(i, i + 1) for i in range(count - 1)])
    window_keys = jnp.concatenate([before[:, :HEAD], swa_k], axis=0)
    window_values = jnp.concatenate([before[:, HEAD:], swa_v], axis=0)
    scores = jnp.einsum(
        "tgd,sd->gts",
        swa_q.reshape(ROWS, heads_swa, HEAD),
        window_keys,
        preferred_element_type=jnp.float32,
    ) * HEAD ** (-0.5)
    key_pos = offset - WINDOW + jnp.arange(WINDOW + ROWS, dtype=jnp.int32)
    distance = block_pos[:, None] - key_pos[None, :]
    allowed = (distance >= 0) & (distance < WINDOW) & (key_pos[None, :] >= 0)
    scores = jnp.where(allowed, scores, MASKED_VALUE)
    sink = lax.dynamic_slice_in_dim(sink_logits, tp_rank * heads_swa, heads_swa, 0)
    sink = sink.reshape(heads_swa, 1, 1)
    row_max = jnp.maximum(jnp.max(scores, axis=-1, keepdims=True), sink)
    raw = jnp.exp(scores - row_max)
    weights = (
        raw / (jnp.sum(raw, axis=-1, keepdims=True) + jnp.exp(sink - row_max))
    ).astype(jnp.bfloat16)
    swa_out = jnp.einsum("gts,sd->tgd", weights, window_values, preferred_element_type=jnp.float32)
    swa_out = swa_out.astype(jnp.bfloat16).reshape(ROWS, heads_swa * HEAD)

    swa_out, keys_own = lax.optimization_barrier((swa_out, keys_own))
    keys_other = from_core(keys_own)
    rank_own = jnp.stack([block, tp_rank]).astype(jnp.int32)
    rank_other = jnp.stack([block, tp_rank + 1 - 2 * c_rank]).astype(jnp.int32)
    state = attend(rank_own, keys_own, q_all, None)
    partial = attend(rank_other, keys_other, q_all, state)
    all_swa = to_everyone(swa_out, TP)
    parts = exchange(partial, "x").astype(jnp.float32)
    stats = parts[:, KV_RANK:]
    m = stats[:, 0] + stats[:, 1] + stats[:, 2]
    l = stats[:, 3] + stats[:, 4]
    w = jnp.exp2((m - jnp.max(m, axis=0)) * EXP_SCALE)
    denominator = jnp.sum(l * w, axis=0)
    weighted = jnp.sum(parts[:, :KV_RANK] * w[:, None], axis=0)
    latent_out = (weighted / denominator).astype(jnp.bfloat16)
    up = lax.dynamic_slice_in_dim(value_up, tp_rank * VDIM, VDIM, 1)
    mla_out = lax.dot_general(
        latent_out, up, (((0,), (0,)), ((), ())), preferred_element_type=jnp.float32
    ).astype(jnp.bfloat16)
    all_mla = to_everyone(mla_out, TP)
    from_swa = jnp.einsum(
        "rtd,rdn->tn", all_swa, out_swa.reshape(8, -1, 256), preferred_element_type=jnp.float32
    )
    from_mla = jnp.einsum(
        "rtd,rdn->tn", all_mla, out_mla.reshape(8, -1, 256), preferred_element_type=jnp.float32
    )
    return (from_mla + from_swa).astype(jnp.bfloat16)


def solution(mesh):
    split = Mesh(mesh.devices.reshape(8, 8, 4, 2), SP_TP)
    placed = (
        P(SP_TP, None),
        P(),
        P(SP, None),
        P(SP, None),
        P(),
        P(None, TP),
        P(),
        P(),
        P(None, TP),
        P(None, TP),
        P(None, TP),
        P(),
        P(None, TP),
        P(None, TP),
    )
    return jax.shard_map(
        shards, mesh=split, in_specs=placed, out_specs=P(SP, TP), check_vma=False
    )
```

time: 361 us -> 231 us (0.64)
  the two profiles are of different devices: /device:TPU:1 before, /device:TPU:384 now
where the time goes in v1:
time: 231 us; the launch traced here: 230 us
  waiting for transfers between devices  96 us (42%)
  starting transfers between devices  55.5 us (24%)
  Pallas kernels  53.4 us (23%)
  matrix products  8.3 us (4%)
  local copies, waits for them, and re-layouts  8.29 us (4%)
  other arithmetic  7.33 us (3%)
    all_to_all x7, waiting for transfers between devices, exchange(): return lax.all_to_all(array, axis, split_axis=0, concat_axis=0, tiled=True)  64.2 us
    pallas_call x2, Pallas kernels, attend(): pl.pallas_call(functools.partial(attend_body, first=first, last=not first...  53.4 us
    all_to_all x7, starting transfers between devices, exchange(): return lax.all_to_all(array, axis, split_axis=0, concat_axis=0, tiled=True)  38.7 us
    ppermute x1, waiting for transfers between devices, shards(): before = lax.ppermute(tail, SP, [(i, i + 1) for i in range(count - 1)])  31.8 us
    ppermute x3, starting transfers between devices, from_x(): lax.ppermute(value, 'x', [(i, (i + step) % count) for i in range(count)])  9.58 us
    broadcast_in_dim x5, local copies, waits for them, and re-layouts, to_everyone(): copies = jnp.broadcast_to(array, (lax.axis_size(axis), *array.shape))  5.5 us
  transfers between devices with their start and end apart: 13, of which 8 were waited for; matrix products, arithmetic and copies ran while one was open for 5% of the time, Pallas kernels for 12%

profile of v1, /device:TPU:384, one launch (start us, length us, event | category | flops | bytes accessed | tf_op | source)
XLA Modules:
  0.0 229.6 jit_solution(14665089733242500245)
XLA Ops:
  0.0 1.1 fusion.6
  1.2 1.1 fusion.8
  2.2 1.0 broadcast_in_dim.20
  3.2 4.3 %all-to-all-start = ((bf16[4,48,2048]{2,1,0:T(8,128)(2,1)}), bf16[4,48,2048]{2,1,0:T(8,128)(2,1)S(1)}, u32[]{:S(2)}, u32[]{:S(2)}) async-start(bf16[4,48,2048]{2,1,0:T(8,128)(2,1)} %broadcast_in_dim.20), calls=%async_computation | async-start | bytes 1572864 | tf_op jit(solution)/shard_map/all_to_all | solution.py:39
  7.7 12.1 %all-to-all-done = bf16[4,48,2048]{2,1,0:T(8,128)(2,1)S(1)} async-done(((bf16[4,48,2048]{2,1,0:T(8,128)(2,1)}), bf16[4,48,2048]{2,1,0:T(8,128)(2,1)S(1)}, u32[]{:S(2)}, u32[]{:S(2)}) %all-to-all-start) | async-done | bytes 786464 | tf_op jit(solution)/shard_map/all_to_all | solution.py:39
  19.8 0.7 broadcast_in_dim.21
  20.5 11.4 %all-to-all-start.1 = ((bf16[64,16,128]{2,1,0:T(8,128)(2,1)}), bf16[64,16,128]{2,1,0:T(8,128)(2,1)S(1)}, u32[]{:S(2)}, u32[]{:S(2)}) async-start(bf16[64,16,128]{2,1,0:T(8,128)(2,1)} %broadcast_in_dim.21), calls=%async_computation.1 | async-start | bytes 524288 | tf_op jit(solution)/shard_map/all_to_all | solution.py:39
  32.0 1.9 collective-permute-start
  33.9 8.5 %all-to-all-done.1 = bf16[64,16,128]{2,1,0:T(8,128)(2,1)S(1)} async-done(((bf16[64,16,128]{2,1,0:T(8,128)(2,1)}), bf16[64,16,128]{2,1,0:T(8,128)(2,1)S(1)}, u32[]{:S(2)}, u32[]{:S(2)}) %all-to-all-start.1) | async-done | bytes 262176 | tf_op jit(solution)/shard_map/all_to_all | solution.py:39
  43.0 0.6 convolution_convert_fusion.10
  43.7 0.8 reshape.149
  44.4 3.3 %all-to-all-start.2 = ((bf16[8,2,960]{2,1,0:T(2,128)(2,1)}), bf16[8,2,960]{2,1,0:T(2,128)(2,1)S(1)}, u32[]{:S(2)}, u32[]{:S(2)}) async-start(bf16[8,2,960]{2,1,0:T(2,128)(2,1)} %reshape.149), calls=%async_computation.2 | async-start | bytes 65536 | tf_op jit(solution)/shard_map/all_to_all | solution.py:39
  47.8 5.4 %all-to-all-done.2 = bf16[8,2,960]{2,1,0:T(2,128)(2,1)S(1)} async-done(((bf16[8,2,960]{2,1,0:T(2,128)(2,1)}), bf16[8,2,960]{2,1,0:T(2,128)(2,1)S(1)}, u32[]{:S(2)}, u32[]{:S(2)}) %all-to-all-start.2) | async-done | bytes 30752 | tf_op jit(solution)/shard_map/all_to_all | solution.py:39
  54.2 1.8 broadcast_in_dim.24
  56.0 9.0 %all-to-all-start.3 = ((bf16[64,128,128]{2,1,0:T(8,128)(2,1)}), bf16[64,128,128]{2,1,0:T(8,128)(2,1)}, u32[]{:S(2)}, u32[]{:S(2)}) async-start(bf16[64,128,128]{2,1,0:T(8,128)(2,1)} %broadcast_in_dim.24), calls=%async_computation.3 | async-start | bytes 4194304 | tf_op jit(solution)/shard_map/all_to_all | solution.py:39
  65.3 0.6 pad_add_fusion.1.where_ref
  65.9 0.6 pad_add_fusion.where_ref
  66.5 0.3 fusion.5
  66.8 0.7 convolution_convert_fusion.4
  67.5 0.3 fusion.30
  67.9 2.6 %collective-permute-start.3 = (bf16[384,256]{0,1:T(8,128)(2,1)S(1)}, bf16[384,256]{0,1:T(8,128)(2,1)S(1)}, u32[]{:S(2)}, u32[]{:S(2)}) collective-permute-start(bf16[384,256]{0,1:T(8,128)(2,1)S(1)} %maximum_maximum_fusion.1), channel_id=1, source_target_pairs={{0,2},{2,4},{4,6},{6,0},{1,3},{3,5},{5,7},{7,1},{8,10},{10,12},{12... | collective-permute-start | bytes 589832 | tf_op jit(solution)/shard_map/ppermute | solution.py:53
  70.6 3.9 %collective-permute-start.4 = (bf16[384,256]{0,1:T(8,128)(2,1)S(1)}, bf16[384,256]{0,1:T(8,128)(2,1)S(1)}, u32[]{:S(2)}, u32[]{:S(2)}) collective-permute-start(bf16[384,256]{0,1:T(8,128)(2,1)S(1)} %maximum_maximum_fusion.1), channel_id=1, source_target_pairs={{0,4},{2,6},{4,0},{6,2},{1,5},{3,7},{5,1},{7,3},{8,12},{10,14},{12... | collective-permute-start | bytes 589832 | tf_op jit(solution)/shard_map/ppermute | solution.py:53
  74.5 3.0 %collective-permute-start.5 = (bf16[384,256]{0,1:T(8,128)(2,1)S(1)}, bf16[384,256]{0,1:T(8,128)(2,1)S(1)}, u32[]{:S(2)}, u32[]{:S(2)}) collective-permute-start(bf16[384,256]{0,1:T(8,128)(2,1)S(1)} %maximum_maximum_fusion.1), channel_id=1, source_target_pairs={{0,6},{2,0},{4,2},{6,4},{1,7},{3,1},{5,3},{7,5},{8,14},{10,8},{12,... | collective-permute-start | bytes 589832 | tf_op jit(solution)/shard_map/ppermute | solution.py:53
  77.5 0.6 convolution_convert_fusion.9
  78.2 0.6 convolution_convert_fusion.8
  78.8 3.4 %collective-permute-start.1 = (bf16[128,128]{0,1:T(8,128)(2,1)S(1)}, bf16[128,128]{0,1:T(8,128)(2,1)S(1)}, u32[]{:S(2)}, u32[]{:S(2)}) collective-permute-start(bf16[128,128]{0,1:T(8,128)(2,1)S(1)} %pad_maximum_fusion.4), channel_id=1, source_target_pairs={{0,8},{8,16},{16,24},{24,32},{32,40},{40,48},{48,56},{56,64},{64,7... | collective-permute-start | bytes 98312 | tf_op jit(solution)/shard_map/ppermute | solution.py:290
  82.2 0.6 convolution_convert_fusion.6
  82.8 31.8 %collective-permute-done.1 = bf16[128,128]{0,1:T(8,128)(2,1)S(1)} collective-permute-done((bf16[128,128]{0,1:T(8,128)(2,1)S(1)}, bf16[128,128]{0,1:T(8,128)(2,1)S(1)}, u32[]{:S(2)}, u32[]{:S(2)}) %collective-permute-start.1) | collective-permute-done | bytes 32800 | tf_op jit(solution)/shard_map/ppermute | solution.py:290
  114.6 0.5 fusion.66
  115.1 0.2 fusion.1
  115.4 0.4 convolution_convert_fusion.5
  115.8 0.4 all-to-all-done.3.keys_ref
  116.3 1.9 collective-permute-start.2
  119.2 0.4 copy-done.5
  120.5 1.2 maximum_maximum_fusion.q_ref
  121.7 26.6 %attend_first.1 = (f32[6,256,256]{2,1,0:T(8,128)}, f32[6,1,256]{2,1,0:T(1,128)}, f32[6,1,256]{2,1,0:T(1,128)}) custom-call(s32[2]{0:T(128)} %pad_add_fusion.1.where_ref, bf16[64,128,128]{2,1,0:T(8,128)(2,1)} %all-to-all-done.3.keys_ref, bf16[1536,384]{1,0:T(8,128)(2,1)} %maximum_maximum_fusion.q_ref), custom_call_target="tpu_custom_call" | custom-call | flops 6039797760 | bytes 6000000 | tf_op jit(solution)/shard_map/attend_first/pallas_call | solution.py:192
  148.3 26.8 %attend_last.1 = bf16[4,272,384]{2,1,0:T(8,128)(2,1)} custom-call(s32[2]{0:T(128)} %pad_add_fusion.where_ref, bf16[64,128,128]{2,1,0:T(8,128)(2,1)} %collective-permute-done.2.keys_ref, bf16[1536,384]{1,0:T(8,128)(2,1)} %maximum_maximum_fusion.q_ref, f32[6,256,256]{2,1,0:T(8,128)} %get-tuple-element.15.refs_0_, f32[6,1,256]{2,1,0:T(1,128)} %get-tuple-element.16.refs_1_, ...), custom_call_target="tpu_custom_call" | custom-call | flops 6039797760 | bytes 6000000 | tf_op jit(solution)/shard_map/attend_last/pallas_call | solution.py:192
  175.1 3.5 %all-to-all-start.4 = ((bf16[4,272,384]{2,1,0:T(8,128)(2,1)}), bf16[4,272,384]{2,1,0:T(8,128)(2,1)S(1)}, u32[]{:S(2)}, u32[]{:S(2)}) async-start(bf16[4,272,384]{2,1,0:T(8,128)(2,1)} %attend_last.1), calls=%async_computation.4 | async-start | bytes 1671168 | tf_op jit(solution)/shard_map/all_to_all | solution.py:39
  178.7 13.6 %all-to-all-done.4 = bf16[4,272,384]{2,1,0:T(8,128)(2,1)S(1)} async-done(((bf16[4,272,384]{2,1,0:T(8,128)(2,1)}), bf16[4,272,384]{2,1,0:T(8,128)(2,1)S(1)}, u32[]{:S(2)}, u32[]{:S(2)}) %all-to-all-start.4) | async-done | bytes 835616 | tf_op jit(solution)/shard_map/all_to_all | solution.py:39
  192.3 1.0 broadcast_in_dim.50
  193.3 3.5 %all-to-all-start.6 = ((bf16[8,384,128]{2,1,0:T(8,128)(2,1)}), bf16[8,384,128]{2,1,0:T(8,128)(2,1)S(1)}, u32[]{:S(2)}, u32[]{:S(2)}) async-start(bf16[8,384,128]{2,1,0:T(8,128)(2,1)} %broadcast_in_dim.50), calls=%async_computation.6 | async-start | bytes 1572864 | tf_op jit(solution)/shard_map/all_to_all | solution.py:39
  197.2 1.1 convolution_convert_fusion.7
  198.3 11.6 %all-to-all-done.6 = bf16[8,384,128]{2,1,0:T(8,128)(2,1)S(1)} async-done(((bf16[8,384,128]{2,1,0:T(8,128)(2,1)}), bf16[8,384,128]{2,1,0:T(8,128)(2,1)S(1)}, u32[]{:S(2)}, u32[]{:S(2)}) %all-to-all-start.6) | async-done | bytes 786464 | tf_op jit(solution)/shard_map/all_to_all | solution.py:39
  209.9 1.0 broadcast_in_dim.26
  210.9 3.5 %all-to-all-start.5 = ((bf16[8,384,128]{2,1,0:T(8,128)(2,1)}), bf16[8,384,128]{2,1,0:T(8,128)(2,1)S(1)}, u32[]{:S(2)}, u32[]{:S(2)}) async-start(bf16[8,384,128]{2,1,0:T(8,128)(2,1)} %broadcast_in_dim.26), calls=%async_computation.5 | async-start | bytes 1572864 | tf_op jit(solution)/shard_map/all_to_all | solution.py:39
  214.5 0.4 convolution_bitcast_fusion
  214.9 12.7 %all-to-all-done.5 = bf16[8,384,128]{2,1,0:T(8,128)(2,1)S(1)} async-done(((bf16[8,384,128]{2,1,0:T(8,128)(2,1)}), bf16[8,384,128]{2,1,0:T(8,128)(2,1)S(1)}, u32[]{:S(2)}, u32[]{:S(2)}) %all-to-all-start.5) | async-done | bytes 786464 | tf_op jit(solution)/shard_map/all_to_all | solution.py:39
  227.5 2.1 fusion.3
  (90 shorter events, 4.5 us)
Async XLA Ops:
  0.0 66.8 %copy-start = (bf16[2048,192]{0,1:T(8,128)(2,1)S(1)}, bf16[2048,192]{0,1:T(8,128)(2,1)}, u32[]{:S(2)}) copy-start(bf16[2048,192]{0,1:T(8,128)(2,1)} %param.19) | copy-start | bytes 2359300
  0.0 7.5 %copy-start.6 = (bf16[32,256]{1,0:T(8,128)(2,1)S(1)}, bf16[32,256]{1,0:T(8,128)(2,1)}, u32[]{:S(2)}) copy-start(bf16[32,256]{1,0:T(8,128)(2,1)} %param.16) | copy-start | bytes 49156
  0.0 7.5 %copy-start.7 = (bf16[32,64]{1,0:T(8,128)(2,1)S(1)}, bf16[32,64]{1,0:T(8,128)(2,1)}, u32[]{:S(2)}) copy-start(bf16[32,64]{1,0:T(8,128)(2,1)} %param.17) | copy-start | bytes 12292
  3.2 16.6 %all-to-all-start = ((bf16[4,48,2048]{2,1,0:T(8,128)(2,1)}), bf16[4,48,2048]{2,1,0:T(8,128)(2,1)S(1)}, u32[]{:S(2)}, u32[]{:S(2)}) async-start(bf16[4,48,2048]{2,1,0:T(8,128)(2,1)} %broadcast_in_dim.20), calls=%async_computation | async-start | bytes 1572864 | tf_op jit(solution)/shard_map/all_to_all | solution.py:39
  20.5 21.9 %all-to-all-start.1 = ((bf16[64,16,128]{2,1,0:T(8,128)(2,1)}), bf16[64,16,128]{2,1,0:T(8,128)(2,1)S(1)}, u32[]{:S(2)}, u32[]{:S(2)}) async-start(bf16[64,16,128]{2,1,0:T(8,128)(2,1)} %broadcast_in_dim.21), calls=%async_computation.1 | async-start | bytes 524288 | tf_op jit(solution)/shard_map/all_to_all | solution.py:39
  32.0 10.7 %collective-permute-start = (bf16[4,48,2048]{2,1,0:T(8,128)(2,1)S(1)}, bf16[4,48,2048]{2,1,0:T(8,128)(2,1)S(1)}, u32[]{:S(2)}, u32[]{:S(2)}) collective-permute-start(bf16[4,48,2048]{2,1,0:T(8,128)(2,1)S(1)} %all-to-all-done), channel_id=1, source_target_pairs={{0,1},{1,0},{2,3},{3,2},{4,5},{5,4},{6,7},{7,6},{8,9},{9,8},{10,11... | collective-permute-start | bytes 2359304 | tf_op jit(solution)/shard_map/ppermute | solution.py:48
  42.9 11.0 %copy-start.8 = (f32[256]{0:T(256)S(1)}, f32[256]{0:T(256)}, u32[]{:S(2)}) copy-start(f32[256]{0:T(256)} %param.18) | copy-start | bytes 3076
  44.4 8.7 %all-to-all-start.2 = ((bf16[8,2,960]{2,1,0:T(2,128)(2,1)}), bf16[8,2,960]{2,1,0:T(2,128)(2,1)S(1)}, u32[]{:S(2)}, u32[]{:S(2)}) async-start(bf16[8,2,960]{2,1,0:T(2,128)(2,1)} %reshape.149), calls=%async_computation.2 | async-start | bytes 65536 | tf_op jit(solution)/shard_map/all_to_all | solution.py:39
  56.0 9.2 %copy-start.9 = (f32[16]{0:T(128)S(1)}, f32[16]{0:T(128)}, u32[]{:S(2)}) copy-start(f32[16]{0:T(128)} %param.25) | copy-start | bytes 196
  56.0 60.3 %all-to-all-start.3 = ((bf16[64,128,128]{2,1,0:T(8,128)(2,1)}), bf16[64,128,128]{2,1,0:T(8,128)(2,1)}, u32[]{:S(2)}, u32[]{:S(2)}) async-start(bf16[64,128,128]{2,1,0:T(8,128)(2,1)} %broadcast_in_dim.24), calls=%async_computation.3 | async-start | bytes 4194304 | tf_op jit(solution)/shard_map/all_to_all | solution.py:39
  66.8 10.8 %copy-start.3 = (bf16[2048,64]{0,1:T(8,128)(2,1)S(1)}, bf16[2048,64]{0,1:T(8,128)(2,1)}, u32[]{:S(2)}) copy-start(bf16[2048,64]{0,1:T(8,128)(2,1)} %param.23) | copy-start | bytes 786436
  67.5 10.7 %copy-start.4 = (bf16[2048,64]{0,1:T(8,128)(2,1)S(1)}, bf16[2048,64]{0,1:T(8,128)(2,1)}, u32[]{:S(2)}) copy-start(bf16[2048,64]{0,1:T(8,128)(2,1)} %param.24) | copy-start | bytes 786436
  67.9 14.3 %copy-start.2 = (bf16[2048,128]{1,0:T(8,128)(2,1)S(1)}, bf16[2048,128]{1,0:T(8,128)(2,1)}, u32[]{:S(2)}) copy-start(bf16[2048,128]{1,0:T(8,128)(2,1)} %param.22) | copy-start | bytes 1572868
  67.9 50.4 %collective-permute-start.3 = (bf16[384,256]{0,1:T(8,128)(2,1)S(1)}, bf16[384,256]{0,1:T(8,128)(2,1)S(1)}, u32[]{:S(2)}, u32[]{:S(2)}) collective-permute-start(bf16[384,256]{0,1:T(8,128)(2,1)S(1)} %maximum_maximum_fusion.1), channel_id=1, source_target_pairs={{0,2},{2,4},{4,6},{6,0},{1,3},{3,5},{5,7},{7,1},{8,10},{10,12},{12... | collective-permute-start | bytes 589832 | tf_op jit(solution)/shard_map/ppermute | solution.py:53
  70.6 47.8 %collective-permute-start.4 = (bf16[384,256]{0,1:T(8,128)(2,1)S(1)}, bf16[384,256]{0,1:T(8,128)(2,1)S(1)}, u32[]{:S(2)}, u32[]{:S(2)}) collective-permute-start(bf16[384,256]{0,1:T(8,128)(2,1)S(1)} %maximum_maximum_fusion.1), channel_id=1, source_target_pairs={{0,4},{2,6},{4,0},{6,2},{1,5},{3,7},{5,1},{7,3},{8,12},{10,14},{12... | collective-permute-start | bytes 589832 | tf_op jit(solution)/shard_map/ppermute | solution.py:53
  74.5 43.8 %collective-permute-start.5 = (bf16[384,256]{0,1:T(8,128)(2,1)S(1)}, bf16[384,256]{0,1:T(8,128)(2,1)S(1)}, u32[]{:S(2)}, u32[]{:S(2)}) collective-permute-start(bf16[384,256]{0,1:T(8,128)(2,1)S(1)} %maximum_maximum_fusion.1), channel_id=1, source_target_pairs={{0,6},{2,0},{4,2},{6,4},{1,7},{3,1},{5,3},{7,5},{8,14},{10,8},{12,... | collective-permute-start | bytes 589832 | tf_op jit(solution)/shard_map/ppermute | solution.py:53
  78.8 35.8 %collective-permute-start.1 = (bf16[128,128]{0,1:T(8,128)(2,1)S(1)}, bf16[128,128]{0,1:T(8,128)(2,1)S(1)}, u32[]{:S(2)}, u32[]{:S(2)}) collective-permute-start(bf16[128,128]{0,1:T(8,128)(2,1)S(1)} %pad_maximum_fusion.4), channel_id=1, source_target_pairs={{0,8},{8,16},{16,24},{24,32},{32,40},{40,48},{48,56},{56,64},{64,7... | collective-permute-start | bytes 98312 | tf_op jit(solution)/shard_map/ppermute | solution.py:290
  116.3 32.0 %collective-permute-start.2 = (bf16[64,128,128]{2,1,0:T(8,128)(2,1)}, bf16[64,128,128]{2,1,0:T(8,128)(2,1)}, u32[]{:S(2)}, u32[]{:S(2)}) collective-permute-start(bf16[64,128,128]{2,1,0:T(8,128)(2,1)} %all-to-all-done.3.keys_ref), channel_id=1, source_target_pairs={{0,1},{1,0},{2,3},{3,2},{4,5},{5,4},{6,7},{7,6},{8,9},{9,8},{10,11... | collective-permute-start | bytes 6291464 | tf_op jit(solution)/shard_map/ppermute | solution.py:48
  118.6 1.0 copy-start.5
  175.1 17.2 %all-to-all-start.4 = ((bf16[4,272,384]{2,1,0:T(8,128)(2,1)}), bf16[4,272,384]{2,1,0:T(8,128)(2,1)S(1)}, u32[]{:S(2)}, u32[]{:S(2)}) async-start(bf16[4,272,384]{2,1,0:T(8,128)(2,1)} %attend_last.1), calls=%async_computation.4 | async-start | bytes 1671168 | tf_op jit(solution)/shard_map/all_to_all | solution.py:39
  193.3 16.6 %all-to-all-start.6 = ((bf16[8,384,128]{2,1,0:T(8,128)(2,1)}), bf16[8,384,128]{2,1,0:T(8,128)(2,1)S(1)}, u32[]{:S(2)}, u32[]{:S(2)}) async-start(bf16[8,384,128]{2,1,0:T(8,128)(2,1)} %broadcast_in_dim.50), calls=%async_computation.6 | async-start | bytes 1572864 | tf_op jit(solution)/shard_map/all_to_all | solution.py:39
  198.3 16.2 %copy-start.1 = (bf16[1024,256]{1,0:T(8,128)(2,1)S(1)}, bf16[1024,256]{1,0:T(8,128)(2,1)}, u32[]{:S(2)}) copy-start(bf16[1024,256]{1,0:T(8,128)(2,1)} %param.27) | copy-start | bytes 1572868
  210.9 16.6 %all-to-all-start.5 = ((bf16[8,384,128]{2,1,0:T(8,128)(2,1)}), bf16[8,384,128]{2,1,0:T(8,128)(2,1)S(1)}, u32[]{:S(2)}, u32[]{:S(2)}) async-start(bf16[8,384,128]{2,1,0:T(8,128)(2,1)} %broadcast_in_dim.26), calls=%async_computation.5 | async-start | bytes 1572864 | tf_op jit(solution)/shard_map/all_to_all | solution.py:39

commit v2 on v1

--- a/solution.py
+++ b/solution.py
@@ -8,6 +8,7 @@
 from jax.experimental.pallas import tpu as pltpu
 from jax.sharding import Mesh
 from jax.sharding import PartitionSpec as P
+
 
 NOPE = 128
 ROPE = 64
@@ -27,7 +28,7 @@
 SOURCES = 64
 ROWS = 384
 CHUNK = 16
-QTILE = 256
+QTILE = 512
 HEADS_CORE = 4
 QROWS = HEADS_CORE * ROWS
 TILES = QROWS // QTILE
@@ -110,17 +111,19 @@
         kc_ref[:, :LANES] = k0
         kc_ref[:, LANES : 2 * LANES] = k1
         kc_ref[:, 2 * LANES :] = kr
-        vt_ref[:LANES] = k0.T
-        vt_ref[LANES:] = k1.T
         if masked:
             row = lax.broadcasted_iota(jnp.int32, (n_keys, 1), 0)
             key_pos = (index * CHUNK + row // OWN) * ROWS + key_rank * OWN + row % OWN
 
-        def tile_step(tile):
-            q = q_ref[pl.ds(tile * QTILE, QTILE)]
-            s = lax.dot_general(
-                kc_ref[...], q, (((1,), (1,)), ((), ())), preferred_element_type=jnp.float32
+        def scores_of(tile):
+            return lax.dot_general(
+                kc_ref[...],
+                q_ref[tile * QTILE : (tile + 1) * QTILE],
+                (((1,), (1,)), ((), ())),
+                preferred_element_type=jnp.float32,
             )
+
+        def absorb(tile, s):
             if masked:
                 col = tile * QTILE + lax.broadcasted_iota(jnp.int32, (1, QTILE), 1)
                 allowed = key_pos <= block * ROWS + col % ROWS
@@ -133,16 +136,15 @@
             alpha = jnp.exp2((old - new) * EXP_SCALE)
             m_ref[tile] = new
             l_ref[tile] = l_ref[tile] * alpha + jnp.sum(p, axis=0, keepdims=True)
-            o_ref[tile] = o_ref[tile] * alpha + jnp.dot(
-                vt_ref[...], p.astype(jnp.bfloat16), preferred_element_type=jnp.float32
+            o_ref[tile] = o_ref[tile] * alpha + lax.dot_general(
+                kc_ref[:, : 2 * LANES], p.astype(jnp.bfloat16), (((0,), (0,)), ((), ())), preferred_element_type=jnp.float32
             )
 
-        def pair_step(pair, carry):
-            tile_step(2 * pair)
-            tile_step(2 * pair + 1)
-            return carry
-
-        lax.fori_loop(0, TILES // 2, pair_step, 0)
+        s = scores_of(0)
+        for tile in range(TILES):
+            ahead = scores_of(tile + 1) if tile + 1 < TILES else None
+            absorb(tile, s)
+            s = ahead
 
     def full_step(index, carry):
         chunk_step(index, False)
@@ -202,7 +204,7 @@
     )(*operands)
 
 
-def shards(
+def layer(
     inputs,
     norm_gain,
     latent_down,
@@ -228,6 +230,17 @@
     block_pos = offset + jnp.arange(ROWS, dtype=jnp.int32)
     heads_swa = swa_query.shape[1] // HEAD
 
+    x_count = lax.axis_size("x")
+
+    def in_place(tiles):
+        tiles = tiles.reshape(2, x_count, own_rows, -1)
+        rows = []
+        for x in range(x_count):
+            both = lax.dynamic_index_in_dim(tiles, (x_rank - x) % x_count, 1, keepdims=False)
+            rows.append(lax.dynamic_index_in_dim(both, c_rank, 0, keepdims=False))
+            rows.append(lax.dynamic_index_in_dim(both, 1 - c_rank, 0, keepdims=False))
+        return jnp.concatenate(rows, axis=0)
+
     down = jnp.concatenate([latent_down, rope_down], axis=1)
     width = down.shape[1] // lax.axis_size(TP)
     down = lax.dynamic_slice_in_dim(down, tp_rank * width, width, 1)
@@ -239,13 +252,18 @@
     down = down.reshape(-1, width)
 
     normed = norm_rows(inputs, norm_gain)
-    mine = to_everyone(normed, "x")
+    mine = [normed] + [from_x(normed, k) for k in range(1, x_count)]
+    mine = jnp.concatenate(mine, axis=0)
     other = from_core(mine)
-    is_first = c_rank == 0
-    pieces = jnp.stack([jnp.where(is_first, mine, other), jnp.where(is_first, other, mine)], axis=1)
-    pieces = pieces.reshape(ROWS, -1)
+    pieces = jnp.concatenate([mine, other], axis=0)
 
     latent = jnp.dot(pieces, down, preferred_element_type=jnp.float32).astype(jnp.bfloat16)
+    latent = in_place(latent)
+    kv_weights = jnp.concatenate([swa_key, swa_value], axis=1)
+    swa_kv = jnp.dot(pieces, kv_weights, preferred_element_type=jnp.float32).astype(jnp.bfloat16)
+    swa_kv = in_place(swa_kv)
+    count = lax.axis_size(SP)
+    before = lax.ppermute(swa_kv[ROWS - WINDOW :], SP, [(i, i + 1) for i in range(count - 1)])
     latent = exchange(latent.reshape(-1, own_rows, width), TP)
     latent = jnp.transpose(latent, (1, 0, 2)).reshape(own_rows, KV_RANK + ROPE)
     keys_latent = norm_rows(latent[:, :KV_RANK], latent_gain)
@@ -259,13 +277,11 @@
         ],
         axis=0,
     )
-    packed, pieces = lax.optimization_barrier((packed, pieces))
+    packed, pieces, before = lax.optimization_barrier((packed, pieces, before))
     keys_own = to_everyone(packed, SP)
 
-    queries = jnp.dot(pieces, mla_query, preferred_element_type=jnp.float32).astype(jnp.bfloat16)
-    swa_q = jnp.dot(pieces, swa_query, preferred_element_type=jnp.float32).astype(jnp.bfloat16)
-    swa_k = jnp.dot(pieces, swa_key, preferred_element_type=jnp.float32).astype(jnp.bfloat16)
-    swa_v = jnp.dot(pieces, swa_value, preferred_element_type=jnp.float32).astype(jnp.bfloat16)
+    queries = jnp.dot(pieces, mla_query, preferred_element_type=jnp.float32)
+    queries = in_place(queries.astype(jnp.bfloat16))
     query = jnp.concatenate(
         [
             queries[:, :NOPE],
@@ -274,10 +290,10 @@
         ],
         axis=1,
     )
-    around = jnp.stack([query] + [from_x(query, k) for k in range(1, 4)], axis=0)
+    around = jnp.stack([query] + [from_x(query, k) for k in range(1, x_count)], axis=0)
     q_heads = []
     for j in range(HEADS_CORE):
-        q_j = lax.dynamic_index_in_dim(around, (x_rank - j) % HEADS_CORE, 0, keepdims=False)
+        q_j = lax.dynamic_index_in_dim(around, (x_rank - j) % x_count, 0, keepdims=False)
         up = lax.dynamic_slice_in_dim(key_up, (2 * j + c_rank) * NOPE, NOPE, 1)
         lat = lax.dot_general(
             q_j[:, :NOPE], up, (((1,), (1,)), ((), ())), preferred_element_type=jnp.float32
@@ -285,11 +301,10 @@
         q_heads.append(jnp.concatenate([lat, q_j[:, NOPE:]], axis=1))
     q_all = jnp.concatenate(q_heads, axis=0)
 
-    tail = jnp.concatenate([swa_k[ROWS - WINDOW :], swa_v[ROWS - WINDOW :]], axis=1)
-    count = lax.axis_size(SP)
-    before = lax.ppermute(tail, SP, [(i, i + 1) for i in range(count - 1)])
-    window_keys = jnp.concatenate([before[:, :HEAD], swa_k], axis=0)
-    window_values = jnp.concatenate([before[:, HEAD:], swa_v], axis=0)
+    swa_q = jnp.dot(pieces, swa_query, preferred_element_type=jnp.float32)
+    swa_q = in_place(swa_q.astype(jnp.bfloat16))
+    window = jnp.concatenate([before, swa_kv], axis=0)
+    window_keys, window_values = window[:, :HEAD], window[:, HEAD:]
     scores = jnp.einsum(
         "tgd,sd->gts",
         swa_q.reshape(ROWS, heads_swa, HEAD),
@@ -309,14 +324,21 @@
     ).astype(jnp.bfloat16)
     swa_out = jnp.einsum("gts,sd->tgd", weights, window_values, preferred_element_type=jnp.float32)
     swa_out = swa_out.astype(jnp.bfloat16).reshape(ROWS, heads_swa * HEAD)
-
-    swa_out, keys_own = lax.optimization_barrier((swa_out, keys_own))
+    swa_x = jnp.stack([swa_out] + [from_x(swa_out, k) for k in range(1, x_count)], axis=0)
+    swa_both = jnp.stack([swa_x, from_core(swa_x)], axis=0)
+    from_swa = jnp.zeros((ROWS, out_swa.shape[1]), jnp.float32)
+    for o in range(2):
+        for k in range(x_count):
+            head = (2 * ((x_rank - k) % x_count)) + (c_rank + o) % 2
+            w = lax.dynamic_slice_in_dim(out_swa, head * 2 * HEAD, 2 * HEAD, 0)
+            from_swa += jnp.dot(swa_both[o, k], w, preferred_element_type=jnp.float32)
+
+    keys_own, q_all, from_swa = lax.optimization_barrier((keys_own, q_all, from_swa))
     keys_other = from_core(keys_own)
     rank_own = jnp.stack([block, tp_rank]).astype(jnp.int32)
     rank_other = jnp.stack([block, tp_rank + 1 - 2 * c_rank]).astype(jnp.int32)
     state = attend(rank_own, keys_own, q_all, None)
     partial = attend(rank_other, keys_other, q_all, state)
-    all_swa = to_everyone(swa_out, TP)
     parts = exchange(partial, "x").astype(jnp.float32)
     stats = parts[:, KV_RANK:]
     m = stats[:, 0] + stats[:, 1] + stats[:, 2]
@@ -330,9 +352,6 @@
         latent_out, up, (((0,), (0,)), ((), ())), preferred_element_type=jnp.float32
     ).astype(jnp.bfloat16)
     all_mla = to_everyone(mla_out, TP)
-    from_swa = jnp.einsum(
-        "rtd,rdn->tn", all_swa, out_swa.reshape(8, -1, 256), preferred_element_type=jnp.float32
-    )
     from_mla = jnp.einsum(
         "rtd,rdn->tn", all_mla, out_mla.reshape(8, -1, 256), preferred_element_type=jnp.float32
     )
@@ -357,6 +376,4 @@
         P(None, TP),
         P(None, TP),
     )
-    return jax.shard_map(
-        shards, mesh=split, in_specs=placed, out_specs=P(SP, TP), check_vma=False
-    )
+    return jax.shard_map(layer, mesh=split, in_specs=placed, out_specs=P(SP, TP), check_vma=False)

time: 231 us -> 195 us (0.84)
  the two profiles are of different devices: /device:TPU:384 before, /device:TPU:472 now
where the time goes in v2:
time: 195 us; the launch traced here: 193 us
  starting transfers between devices  70 us (36%)
  waiting for transfers between devices  39.1 us (20%)
  Pallas kernels  29.3 us (15%)
  blocking collectives  15.7 us (8%)
  local copies, waits for them, and re-layouts  14.4 us (7%)
  other arithmetic  12 us (6%)
  matrix products  11.7 us (6%)
    all_to_all x4, waiting for transfers between devices, exchange(): return lax.all_to_all(array, axis, split_axis=0, concat_axis=0, tiled=True)  35.8 us
    ppermute x9, starting transfers between devices, from_x(): lax.ppermute(value, 'x', [(i, (i + step) % count) for i in range(count)])  31.1 us
    all_to_all x4, starting transfers between devices, exchange(): return lax.all_to_all(array, axis, split_axis=0, concat_axis=0, tiled=True)  30.5 us
    pallas_call x2, Pallas kernels, attend(): pl.pallas_call(functools.partial(attend_body, first=first, last=not first...  29.3 us
    all_to_all x1, blocking collectives, exchange(): return lax.all_to_all(array, axis, split_axis=0, concat_axis=0, tiled=True)  15.7 us
    ppermute x3, starting transfers between devices, from_core(): return lax.ppermute(value, 'c', [(0, 1), (1, 0)])  5.91 us
    dot_general x8, matrix products, layer(): from_swa += jnp.dot(swa_both[o, k], w, preferred_element_type=jnp.float32)  5.49 us
  transfers between devices with their start and end apart: 17, of which 4 were waited for; matrix products, arithmetic and copies ran while one was open for 14% of the time, Pallas kernels for 7%

profile of v2, /device:TPU:472, one launch (start us, length us, event | category | flops | bytes accessed | tf_op | source)
XLA Modules:
  0.0 193.3 jit_solution(14875877342357583186)
XLA Ops:
  0.0 1.2 fusion.12
  1.2 1.1 constant_dynamic-update-slice_fusion.4
  2.2 3.4 %collective-permute-start = (bf16[48,2048]{1,0:T(8,128)(2,1)S(1)}, bf16[48,2048]{1,0:T(8,128)(2,1)S(1)}, u32[]{:S(2)}, u32[]{:S(2)}) collective-permute-start(bf16[48,2048]{1,0:T(8,128)(2,1)S(1)} %get-tuple-element.26), channel_id=1, source_target_pairs={{0,2},{2,4},{4,6},{6,0},{1,3},{3,5},{5,7},{7,1},{8,10},{10,12},{12... | collective-permute-start | bytes 589832 | tf_op jit(solution)/shard_map/ppermute | solution.py:54
  5.7 4.6 %collective-permute-start.1 = (bf16[48,2048]{1,0:T(8,128)(2,1)S(1)}, bf16[48,2048]{1,0:T(8,128)(2,1)S(1)}, u32[]{:S(2)}, u32[]{:S(2)}) collective-permute-start(bf16[48,2048]{1,0:T(8,128)(2,1)S(1)} %get-tuple-element.26), channel_id=1, source_target_pairs={{0,4},{2,6},{4,0},{6,2},{1,5},{3,7},{5,1},{7,3},{8,12},{10,14},{12... | collective-permute-start | bytes 589832 | tf_op jit(solution)/shard_map/ppermute | solution.py:54
  10.3 3.3 %collective-permute-start.2 = (bf16[48,2048]{1,0:T(8,128)(2,1)S(1)}, bf16[48,2048]{1,0:T(8,128)(2,1)S(1)}, u32[]{:S(2)}, u32[]{:S(2)}) collective-permute-start(bf16[48,2048]{1,0:T(8,128)(2,1)S(1)} %get-tuple-element.26), channel_id=1, source_target_pairs={{0,6},{2,0},{4,2},{6,4},{1,7},{3,1},{5,3},{7,5},{8,14},{10,8},{12,... | collective-permute-start | bytes 589832 | tf_op jit(solution)/shard_map/ppermute | solution.py:54
  13.7 0.8 fusion.68
  14.6 0.8 broadcast_in_dim.14
  15.3 10.3 %all-to-all-start = ((bf16[64,16,128]{2,1,0:T(8,128)(2,1)}), bf16[64,16,128]{2,1,0:T(8,128)(2,1)S(1)}, u32[]{:S(2)}, u32[]{:S(2)}) async-start(bf16[64,16,128]{2,1,0:T(8,128)(2,1)} %broadcast_in_dim.14), calls=%async_computation | async-start | bytes 524288 | tf_op jit(solution)/shard_map/all_to_all | solution.py:40
  26.6 1.0 fusion.8
  27.6 0.9 pad_maximum_fusion
  28.5 1.9 collective-permute-start.3
  30.5 4.9 %all-to-all-done = bf16[64,16,128]{2,1,0:T(8,128)(2,1)S(1)} async-done(((bf16[64,16,128]{2,1,0:T(8,128)(2,1)}), bf16[64,16,128]{2,1,0:T(8,128)(2,1)S(1)}, u32[]{:S(2)}, u32[]{:S(2)}) %all-to-all-start) | async-done | bytes 262176 | tf_op jit(solution)/shard_map/all_to_all | solution.py:40
  35.7 1.2 constant_dynamic-update-slice_fusion
  38.1 0.7 reshape.233
  38.9 3.3 %all-to-all-start.1 = ((bf16[8,2,960]{2,1,0:T(2,128)(2,1)}), bf16[8,2,960]{2,1,0:T(2,128)(2,1)S(1)}, u32[]{:S(2)}, u32[]{:S(2)}) async-start(bf16[8,2,960]{2,1,0:T(2,128)(2,1)} %reshape.233), calls=%async_computation.1 | async-start | bytes 65536 | tf_op jit(solution)/shard_map/all_to_all | solution.py:40
  43.3 2.5 %collective-permute-start.4 = (bf16[128,128]{0,1:T(8,128)(2,1)S(1)}, bf16[128,128]{0,1:T(8,128)(2,1)}, u32[]{:S(2)}, u32[]{:S(2)}) collective-permute-start(bf16[128,128]{0,1:T(8,128)(2,1)S(1)} %pad_maximum_fusion.4), channel_id=1, source_target_pairs={{0,8},{8,16},{16,24},{24,32},{32,40},{40,48},{48,56},{56,64},{64,7... | collective-permute-start | bytes 98312 | tf_op jit(solution)/shard_map/ppermute | solution.py:266
  45.9 0.7 copy.150
  46.6 0.7 copy.151
  47.3 0.7 copy.152
  48.1 0.7 copy.153
  52.1 0.8 maximum_maximum_fusion.1
  52.9 5.1 %collective-permute-start.7 = (bf16[384,256]{0,1:T(8,128)(2,1)}, bf16[384,256]{0,1:T(8,128)(2,1)S(1)}, u32[]{:S(2)}, u32[]{:S(2)}) collective-permute-start(bf16[384,256]{0,1:T(8,128)(2,1)} %maximum_maximum_fusion.1), channel_id=1, source_target_pairs={{0,6},{2,0},{4,2},{6,4},{1,7},{3,1},{5,3},{7,5},{8,14},{10,8},{12,... | collective-permute-start | bytes 589832 | tf_op jit(solution)/shard_map/ppermute | solution.py:54
  58.0 2.7 %collective-permute-start.6 = (bf16[384,256]{0,1:T(8,128)(2,1)}, bf16[384,256]{0,1:T(8,128)(2,1)}, u32[]{:S(2)}, u32[]{:S(2)}) collective-permute-start(bf16[384,256]{0,1:T(8,128)(2,1)} %maximum_maximum_fusion.1), channel_id=1, source_target_pairs={{0,4},{2,6},{4,0},{6,2},{1,5},{3,7},{5,1},{7,3},{8,12},{10,14},{12... | collective-permute-start | bytes 589832 | tf_op jit(solution)/shard_map/ppermute | solution.py:54
  60.7 1.8 broadcast_in_dim.15
  62.6 11.3 %all-to-all-start.2 = ((bf16[64,128,128]{2,1,0:T(8,128)(2,1)}), bf16[64,128,128]{2,1,0:T(8,128)(2,1)}, u32[]{:S(2)}, u32[]{:S(2)}) async-start(bf16[64,128,128]{2,1,0:T(8,128)(2,1)} %broadcast_in_dim.15), calls=%async_computation.2 | async-start | bytes 4194304 | tf_op jit(solution)/shard_map/all_to_all | solution.py:40
  75.5 1.0 concatenate.102
  77.9 2.8 %collective-permute-start.10 = (bf16[384,128]{0,1:T(8,128)(2,1)S(1)}, bf16[384,128]{0,1:T(8,128)(2,1)S(1)}, u32[]{:S(2)}, u32[]{:S(2)}) collective-permute-start(bf16[384,128]{0,1:T(8,128)(2,1)S(1)} %bitcast.193), channel_id=1, source_target_pairs={{0,6},{2,0},{4,2},{6,4},{1,7},{3,1},{5,3},{7,5},{8,14},{10,8},{12,... | collective-permute-start | bytes 294920 | tf_op jit(solution)/shard_map/ppermute | solution.py:54
  80.7 4.1 %collective-permute-start.9 = (bf16[384,128]{0,1:T(8,128)(2,1)S(1)}, bf16[384,128]{0,1:T(8,128)(2,1)S(1)}, u32[]{:S(2)}, u32[]{:S(2)}) collective-permute-start(bf16[384,128]{0,1:T(8,128)(2,1)S(1)} %bitcast.194), channel_id=1, source_target_pairs={{0,4},{2,6},{4,0},{6,2},{1,5},{3,7},{5,1},{7,3},{8,12},{10,14},{12... | collective-permute-start | bytes 294920 | tf_op jit(solution)/shard_map/ppermute | solution.py:54
  84.8 3.1 %collective-permute-start.8 = (bf16[384,128]{0,1:T(8,128)(2,1)S(1)}, bf16[384,128]{0,1:T(8,128)(2,1)S(1)}, u32[]{:S(2)}, u32[]{:S(2)}) collective-permute-start(bf16[384,128]{0,1:T(8,128)(2,1)S(1)} %bitcast.195), channel_id=1, source_target_pairs={{0,2},{2,4},{4,6},{6,0},{1,3},{3,5},{5,7},{7,1},{8,10},{10,12},{12... | collective-permute-start | bytes 294920 | tf_op jit(solution)/shard_map/ppermute | solution.py:54
  88.0 2.0 %collective-permute-start.5 = (bf16[384,256]{0,1:T(8,128)(2,1)}, bf16[384,256]{0,1:T(8,128)(2,1)S(1)}, u32[]{:S(2)}, u32[]{:S(2)}) collective-permute-start(bf16[384,256]{0,1:T(8,128)(2,1)} %maximum_maximum_fusion.1), channel_id=1, source_target_pairs={{0,2},{2,4},{4,6},{6,0},{1,3},{3,5},{5,7},{7,1},{8,10},{10,12},{12... | collective-permute-start | bytes 589832 | tf_op jit(solution)/shard_map/ppermute | solution.py:54
  90.0 3.2 %collective-permute-done.8 = bf16[384,128]{0,1:T(8,128)(2,1)S(1)} collective-permute-done((bf16[384,128]{0,1:T(8,128)(2,1)S(1)}, bf16[384,128]{0,1:T(8,128)(2,1)S(1)}, u32[]{:S(2)}, u32[]{:S(2)}) %collective-permute-start.8) | collective-permute-done | bytes 98336 | tf_op jit(solution)/shard_map/ppermute | solution.py:54
  93.3 0.8 fusion.82
  94.1 2.1 %collective-permute-start.11 = (bf16[4,384,128]{1,2,0:T(8,128)(2,1)}, bf16[4,384,128]{1,2,0:T(8,128)(2,1)}, u32[]{:S(2)}, u32[]{:S(2)}) collective-permute-start(bf16[4,384,128]{1,2,0:T(8,128)(2,1)} %get-tuple-element.35), channel_id=1, source_target_pairs={{0,1},{1,0},{2,3},{3,2},{4,5},{5,4},{6,7},{7,6},{8,9},{9,8},{10,11... | collective-permute-start | bytes 1179656 | tf_op jit(solution)/shard_map/ppermute | solution.py:49
  97.2 1.1 pad_maximum_fusion.1
  100.3 1.2 maximum_maximum_fusion.q_ref
  101.4 1.1 fusion.15
  102.6 1.1 fusion.16
  103.7 1.1 fusion.17
  104.8 1.2 fusion.4
  106.0 17.4 %all-to-all-done.2.keys_ref = bf16[64,128,128]{2,1,0:T(8,128)(2,1)} async-done(((bf16[64,128,128]{2,1,0:T(8,128)(2,1)}), bf16[64,128,128]{2,1,0:T(8,128)(2,1)}, u32[]{:S(2)}, u32[]{:S(2)}) %all-to-all-start.2) | async-done | bytes 2097184 | tf_op jit(solution)/shard_map/all_to_all | solution.py:40
  123.4 1.9 collective-permute-start.12
  126.6 14.2 %attend_first.1 = (f32[3,256,512]{2,1,0:T(8,128)}, f32[3,1,512]{2,1,0:T(1,128)}, f32[3,1,512]{2,1,0:T(1,128)}) custom-call(s32[2]{0:T(128)} %pad_add_fusion.1.where_ref, bf16[64,128,128]{2,1,0:T(8,128)(2,1)} %all-to-all-done.2.keys_ref, bf16[1536,384]{1,0:T(8,128)(2,1)} %maximum_maximum_fusion.q_ref), custom_call_target="tpu_custom_call" | custom-call | flops 6039797760 | bytes 6000000 | tf_op jit(solution)/shard_map/attend_first/pallas_call | solution.py:194
  140.8 15.1 %attend_last.1 = bf16[4,272,384]{2,1,0:T(8,128)(2,1)} custom-call(s32[2]{0:T(128)} %pad_add_fusion.where_ref, bf16[64,128,128]{2,1,0:T(8,128)(2,1)} %collective-permute-done.12.keys_ref, bf16[1536,384]{1,0:T(8,128)(2,1)} %maximum_maximum_fusion.q_ref, f32[3,256,512]{2,1,0:T(8,128)} %get-tuple-element.19.refs_0_, f32[3,1,512]{2,1,0:T(1,128)} %get-tuple-element.20.refs_1_, ...), custom_call_target="tpu_custom_call" | custom-call | flops 6039797760 | bytes 6000000 | tf_op jit(solution)/shard_map/attend_last/pallas_call | solution.py:194
  155.9 5.6 %all-to-all-start.3 = ((bf16[4,272,384]{2,1,0:T(8,128)(2,1)}), bf16[4,272,384]{2,1,0:T(8,128)(2,1)S(1)}, u32[]{:S(2)}, u32[]{:S(2)}) async-start(bf16[4,272,384]{2,1,0:T(8,128)(2,1)} %attend_last.1), calls=%async_computation.3 | async-start | bytes 1671168 | tf_op jit(solution)/shard_map/all_to_all | solution.py:40
  161.5 13.5 %all-to-all-done.3 = bf16[4,272,384]{2,1,0:T(8,128)(2,1)S(1)} async-done(((bf16[4,272,384]{2,1,0:T(8,128)(2,1)}), bf16[4,272,384]{2,1,0:T(8,128)(2,1)S(1)}, u32[]{:S(2)}, u32[]{:S(2)}) %all-to-all-start.3) | async-done | bytes 835616 | tf_op jit(solution)/shard_map/all_to_all | solution.py:40
  175.3 1.1 convolution_convert_fusion.8
  176.5 15.7 %all_to_all.25 = bf16[8,384,128]{2,1,0:T(8,128)(2,1)S(1)} all-to-all(bf16[8,384,128]{2,1,0:T(8,128)(2,1)S(1)} %broadcast_in_dim.21), channel_id=1, replica_groups=mesh['z'=8,'y'=8,'x'=4,'c'=2] {'x','c'}, dimensions={0} | all-to-all | bytes 1572864 | tf_op jit(solution)/shard_map/all_to_all | solution.py:40
  192.2 1.1 fusion.6
  (146 shorter events, 14.3 us)
Async XLA Ops:
  0.0 49.8 %copy-start = (bf16[2048,192]{0,1:T(8,128)(2,1)S(1)}, bf16[2048,192]{0,1:T(8,128)(2,1)}, u32[]{:S(2)}) copy-start(bf16[2048,192]{0,1:T(8,128)(2,1)} %param.19) | copy-start | bytes 2359300
  0.0 25.9 %copy-start.12 = (f32[16]{0:T(128)S(1)}, f32[16]{0:T(128)}, u32[]{:S(2)}) copy-start(f32[16]{0:T(128)} %param.25) | copy-start | bytes 196
  2.2 25.3 %collective-permute-start = (bf16[48,2048]{1,0:T(8,128)(2,1)S(1)}, bf16[48,2048]{1,0:T(8,128)(2,1)S(1)}, u32[]{:S(2)}, u32[]{:S(2)}) collective-permute-start(bf16[48,2048]{1,0:T(8,128)(2,1)S(1)} %get-tuple-element.26), channel_id=1, source_target_pairs={{0,2},{2,4},{4,6},{6,0},{1,3},{3,5},{5,7},{7,1},{8,10},{10,12},{12... | collective-permute-start | bytes 589832 | tf_op jit(solution)/shard_map/ppermute | solution.py:54
  5.7 21.9 %collective-permute-start.1 = (bf16[48,2048]{1,0:T(8,128)(2,1)S(1)}, bf16[48,2048]{1,0:T(8,128)(2,1)S(1)}, u32[]{:S(2)}, u32[]{:S(2)}) collective-permute-start(bf16[48,2048]{1,0:T(8,128)(2,1)S(1)} %get-tuple-element.26), channel_id=1, source_target_pairs={{0,4},{2,6},{4,0},{6,2},{1,5},{3,7},{5,1},{7,3},{8,12},{10,14},{12... | collective-permute-start | bytes 589832 | tf_op jit(solution)/shard_map/ppermute | solution.py:54
  10.3 17.3 %collective-permute-start.2 = (bf16[48,2048]{1,0:T(8,128)(2,1)S(1)}, bf16[48,2048]{1,0:T(8,128)(2,1)S(1)}, u32[]{:S(2)}, u32[]{:S(2)}) collective-permute-start(bf16[48,2048]{1,0:T(8,128)(2,1)S(1)} %get-tuple-element.26), channel_id=1, source_target_pairs={{0,6},{2,0},{4,2},{6,4},{1,7},{3,1},{5,3},{7,5},{8,14},{10,8},{12,... | collective-permute-start | bytes 589832 | tf_op jit(solution)/shard_map/ppermute | solution.py:54
  15.3 20.1 %all-to-all-start = ((bf16[64,16,128]{2,1,0:T(8,128)(2,1)}), bf16[64,16,128]{2,1,0:T(8,128)(2,1)S(1)}, u32[]{:S(2)}, u32[]{:S(2)}) async-start(bf16[64,16,128]{2,1,0:T(8,128)(2,1)} %broadcast_in_dim.14), calls=%async_computation | async-start | bytes 524288 | tf_op jit(solution)/shard_map/all_to_all | solution.py:40
  25.9 26.2 %copy-start.6 = (bf16[256]{0:T(256)(128)(2,1)}, bf16[256]{0:T(256)(128)(2,1)S(1)}, u32[]{:S(2)}) copy-start(bf16[256]{0:T(256)(128)(2,1)S(1)} %pad.31.clone) | copy-start | bytes 1540
  28.5 7.1 %collective-permute-start.3 = (bf16[192,2048]{1,0:T(8,128)(2,1)}, bf16[192,2048]{1,0:T(8,128)(2,1)}, u32[]{:S(2)}, u32[]{:S(2)}) collective-permute-start(bf16[192,2048]{1,0:T(8,128)(2,1)} %pad_maximum_fusion), channel_id=1, source_target_pairs={{0,1},{1,0},{2,3},{3,2},{4,5},{5,4},{6,7},{7,6},{8,9},{9,8},{10,11... | collective-permute-start | bytes 2359304 | tf_op jit(solution)/shard_map/ppermute | solution.py:49
  36.9 5.3 %copy-start.10 = (bf16[2048,64]{0,1:T(8,128)(2,1)S(1)}, bf16[2048,64]{0,1:T(8,128)(2,1)}, u32[]{:S(2)}) copy-start(bf16[2048,64]{0,1:T(8,128)(2,1)} %param.24) | copy-start | bytes 786436
  36.9 5.3 %copy-start.11 = (bf16[2048,64]{0,1:T(8,128)(2,1)S(1)}, bf16[2048,64]{0,1:T(8,128)(2,1)}, u32[]{:S(2)}) copy-start(bf16[2048,64]{0,1:T(8,128)(2,1)} %param.23) | copy-start | bytes 786436
  38.9 9.9 %all-to-all-start.1 = ((bf16[8,2,960]{2,1,0:T(2,128)(2,1)}), bf16[8,2,960]{2,1,0:T(2,128)(2,1)S(1)}, u32[]{:S(2)}, u32[]{:S(2)}) async-start(bf16[8,2,960]{2,1,0:T(2,128)(2,1)} %reshape.233), calls=%async_computation.1 | async-start | bytes 65536 | tf_op jit(solution)/shard_map/all_to_all | solution.py:40
  42.2 7.4 %copy-start.9 = (f32[256]{0:T(256)S(1)}, f32[256]{0:T(256)}, u32[]{:S(2)}) copy-start(f32[256]{0:T(256)} %param.18) | copy-start | bytes 3076
  43.3 6.4 %collective-permute-start.4 = (bf16[128,128]{0,1:T(8,128)(2,1)S(1)}, bf16[128,128]{0,1:T(8,128)(2,1)}, u32[]{:S(2)}, u32[]{:S(2)}) collective-permute-start(bf16[128,128]{0,1:T(8,128)(2,1)S(1)} %pad_maximum_fusion.4), channel_id=1, source_target_pairs={{0,8},{8,16},{16,24},{24,32},{32,40},{40,48},{48,56},{56,64},{64,7... | collective-permute-start | bytes 98312 | tf_op jit(solution)/shard_map/ppermute | solution.py:266
  52.9 44.3 %collective-permute-start.7 = (bf16[384,256]{0,1:T(8,128)(2,1)}, bf16[384,256]{0,1:T(8,128)(2,1)S(1)}, u32[]{:S(2)}, u32[]{:S(2)}) collective-permute-start(bf16[384,256]{0,1:T(8,128)(2,1)} %maximum_maximum_fusion.1), channel_id=1, source_target_pairs={{0,6},{2,0},{4,2},{6,4},{1,7},{3,1},{5,3},{7,5},{8,14},{10,8},{12,... | collective-permute-start | bytes 589832 | tf_op jit(solution)/shard_map/ppermute | solution.py:54
  58.0 39.2 %collective-permute-start.6 = (bf16[384,256]{0,1:T(8,128)(2,1)}, bf16[384,256]{0,1:T(8,128)(2,1)}, u32[]{:S(2)}, u32[]{:S(2)}) collective-permute-start(bf16[384,256]{0,1:T(8,128)(2,1)} %maximum_maximum_fusion.1), channel_id=1, source_target_pairs={{0,4},{2,6},{4,0},{6,2},{1,5},{3,7},{5,1},{7,3},{8,12},{10,14},{12... | collective-permute-start | bytes 589832 | tf_op jit(solution)/shard_map/ppermute | solution.py:54
  62.6 11.3 %copy-start.2 = (bf16[2048,128]{1,0:T(8,128)(2,1)S(1)}, bf16[2048,128]{1,0:T(8,128)(2,1)}, u32[]{:S(2)}) copy-start(bf16[2048,128]{1,0:T(8,128)(2,1)} %param.22) | copy-start | bytes 1572868
  62.6 60.9 %all-to-all-start.2 = ((bf16[64,128,128]{2,1,0:T(8,128)(2,1)}), bf16[64,128,128]{2,1,0:T(8,128)(2,1)}, u32[]{:S(2)}, u32[]{:S(2)}) async-start(bf16[64,128,128]{2,1,0:T(8,128)(2,1)} %broadcast_in_dim.15), calls=%async_computation.2 | async-start | bytes 4194304 | tf_op jit(solution)/shard_map/all_to_all | solution.py:40
  73.8 2.8 %copy-start.4 = (pred[384,512]{0,1:T(8,128)(4,1)S(1)}, pred[384,512]{0,1:T(8,128)(4,1)}, u32[]{:S(2)}) copy-start(pred[384,512]{0,1:T(8,128)(4,1)} %fusion.8) | copy-start | bytes 589828
  74.7 2.4 %copy-start.8 = (f32[2]{0:T(128)S(1)}, f32[2]{0:T(128)}, u32[]{:S(2)}) copy-start(f32[2]{0:T(128)} %dynamic_slice.217) | copy-start | bytes 28
  77.5 10.4 %copy-start.7 = (bf16[256]{0:T(256)(128)(2,1)S(1)}, bf16[256]{0:T(256)(128)(2,1)}, u32[]{:S(2)}) copy-start(bf16[256]{0:T(256)(128)(2,1)} %copy-done.6) | copy-start | bytes 1540
  77.9 18.3 %copy-start.1 = (bf16[1024,256]{1,0:T(8,128)(2,1)S(1)}, bf16[1024,256]{1,0:T(8,128)(2,1)}, u32[]{:S(2)}) copy-start(bf16[1024,256]{1,0:T(8,128)(2,1)} %param.27) | copy-start | bytes 1572868
  77.9 10.1 %collective-permute-start.10 = (bf16[384,128]{0,1:T(8,128)(2,1)S(1)}, bf16[384,128]{0,1:T(8,128)(2,1)S(1)}, u32[]{:S(2)}, u32[]{:S(2)}) collective-permute-start(bf16[384,128]{0,1:T(8,128)(2,1)S(1)} %bitcast.193), channel_id=1, source_target_pairs={{0,6},{2,0},{4,2},{6,4},{1,7},{3,1},{5,3},{7,5},{8,14},{10,8},{12,... | collective-permute-start | bytes 294920 | tf_op jit(solution)/shard_map/ppermute | solution.py:54
  80.7 9.4 %collective-permute-start.9 = (bf16[384,128]{0,1:T(8,128)(2,1)S(1)}, bf16[384,128]{0,1:T(8,128)(2,1)S(1)}, u32[]{:S(2)}, u32[]{:S(2)}) collective-permute-start(bf16[384,128]{0,1:T(8,128)(2,1)S(1)} %bitcast.194), channel_id=1, source_target_pairs={{0,4},{2,6},{4,0},{6,2},{1,5},{3,7},{5,1},{7,3},{8,12},{10,14},{12... | collective-permute-start | bytes 294920 | tf_op jit(solution)/shard_map/ppermute | solution.py:54
  84.8 8.5 %collective-permute-start.8 = (bf16[384,128]{0,1:T(8,128)(2,1)S(1)}, bf16[384,128]{0,1:T(8,128)(2,1)S(1)}, u32[]{:S(2)}, u32[]{:S(2)}) collective-permute-start(bf16[384,128]{0,1:T(8,128)(2,1)S(1)} %bitcast.195), channel_id=1, source_target_pairs={{0,2},{2,4},{4,6},{6,0},{1,3},{3,5},{5,7},{7,1},{8,10},{10,12},{12... | collective-permute-start | bytes 294920 | tf_op jit(solution)/shard_map/ppermute | solution.py:54
  88.0 9.2 %collective-permute-start.5 = (bf16[384,256]{0,1:T(8,128)(2,1)}, bf16[384,256]{0,1:T(8,128)(2,1)S(1)}, u32[]{:S(2)}, u32[]{:S(2)}) collective-permute-start(bf16[384,256]{0,1:T(8,128)(2,1)} %maximum_maximum_fusion.1), channel_id=1, source_target_pairs={{0,2},{2,4},{4,6},{6,0},{1,3},{3,5},{5,7},{7,1},{8,10},{10,12},{12... | collective-permute-start | bytes 589832 | tf_op jit(solution)/shard_map/ppermute | solution.py:54
  94.1 7.3 %collective-permute-start.11 = (bf16[4,384,128]{1,2,0:T(8,128)(2,1)}, bf16[4,384,128]{1,2,0:T(8,128)(2,1)}, u32[]{:S(2)}, u32[]{:S(2)}) collective-permute-start(bf16[4,384,128]{1,2,0:T(8,128)(2,1)} %get-tuple-element.35), channel_id=1, source_target_pairs={{0,1},{1,0},{2,3},{3,2},{4,5},{5,4},{6,7},{7,6},{8,9},{9,8},{10,11... | collective-permute-start | bytes 1179656 | tf_op jit(solution)/shard_map/ppermute | solution.py:49
  98.3 1.0 copy-start.5
  123.4 17.3 %collective-permute-start.12 = (bf16[64,128,128]{2,1,0:T(8,128)(2,1)}, bf16[64,128,128]{2,1,0:T(8,128)(2,1)}, u32[]{:S(2)}, u32[]{:S(2)}) collective-permute-start(bf16[64,128,128]{2,1,0:T(8,128)(2,1)} %all-to-all-done.2.keys_ref), channel_id=1, source_target_pairs={{0,1},{1,0},{2,3},{3,2},{4,5},{5,4},{6,7},{7,6},{8,9},{9,8},{10,11... | collective-permute-start | bytes 6291464 | tf_op jit(solution)/shard_map/ppermute | solution.py:49
  155.9 19.1 %all-to-all-start.3 = ((bf16[4,272,384]{2,1,0:T(8,128)(2,1)}), bf16[4,272,384]{2,1,0:T(8,128)(2,1)S(1)}, u32[]{:S(2)}, u32[]{:S(2)}) async-start(bf16[4,272,384]{2,1,0:T(8,128)(2,1)} %attend_last.1), calls=%async_computation.3 | async-start | bytes 1671168 | tf_op jit(solution)/shard_map/all_to_all | solution.py:40
  176.4 15.8 %copy-start.3 = (bf16[1024,256]{1,0:T(8,128)(2,1)S(1)}, bf16[1024,256]{1,0:T(8,128)(2,1)}, u32[]{:S(2)}) copy-start(bf16[1024,256]{1,0:T(8,128)(2,1)} %param.26) | copy-start | bytes 1572868

commit v3 on v2

--- a/solution.py
+++ b/solution.py
@@ -83,11 +83,20 @@
     ).astype(jnp.bfloat16)
 
 
-def attend_body(where_ref, keys_ref, q_ref, *refs, first, last):
+def attend_body(where_ref, keys_ref, *refs, first, last):
     if first:
-        (o_ref, m_ref, l_ref, kc_ref, vt_ref) = refs
+        (sent_ref, up_ref, o_ref, m_ref, l_ref, q_ref, kc_ref) = refs
+        for h in range(HEADS_CORE):
+            rows = pl.ds(h * ROWS, ROWS)
+            q_ref[rows, :KV_RANK] = lax.dot_general(
+                sent_ref[h, :, :NOPE],
+                up_ref[h],
+                (((1,), (1,)), ((), ())),
+                preferred_element_type=jnp.float32,
+            ).astype(jnp.bfloat16)
+            q_ref[rows, KV_RANK:] = sent_ref[h, :, NOPE : 2 * LANES]
     elif last:
-        (o_in, m_in, l_in, out_ref, o_ref, m_ref, l_ref, kc_ref, vt_ref) = refs
+        (q_ref, o_in, m_in, l_in, out_ref, o_ref, m_ref, l_ref, kc_ref) = refs
     block = where_ref[0]
     key_rank = where_ref[1]
     if first:
@@ -104,10 +113,9 @@
         part = keys_ref[pl.ds(index * CHUNK, CHUNK)]
         k0 = part[:, :OWN].reshape(n_keys, LANES)
         k1 = part[:, OWN : 2 * OWN].reshape(n_keys, LANES)
-        t0 = part[:, 2 * OWN : 2 * OWN + 16]
-        t1 = part[:, 2 * OWN + 16 :]
-        t0s = jnp.concatenate([t0[..., ROPE:], t0[..., :ROPE]], axis=-1)
-        kr = jnp.stack([t0, t0s, t1], axis=1).reshape(n_keys, LANES)
+        tail = part[:, 2 * OWN :]
+        turned = jnp.concatenate([tail[..., ROPE:], tail[..., :ROPE]], axis=-1)
+        kr = jnp.concatenate([tail, turned], axis=1).reshape(n_keys, LANES)
         kc_ref[:, :LANES] = k0
         kc_ref[:, LANES : 2 * LANES] = k1
         kc_ref[:, 2 * LANES :] = kr
@@ -169,7 +177,7 @@
             out_ref[h, KV_RANK:] = stats[:, h * ROWS : (h + 1) * ROWS]
 
 
-def attend(where, keys, q, state):
+def attend(where, keys, queries, state):
     state_shapes = (
         jax.ShapeDtypeStruct((TILES, KV_RANK, QTILE), jnp.float32),
         jax.ShapeDtypeStruct((TILES, 1, QTILE), jnp.float32),
@@ -178,18 +186,14 @@
     first = state is None
     smem = pl.BlockSpec(memory_space=pltpu.SMEM)
     vmem = pl.BlockSpec(memory_space=pltpu.VMEM)
-    scratch = [
-        pltpu.VMEM((CHUNK * OWN, 3 * LANES), jnp.bfloat16),
-        pltpu.VMEM((KV_RANK, CHUNK * OWN), jnp.bfloat16),
-    ]
-    if not first:
+    scratch = [pltpu.VMEM((CHUNK * OWN, 3 * LANES), jnp.bfloat16)]
+    if first:
+        out_shape = (*state_shapes, jax.ShapeDtypeStruct((QROWS, 3 * LANES), jnp.bfloat16))
+        operands = (where, keys, *queries)
+    else:
+        out_shape = jax.ShapeDtypeStruct((HEADS_CORE, KV_RANK + STAT_ROWS, ROWS), jnp.bfloat16)
+        operands = (where, keys, queries, *state)
         scratch = [pltpu.VMEM(s.shape, s.dtype) for s in state_shapes] + scratch
-    out_shape = (
-        state_shapes
-        if first
-        else jax.ShapeDtypeStruct((HEADS_CORE, KV_RANK + STAT_ROWS, ROWS), jnp.bfloat16)
-    )
-    operands = (where, keys, q) + (() if first else tuple(state))
     flops = 2 * QROWS * SOURCES * OWN * (3 * LANES + KV_RANK)
     return pl.pallas_call(
         functools.partial(attend_body, first=first, last=not first),
@@ -232,39 +236,53 @@
 
     x_count = lax.axis_size("x")
 
-    def in_place(tiles):
-        tiles = tiles.reshape(2, x_count, own_rows, -1)
-        rows = []
-        for x in range(x_count):
-            both = lax.dynamic_index_in_dim(tiles, (x_rank - x) % x_count, 1, keepdims=False)
-            rows.append(lax.dynamic_index_in_dim(both, c_rank, 0, keepdims=False))
-            rows.append(lax.dynamic_index_in_dim(both, 1 - c_rank, 0, keepdims=False))
-        return jnp.concatenate(rows, axis=0)
+    def by_x(values):
+        placed = jnp.zeros((x_count, *values.shape), values.dtype)
+        arrived = [values] + [from_x(values, k) for k in range(1, x_count)]
+        for k, value in enumerate(arrived):
+            at = (x_rank - k) % x_count
+            placed = lax.dynamic_update_index_in_dim(placed, value, at, 0)
+        return placed
+
+    def by_core(values):
+        return tuple(
+            lax.dynamic_index_in_dim(values, rank, 0, keepdims=False)
+            for rank in (c_rank, 1 - c_rank)
+        )
 
     down = jnp.concatenate([latent_down, rope_down], axis=1)
-    width = down.shape[1] // lax.axis_size(TP)
-    down = lax.dynamic_slice_in_dim(down, tp_rank * width, width, 1)
-    half = down.shape[0] // 2
-    fill = ((0, 0), (0, LANES // 2 - width))
-    down = jnp.concatenate([jnp.pad(down[:half], fill), jnp.pad(down[half:], fill)], axis=1)
+    width = down.shape[1] // x_count
+    down = lax.dynamic_slice_in_dim(down, x_rank * width, width, 1)
+    rest = LANES - width
+    low, high = (down[:16], down[16:])
+    bottom = jnp.concatenate([high[:8, rest:], high[8:, rest:]], axis=1)
+    bottom = jnp.pad(bottom, ((0, 0), (0, LANES - bottom.shape[1])))
+    down = jnp.concatenate([jnp.concatenate([low, high[:, :rest]], axis=1), bottom], axis=0)
     down = to_everyone(down, SP)
-    down = jnp.stack([down[:, :, :width], down[:, :, LANES // 2 : LANES // 2 + width]], axis=1)
-    down = down.reshape(-1, width)
+    left = width - rest
+    ends = jnp.concatenate([down[:, 16:, :left], down[:, 16:, left : 2 * left]], axis=1)
+    high = jnp.concatenate([down[:, :16, width:], ends], axis=2)
+    down = jnp.stack([down[:, :16, :width], high], axis=1).reshape(-1, width)
 
     normed = norm_rows(inputs, norm_gain)
-    mine = [normed] + [from_x(normed, k) for k in range(1, x_count)]
-    mine = jnp.concatenate(mine, axis=0)
-    other = from_core(mine)
-    pieces = jnp.concatenate([mine, other], axis=0)
-
-    latent = jnp.dot(pieces, down, preferred_element_type=jnp.float32).astype(jnp.bfloat16)
-    latent = in_place(latent)
     kv_weights = jnp.concatenate([swa_key, swa_value], axis=1)
-    swa_kv = jnp.dot(pieces, kv_weights, preferred_element_type=jnp.float32).astype(jnp.bfloat16)
-    swa_kv = in_place(swa_kv)
+    mine = by_x(normed)
+    mine = lax.optimization_barrier(mine)
+    kv_weights_other = from_core(kv_weights)
+
+    latent = jnp.dot(mine.reshape(-1, mine.shape[2]), down, preferred_element_type=jnp.float32)
+    latent = latent.astype(jnp.bfloat16).reshape(x_count, own_rows, width)
+    latent = exchange(latent, "x")
+    tail_rows = mine[x_count // 2 :].reshape(2 * own_rows, -1)
+    tail = jnp.concatenate(
+        [
+            jnp.dot(tail_rows, weights, preferred_element_type=jnp.float32)
+            for weights in (kv_weights, kv_weights_other)
+        ],
+        axis=1,
+    ).astype(jnp.bfloat16)
     count = lax.axis_size(SP)
-    before = lax.ppermute(swa_kv[ROWS - WINDOW :], SP, [(i, i + 1) for i in range(count - 1)])
-    latent = exchange(latent.reshape(-1, own_rows, width), TP)
+    before = lax.ppermute(tail, SP, [(i, i + 1) for i in range(count - 1)])
     latent = jnp.transpose(latent, (1, 0, 2)).reshape(own_rows, KV_RANK + ROPE)
     keys_latent = norm_rows(latent[:, :KV_RANK], latent_gain)
     keys_rope = rotate(latent[:, KV_RANK:], own_pos)
@@ -272,16 +290,27 @@
         [
             keys_latent[:, :LANES],
             keys_latent[:, LANES:],
-            jnp.concatenate([keys_rope[:16], keys_rope[16:32]], axis=1),
-            jnp.concatenate([keys_rope[32:], jnp.zeros((16, ROPE), jnp.bfloat16)], axis=1),
+            jnp.concatenate([keys_rope[: OWN // 2], keys_rope[OWN // 2 :]], axis=1),
         ],
         axis=0,
     )
-    packed, pieces, before = lax.optimization_barrier((packed, pieces, before))
+    packed, mine, before = lax.optimization_barrier((packed, mine, before))
     keys_own = to_everyone(packed, SP)
 
+    other = from_core(mine)
+    pieces = jnp.zeros((x_count, 2, *mine.shape[1:]), jnp.bfloat16)
+    pieces = lax.dynamic_update_index_in_dim(pieces, mine, c_rank, 1)
+    pieces = lax.dynamic_update_index_in_dim(pieces, other, 1 - c_rank, 1)
+    pieces = pieces.reshape(ROWS, -1)
+    before_other = from_core(before[:, LANES:])
+    swa_kv = jnp.dot(pieces, kv_weights, preferred_element_type=jnp.float32)
+    swa_kv = swa_kv.astype(jnp.bfloat16)
+    before_both = jnp.stack([before[:, :LANES], before_other])
+    rows_0, rows_1 = by_core(before_both)
+    before = jnp.concatenate([rows_1[3 * OWN - WINDOW : OWN], rows_0[OWN:], rows_1[OWN:]], axis=0)
+
     queries = jnp.dot(pieces, mla_query, preferred_element_type=jnp.float32)
-    queries = in_place(queries.astype(jnp.bfloat16))
+    queries = queries.astype(jnp.bfloat16)
     query = jnp.concatenate(
         [
             queries[:, :NOPE],
@@ -290,19 +319,9 @@
         ],
         axis=1,
     )
-    around = jnp.stack([query] + [from_x(query, k) for k in range(1, x_count)], axis=0)
-    q_heads = []
-    for j in range(HEADS_CORE):
-        q_j = lax.dynamic_index_in_dim(around, (x_rank - j) % x_count, 0, keepdims=False)
-        up = lax.dynamic_slice_in_dim(key_up, (2 * j + c_rank) * NOPE, NOPE, 1)
-        lat = lax.dot_general(
-            q_j[:, :NOPE], up, (((1,), (1,)), ((), ())), preferred_element_type=jnp.float32
-        ).astype(jnp.bfloat16)
-        q_heads.append(jnp.concatenate([lat, q_j[:, NOPE:]], axis=1))
-    q_all = jnp.concatenate(q_heads, axis=0)
 
     swa_q = jnp.dot(pieces, swa_query, preferred_element_type=jnp.float32)
-    swa_q = in_place(swa_q.astype(jnp.bfloat16))
+    swa_q = swa_q.astype(jnp.bfloat16)
     window = jnp.concatenate([before, swa_kv], axis=0)
     window_keys, window_values = window[:, :HEAD], window[:, HEAD:]
     scores = jnp.einsum(
@@ -324,22 +343,28 @@
     ).astype(jnp.bfloat16)
     swa_out = jnp.einsum("gts,sd->tgd", weights, window_values, preferred_element_type=jnp.float32)
     swa_out = swa_out.astype(jnp.bfloat16).reshape(ROWS, heads_swa * HEAD)
-    swa_x = jnp.stack([swa_out] + [from_x(swa_out, k) for k in range(1, x_count)], axis=0)
-    swa_both = jnp.stack([swa_x, from_core(swa_x)], axis=0)
-    from_swa = jnp.zeros((ROWS, out_swa.shape[1]), jnp.float32)
-    for o in range(2):
-        for k in range(x_count):
-            head = (2 * ((x_rank - k) % x_count)) + (c_rank + o) % 2
-            w = lax.dynamic_slice_in_dim(out_swa, head * 2 * HEAD, 2 * HEAD, 0)
-            from_swa += jnp.dot(swa_both[o, k], w, preferred_element_type=jnp.float32)
-
-    keys_own, q_all, from_swa = lax.optimization_barrier((keys_own, q_all, from_swa))
+    sent = jnp.concatenate([query, swa_out], axis=1)
+    sent = by_x(sent)
+    swa_x = sent[:, :, 2 * LANES :]
+    up_heads = lax.dynamic_index_in_dim(
+        key_up.reshape(KV_RANK, x_count, 2, NOPE), c_rank, 2, keepdims=False
+    )
+    up_heads = jnp.transpose(up_heads, (1, 0, 2))
+    keys_own, sent, up_heads, swa_x = lax.optimization_barrier((keys_own, sent, up_heads, swa_x))
     keys_other = from_core(keys_own)
+    swa_other = from_core(swa_x)
     rank_own = jnp.stack([block, tp_rank]).astype(jnp.int32)
     rank_other = jnp.stack([block, tp_rank + 1 - 2 * c_rank]).astype(jnp.int32)
-    state = attend(rank_own, keys_own, q_all, None)
+    *state, q_all = attend(rank_own, keys_own, (sent, up_heads), None)
     partial = attend(rank_other, keys_other, q_all, state)
-    parts = exchange(partial, "x").astype(jnp.float32)
+    parts = exchange(partial, "x")
+    per_head = out_swa.reshape(x_count, 2, 2 * HEAD, -1)
+    from_swa = jnp.zeros((ROWS, out_swa.shape[1]), jnp.float32)
+    for values, core in ((swa_x, c_rank), (swa_other, 1 - c_rank)):
+        weights = lax.dynamic_index_in_dim(per_head, core, 1, keepdims=False)
+        for x in range(x_count):
+            from_swa += jnp.dot(values[x], weights[x], preferred_element_type=jnp.float32)
+    parts = parts.astype(jnp.float32)
     stats = parts[:, KV_RANK:]
     m = stats[:, 0] + stats[:, 1] + stats[:, 2]
     l = stats[:, 3] + stats[:, 4]

time: 195 us -> 197 us (1.010)
  the two profiles are of different devices: /device:TPU:472 before, /device:TPU:384 now
where the time goes in v3:
time: 197 us; the launch traced here: 196 us
  starting transfers between devices  69.5 us (35%)
  waiting for transfers between devices  57.9 us (29%)
  Pallas kernels  29.6 us (15%)
  matrix products  14.9 us (8%)
  local copies, waits for them, and re-layouts  12.9 us (7%)
  other arithmetic  9.89 us (5%)
    all_to_all x5, waiting for transfers between devices, exchange(): return lax.all_to_all(array, axis, split_axis=0, concat_axis=0, tiled=True)  47.6 us
    all_to_all x5, starting transfers between devices, exchange(): return lax.all_to_all(array, axis, split_axis=0, concat_axis=0, tiled=True)  32.5 us
    pallas_call x2, Pallas kernels, attend(): pl.pallas_call(functools.partial(attend_body, first=first, last=not first...  29.6 us
    ppermute x6, starting transfers between devices, from_x(): lax.ppermute(value, 'x', [(i, (i + step) % count) for i in range(count)])  23.2 us
    ppermute x5, starting transfers between devices, from_core(): return lax.ppermute(value, 'c', [(0, 1), (1, 0)])  10.5 us
    ppermute x6, waiting for transfers between devices, from_x(): lax.ppermute(value, 'x', [(i, (i + step) % count) for i in range(count)])  8.38 us
    dot_general x8, matrix products, layer(): jnp.dot(values[x], weights[x], preferred_element_type=jnp.float32)  7.54 us
  transfers between devices with their start and end apart: 17, of which 8 were waited for; matrix products, arithmetic and copies ran while one was open for 15% of the time, Pallas kernels for 15%

profile of v3, /device:TPU:384, one launch (start us, length us, event | category | flops | bytes accessed | tf_op | source)
XLA Modules:
  0.0 195.6 jit_solution(4121679562736101124)
XLA Ops:
  0.0 1.2 fusion.9
  1.3 1.7 bitcast_dynamic-update-slice_fusion.9
  3.1 3.4 %collective-permute-start = (bf16[48,2048]{1,0:T(8,128)(2,1)}, bf16[48,2048]{1,0:T(8,128)(2,1)}, u32[]{:S(2)}, u32[]{:S(2)}) collective-permute-start(bf16[48,2048]{1,0:T(8,128)(2,1)} %get-tuple-element.30), channel_id=1, source_target_pairs={{0,2},{2,4},{4,6},{6,0},{1,3},{3,5},{5,7},{7,1},{8,10},{10,12},{12... | collective-permute-start | bytes 589832 | tf_op jit(solution)/shard_map/ppermute | solution.py:54
  6.5 4.6 %collective-permute-start.1 = (bf16[48,2048]{1,0:T(8,128)(2,1)}, bf16[48,2048]{1,0:T(8,128)(2,1)}, u32[]{:S(2)}, u32[]{:S(2)}) collective-permute-start(bf16[48,2048]{1,0:T(8,128)(2,1)} %get-tuple-element.30), channel_id=1, source_target_pairs={{0,4},{2,6},{4,0},{6,2},{1,5},{3,7},{5,1},{7,3},{8,12},{10,14},{12... | collective-permute-start | bytes 589832 | tf_op jit(solution)/shard_map/ppermute | solution.py:54
  11.1 3.3 %collective-permute-start.2 = (bf16[48,2048]{1,0:T(8,128)(2,1)}, bf16[48,2048]{1,0:T(8,128)(2,1)}, u32[]{:S(2)}, u32[]{:S(2)}) collective-permute-start(bf16[48,2048]{1,0:T(8,128)(2,1)} %get-tuple-element.30), channel_id=1, source_target_pairs={{0,6},{2,0},{4,2},{6,4},{1,7},{3,1},{5,3},{7,5},{8,14},{10,8},{12,... | collective-permute-start | bytes 589832 | tf_op jit(solution)/shard_map/ppermute | solution.py:54
  14.5 1.9 collective-permute-start.3
  16.8 0.8 broadcast_in_dim.83
  17.6 11.4 %all-to-all-start = ((bf16[64,24,128]{2,1,0:T(8,128)(2,1)}), bf16[64,24,128]{2,1,0:T(8,128)(2,1)S(1)}, u32[]{:S(2)}, u32[]{:S(2)}) async-start(bf16[64,24,128]{2,1,0:T(8,128)(2,1)} %broadcast_in_dim.83), calls=%async_computation | async-start | bytes 786432 | tf_op jit(solution)/shard_map/all_to_all | solution.py:40
  30.7 1.4 reshape.173
  32.9 1.6 fusion.8
  34.5 0.9 bitcast_dynamic-update-slice_fusion.8
  35.4 0.9 bitcast_dynamic-update-slice_fusion.7
  36.4 0.9 bitcast_dynamic-update-slice_fusion.6
  37.4 0.9 convolution_convert_fusion.7
  38.3 1.0 convolution_convert_fusion.6
  39.3 4.0 %all-to-all-done = bf16[64,24,128]{2,1,0:T(8,128)(2,1)S(1)} async-done(((bf16[64,24,128]{2,1,0:T(8,128)(2,1)}), bf16[64,24,128]{2,1,0:T(8,128)(2,1)S(1)}, u32[]{:S(2)}, u32[]{:S(2)}) %all-to-all-start) | async-done | bytes 393248 | tf_op jit(solution)/shard_map/all_to_all | solution.py:40
  45.0 3.3 %all-to-all-start.1 = ((bf16[4,48,80]{2,1,0:T(8,128)(2,1)}), bf16[4,48,80]{2,1,0:T(8,128)(2,1)S(1)}, u32[]{:S(2)}, u32[]{:S(2)}) async-start(bf16[4,48,80]{2,1,0:T(8,128)(2,1)} %bitcast.11), calls=%async_computation.1 | async-start | bytes 98304 | tf_op jit(solution)/shard_map/all_to_all | solution.py:40
  48.3 3.2 %collective-permute-start.4 = (bf16[96,256]{1,0:T(8,128)(2,1)S(1)}, bf16[96,256]{1,0:T(8,128)(2,1)S(1)}, u32[]{:S(2)}, u32[]{:S(2)}) collective-permute-start(bf16[96,256]{1,0:T(8,128)(2,1)S(1)} %pad_maximum_fusion.2), channel_id=1, source_target_pairs={{0,8},{8,16},{16,24},{24,32},{32,40},{40,48},{48,56},{56,64},{64,7... | collective-permute-start | bytes 147464 | tf_op jit(solution)/shard_map/ppermute | solution.py:285
  51.5 2.2 %all-to-all-done.1 = bf16[4,48,80]{2,1,0:T(8,128)(2,1)S(1)} async-done(((bf16[4,48,80]{2,1,0:T(8,128)(2,1)}), bf16[4,48,80]{2,1,0:T(8,128)(2,1)S(1)}, u32[]{:S(2)}, u32[]{:S(2)}) %all-to-all-start.1) | async-done | bytes 30752 | tf_op jit(solution)/shard_map/all_to_all | solution.py:40
  54.5 1.9 collective-permute-done.4
  56.4 1.9 collective-permute-start.5
  58.3 2.4 %collective-permute-start.6 = (bf16[96,128]{1,0:T(8,128)(2,1)S(1)}, bf16[96,128]{1,0:T(8,128)(2,1)S(1)}, u32[]{:S(2)}, u32[]{:S(2)}) collective-permute-start(bf16[96,128]{1,0:T(8,128)(2,1)S(1)} %get-tuple-element.38), channel_id=1, source_target_pairs={{0,1},{1,0},{2,3},{3,2},{4,5},{5,4},{6,7},{7,6},{8,9},{9,8},{10,11... | collective-permute-start | bytes 73736 | tf_op jit(solution)/shard_map/ppermute | solution.py:49
  60.7 1.5 broadcast_in_dim.84
  62.3 9.4 %all-to-all-start.2 = ((bf16[64,120,128]{2,1,0:T(8,128)(2,1)}), bf16[64,120,128]{2,1,0:T(8,128)(2,1)}, u32[]{:S(2)}, u32[]{:S(2)}) async-start(bf16[64,120,128]{2,1,0:T(8,128)(2,1)} %broadcast_in_dim.84), calls=%async_computation.2 | async-start | bytes 3932160 | tf_op jit(solution)/shard_map/all_to_all | solution.py:40
  76.2 0.8 fusion.19
  77.2 3.9 %collective-permute-start.7 = (bf16[384,384]{1,0:T(8,128)(2,1)S(1)}, bf16[384,384]{1,0:T(8,128)(2,1)S(1)}, u32[]{:S(2)}, u32[]{:S(2)}) collective-permute-start(bf16[384,384]{1,0:T(8,128)(2,1)S(1)} %concatenate.56), channel_id=1, source_target_pairs={{0,2},{2,4},{4,6},{6,0},{1,3},{3,5},{5,7},{7,1},{8,10},{10,12},{12... | collective-permute-start | bytes 884744 | tf_op jit(solution)/shard_map/ppermute | solution.py:54
  82.4 4.6 %collective-permute-start.8 = (bf16[384,384]{1,0:T(8,128)(2,1)S(1)}, bf16[384,384]{1,0:T(8,128)(2,1)S(1)}, u32[]{:S(2)}, u32[]{:S(2)}) collective-permute-start(bf16[384,384]{1,0:T(8,128)(2,1)S(1)} %concatenate.56), channel_id=1, source_target_pairs={{0,4},{2,6},{4,0},{6,2},{1,5},{3,7},{5,1},{7,3},{8,12},{10,14},{12... | collective-permute-start | bytes 884744 | tf_op jit(solution)/shard_map/ppermute | solution.py:54
  87.0 3.4 %collective-permute-start.9 = (bf16[384,384]{1,0:T(8,128)(2,1)S(1)}, bf16[384,384]{1,0:T(8,128)(2,1)S(1)}, u32[]{:S(2)}, u32[]{:S(2)}) collective-permute-start(bf16[384,384]{1,0:T(8,128)(2,1)S(1)} %concatenate.56), channel_id=1, source_target_pairs={{0,6},{2,0},{4,2},{6,4},{1,7},{3,1},{5,3},{7,5},{8,14},{10,8},{12,... | collective-permute-start | bytes 884744 | tf_op jit(solution)/shard_map/ppermute | solution.py:54
  90.6 5.8 %collective-permute-done.8 = bf16[384,384]{1,0:T(8,128)(2,1)S(1)} collective-permute-done((bf16[384,384]{1,0:T(8,128)(2,1)S(1)}, bf16[384,384]{1,0:T(8,128)(2,1)S(1)}, u32[]{:S(2)}, u32[]{:S(2)}) %collective-permute-start.8) | collective-permute-done | bytes 294944 | tf_op jit(solution)/shard_map/ppermute | solution.py:54
  96.5 2.6 %collective-permute-done.9 = bf16[384,384]{1,0:T(8,128)(2,1)S(1)} collective-permute-done((bf16[384,384]{1,0:T(8,128)(2,1)S(1)}, bf16[384,384]{1,0:T(8,128)(2,1)S(1)}, u32[]{:S(2)}, u32[]{:S(2)}) %collective-permute-start.9) | collective-permute-done | bytes 294944 | tf_op jit(solution)/shard_map/ppermute | solution.py:54
  99.2 20.0 %all-to-all-done.2.keys_ref = bf16[64,120,128]{2,1,0:T(8,128)(2,1)} async-done(((bf16[64,120,128]{2,1,0:T(8,128)(2,1)}), bf16[64,120,128]{2,1,0:T(8,128)(2,1)}, u32[]{:S(2)}, u32[]{:S(2)}) %all-to-all-start.2) | async-done | bytes 1966112 | tf_op jit(solution)/shard_map/all_to_all | solution.py:40
  119.2 1.9 collective-permute-start.10
  122.4 2.4 %collective-permute-start.11 = (bf16[4,384,128]{2,1,0:T(8,128)(2,1)S(1)}, bf16[4,384,128]{2,1,0:T(8,128)(2,1)}, u32[]{:S(2)}, u32[]{:S(2)}) collective-permute-start(bf16[4,384,128]{2,1,0:T(8,128)(2,1)S(1)} %slice.259), channel_id=1, source_target_pairs={{0,1},{1,0},{2,3},{3,2},{4,5},{5,4},{6,7},{7,6},{8,9},{9,8},{10,11... | collective-permute-start | bytes 1179656 | tf_op jit(solution)/shard_map/ppermute | solution.py:49
  124.8 1.0 fusion.26
  125.8 14.8 %attend_first.1 = (f32[3,256,512]{2,1,0:T(8,128)}, f32[3,1,512]{2,1,0:T(1,128)}, f32[3,1,512]{2,1,0:T(1,128)}, bf16[1536,384]{1,0:T(8,128)(2,1)}) custom-call(s32[2]{0:T(128)} %pad_add_fusion.1.where_ref, bf16[64,120,128]{2,1,0:T(8,128)(2,1)} %all-to-all-done.2.keys_ref, bf16[4,384,384]{2,1,0:T(8,128)(2,1)} %copy-done.1, bf16[4,256,128]{2,1,0:T(8,128)(2,1)} %bitcast.162), custom_call_target="tpu_custom_call" | custom-call | flops 6039797760 | bytes 6000000 | tf_op jit(solution)/shard_map/attend_first/pallas_call | solution.py:198
  140.6 14.8 %attend_last.1 = bf16[4,272,384]{2,1,0:T(8,128)(2,1)} custom-call(s32[2]{0:T(128)} %pad_add_fusion.where_ref, bf16[64,120,128]{2,1,0:T(8,128)(2,1)} %collective-permute-done.10.keys_ref, bf16[1536,384]{1,0:T(8,128)(2,1)} %get-tuple-element.22.refs_0_, f32[3,256,512]{2,1,0:T(8,128)} %get-tuple-element.23.refs_1_, f32[3,1,512]{2,1,0:T(1,128)} %get-tuple-element.24.refs_2_, ...), custom_call_target="tpu_custom_call" | custom-call | flops 6039797760 | bytes 6000000 | tf_op jit(solution)/shard_map/attend_last/pallas_call | solution.py:198
  155.4 4.9 %all-to-all-start.3 = ((bf16[4,272,384]{2,1,0:T(8,128)(2,1)}), bf16[4,272,384]{2,1,0:T(8,128)(2,1)S(1)}, u32[]{:S(2)}, u32[]{:S(2)}) async-start(bf16[4,272,384]{2,1,0:T(8,128)(2,1)} %attend_last.1), calls=%async_computation.3 | async-start | bytes 1671168 | tf_op jit(solution)/shard_map/all_to_all | solution.py:40
  160.3 1.0 convolution_add_fusion.3
  161.7 11.6 %all-to-all-done.3 = bf16[4,272,384]{2,1,0:T(8,128)(2,1)S(1)} async-done(((bf16[4,272,384]{2,1,0:T(8,128)(2,1)}), bf16[4,272,384]{2,1,0:T(8,128)(2,1)S(1)}, u32[]{:S(2)}, u32[]{:S(2)}) %all-to-all-start.3) | async-done | bytes 835616 | tf_op jit(solution)/shard_map/all_to_all | solution.py:40
  173.6 1.1 convolution_convert_fusion.4
  174.7 1.0 broadcast_in_dim.96
  175.7 3.5 %all-to-all-start.4 = ((bf16[8,384,128]{2,1,0:T(8,128)(2,1)}), bf16[8,384,128]{2,1,0:T(8,128)(2,1)S(1)}, u32[]{:S(2)}, u32[]{:S(2)}) async-start(bf16[8,384,128]{2,1,0:T(8,128)(2,1)} %broadcast_in_dim.96), calls=%async_computation.4 | async-start | bytes 1572864 | tf_op jit(solution)/shard_map/all_to_all | solution.py:40
  179.3 1.1 fusion.20
  180.4 1.1 fusion.21
  181.5 1.1 fusion.22
  182.6 9.8 %all-to-all-done.4 = bf16[8,384,128]{2,1,0:T(8,128)(2,1)S(1)} async-done(((bf16[8,384,128]{2,1,0:T(8,128)(2,1)}), bf16[8,384,128]{2,1,0:T(8,128)(2,1)S(1)}, u32[]{:S(2)}, u32[]{:S(2)}) %all-to-all-start.4) | async-done | bytes 786464 | tf_op jit(solution)/shard_map/all_to_all | solution.py:40
  192.3 1.4 convolution_bitcast_fusion
  193.7 1.8 fusion.6
  (120 shorter events, 13.3 us)
Async XLA Ops:
  0.0 72.1 %copy-start = (bf16[2048,192]{0,1:T(8,128)(2,1)S(1)}, bf16[2048,192]{0,1:T(8,128)(2,1)}, u32[]{:S(2)}) copy-start(bf16[2048,192]{0,1:T(8,128)(2,1)} %param.19) | copy-start | bytes 2359300
  0.0 14.5 %copy-start.5 = (bf16[2048,64]{0,1:T(8,128)(2,1)S(1)}, bf16[2048,64]{0,1:T(8,128)(2,1)}, u32[]{:S(2)}) copy-start(bf16[2048,64]{0,1:T(8,128)(2,1)} %param.23) | copy-start | bytes 786436
  0.0 14.5 %copy-start.6 = (bf16[2048,64]{0,1:T(8,128)(2,1)S(1)}, bf16[2048,64]{0,1:T(8,128)(2,1)}, u32[]{:S(2)}) copy-start(bf16[2048,64]{0,1:T(8,128)(2,1)} %param.24) | copy-start | bytes 786436
  0.0 16.5 %copy-start.10 = (bf16[32,256]{1,0:T(8,128)(2,1)S(1)}, bf16[32,256]{1,0:T(8,128)(2,1)}, u32[]{:S(2)}) copy-start(bf16[32,256]{1,0:T(8,128)(2,1)} %param.16) | copy-start | bytes 49156
  0.0 16.5 %copy-start.11 = (bf16[32,64]{1,0:T(8,128)(2,1)S(1)}, bf16[32,64]{1,0:T(8,128)(2,1)}, u32[]{:S(2)}) copy-start(bf16[32,64]{1,0:T(8,128)(2,1)} %param.17) | copy-start | bytes 12292
  3.1 31.4 %collective-permute-start = (bf16[48,2048]{1,0:T(8,128)(2,1)}, bf16[48,2048]{1,0:T(8,128)(2,1)}, u32[]{:S(2)}, u32[]{:S(2)}) collective-permute-start(bf16[48,2048]{1,0:T(8,128)(2,1)} %get-tuple-element.30), channel_id=1, source_target_pairs={{0,2},{2,4},{4,6},{6,0},{1,3},{3,5},{5,7},{7,1},{8,10},{10,12},{12... | collective-permute-start | bytes 589832 | tf_op jit(solution)/shard_map/ppermute | solution.py:54
  6.5 28.9 %collective-permute-start.1 = (bf16[48,2048]{1,0:T(8,128)(2,1)}, bf16[48,2048]{1,0:T(8,128)(2,1)}, u32[]{:S(2)}, u32[]{:S(2)}) collective-permute-start(bf16[48,2048]{1,0:T(8,128)(2,1)} %get-tuple-element.30), channel_id=1, source_target_pairs={{0,4},{2,6},{4,0},{6,2},{1,5},{3,7},{5,1},{7,3},{8,12},{10,14},{12... | collective-permute-start | bytes 589832 | tf_op jit(solution)/shard_map/ppermute | solution.py:54
  11.1 25.3 %collective-permute-start.2 = (bf16[48,2048]{1,0:T(8,128)(2,1)}, bf16[48,2048]{1,0:T(8,128)(2,1)}, u32[]{:S(2)}, u32[]{:S(2)}) collective-permute-start(bf16[48,2048]{1,0:T(8,128)(2,1)} %get-tuple-element.30), channel_id=1, source_target_pairs={{0,6},{2,0},{4,2},{6,4},{1,7},{3,1},{5,3},{7,5},{8,14},{10,8},{12,... | collective-permute-start | bytes 589832 | tf_op jit(solution)/shard_map/ppermute | solution.py:54
  14.5 23.8 %collective-permute-start.3 = (bf16[2048,128]{0,1:T(8,128)(2,1)S(1)}, bf16[2048,128]{0,1:T(8,128)(2,1)S(1)}, u32[]{:S(2)}, u32[]{:S(2)}) collective-permute-start(bf16[2048,128]{0,1:T(8,128)(2,1)S(1)} %constant_dynamic-update-slice_fusion), channel_id=1, source_target_pairs={{0,1},{1,0},{2,3},{3,2},{4,5},{5,4},{6,7},{7,6},{8,9},{9,8},{10,11... | collective-permute-start | bytes 1572872 | tf_op jit(solution)/shard_map/ppermute | solution.py:49
  17.6 25.6 %all-to-all-start = ((bf16[64,24,128]{2,1,0:T(8,128)(2,1)}), bf16[64,24,128]{2,1,0:T(8,128)(2,1)S(1)}, u32[]{:S(2)}, u32[]{:S(2)}) async-start(bf16[64,24,128]{2,1,0:T(8,128)(2,1)} %broadcast_in_dim.83), calls=%async_computation | async-start | bytes 786432 | tf_op jit(solution)/shard_map/all_to_all | solution.py:40
  43.7 4.6 %copy-start.8 = (bf16[96,128]{1,0:T(8,128)(2,1)S(1)}, bf16[96,128]{1,0:T(8,128)(2,1)}, u32[]{:S(2)}) copy-start(bf16[96,128]{1,0:T(8,128)(2,1)} %convolution_convert_fusion.7) | copy-start | bytes 73732
  43.7 4.6 %copy-start.9 = (bf16[96,128]{1,0:T(8,128)(2,1)S(1)}, bf16[96,128]{1,0:T(8,128)(2,1)}, u32[]{:S(2)}) copy-start(bf16[96,128]{1,0:T(8,128)(2,1)} %convolution_convert_fusion.6) | copy-start | bytes 73732
  43.7 10.3 %copy-start.13 = (f32[256]{0:T(256)S(1)}, f32[256]{0:T(256)}, u32[]{:S(2)}) copy-start(f32[256]{0:T(256)} %param.18) | copy-start | bytes 3076
  43.7 10.4 %copy-start.12 = (f32[32]{0:T(128)S(1)}, f32[32]{0:T(128)}, u32[]{:S(2)}) copy-start(f32[32]{0:T(128)} %multiply_power_fusion) | copy-start | bytes 388
  43.7 10.4 %copy-start.14 = (f32[48]{0:T(128)S(1)}, f32[48]{0:T(128)}, u32[]{:S(2)}) copy-start(f32[48]{0:T(128)} %add_convert_fusion) | copy-start | bytes 580
  45.0 8.8 %all-to-all-start.1 = ((bf16[4,48,80]{2,1,0:T(8,128)(2,1)}), bf16[4,48,80]{2,1,0:T(8,128)(2,1)S(1)}, u32[]{:S(2)}, u32[]{:S(2)}) async-start(bf16[4,48,80]{2,1,0:T(8,128)(2,1)} %bitcast.11), calls=%async_computation.1 | async-start | bytes 98304 | tf_op jit(solution)/shard_map/all_to_all | solution.py:40
  48.3 8.1 %collective-permute-start.4 = (bf16[96,256]{1,0:T(8,128)(2,1)S(1)}, bf16[96,256]{1,0:T(8,128)(2,1)S(1)}, u32[]{:S(2)}, u32[]{:S(2)}) collective-permute-start(bf16[96,256]{1,0:T(8,128)(2,1)S(1)} %pad_maximum_fusion.2), channel_id=1, source_target_pairs={{0,8},{8,16},{16,24},{24,32},{32,40},{40,48},{48,56},{56,64},{64,7... | collective-permute-start | bytes 147464 | tf_op jit(solution)/shard_map/ppermute | solution.py:285
  56.4 15.7 %collective-permute-start.5 = (bf16[4,48,2048]{2,1,0:T(8,128)(2,1)S(1)}, bf16[4,48,2048]{2,1,0:T(8,128)(2,1)S(1)}, u32[]{:S(2)}, u32[]{:S(2)}) collective-permute-start(bf16[4,48,2048]{2,1,0:T(8,128)(2,1)S(1)} %bitcast_dynamic-update-slice_fusion.6), channel_id=1, source_target_pairs={{0,1},{1,0},{2,3},{3,2},{4,5},{5,4},{6,7},{7,6},{8,9},{9,8},{10,11... | collective-permute-start | bytes 2359304 | tf_op jit(solution)/shard_map/ppermute | solution.py:49
  58.3 13.6 %collective-permute-start.6 = (bf16[96,128]{1,0:T(8,128)(2,1)S(1)}, bf16[96,128]{1,0:T(8,128)(2,1)S(1)}, u32[]{:S(2)}, u32[]{:S(2)}) collective-permute-start(bf16[96,128]{1,0:T(8,128)(2,1)S(1)} %get-tuple-element.38), channel_id=1, source_target_pairs={{0,1},{1,0},{2,3},{3,2},{4,5},{5,4},{6,7},{7,6},{8,9},{9,8},{10,11... | collective-permute-start | bytes 73736 | tf_op jit(solution)/shard_map/ppermute | solution.py:49
  62.3 57.0 %all-to-all-start.2 = ((bf16[64,120,128]{2,1,0:T(8,128)(2,1)}), bf16[64,120,128]{2,1,0:T(8,128)(2,1)}, u32[]{:S(2)}, u32[]{:S(2)}) async-start(bf16[64,120,128]{2,1,0:T(8,128)(2,1)} %broadcast_in_dim.84), calls=%async_computation.2 | async-start | bytes 3932160 | tf_op jit(solution)/shard_map/all_to_all | solution.py:40
  72.7 1.7 copy-start.4
  72.7 1.1 copy-start.3
  73.3 1.1 copy-start.7
  75.3 0.9 slice-start
  75.3 1.8 slice-start.1
  77.2 13.3 %collective-permute-start.7 = (bf16[384,384]{1,0:T(8,128)(2,1)S(1)}, bf16[384,384]{1,0:T(8,128)(2,1)S(1)}, u32[]{:S(2)}, u32[]{:S(2)}) collective-permute-start(bf16[384,384]{1,0:T(8,128)(2,1)S(1)} %concatenate.56), channel_id=1, source_target_pairs={{0,2},{2,4},{4,6},{6,0},{1,3},{3,5},{5,7},{7,1},{8,10},{10,12},{12... | collective-permute-start | bytes 884744 | tf_op jit(solution)/shard_map/ppermute | solution.py:54
  82.4 14.0 %collective-permute-start.8 = (bf16[384,384]{1,0:T(8,128)(2,1)S(1)}, bf16[384,384]{1,0:T(8,128)(2,1)S(1)}, u32[]{:S(2)}, u32[]{:S(2)}) collective-permute-start(bf16[384,384]{1,0:T(8,128)(2,1)S(1)} %concatenate.56), channel_id=1, source_target_pairs={{0,4},{2,6},{4,0},{6,2},{1,5},{3,7},{5,1},{7,3},{8,12},{10,14},{12... | collective-permute-start | bytes 884744 | tf_op jit(solution)/shard_map/ppermute | solution.py:54
  87.0 12.0 %collective-permute-start.9 = (bf16[384,384]{1,0:T(8,128)(2,1)S(1)}, bf16[384,384]{1,0:T(8,128)(2,1)S(1)}, u32[]{:S(2)}, u32[]{:S(2)}) collective-permute-start(bf16[384,384]{1,0:T(8,128)(2,1)S(1)} %concatenate.56), channel_id=1, source_target_pairs={{0,6},{2,0},{4,2},{6,4},{1,7},{3,1},{5,3},{7,5},{8,14},{10,8},{12,... | collective-permute-start | bytes 884744 | tf_op jit(solution)/shard_map/ppermute | solution.py:54
  99.1 26.7 %copy-start.1 = (bf16[4,384,384]{2,1,0:T(8,128)(2,1)}, bf16[4,384,384]{2,1,0:T(8,128)(2,1)S(1)}, u32[]{:S(2)}) copy-start(bf16[4,384,384]{2,1,0:T(8,128)(2,1)S(1)} %bitcast_dynamic-update-slice_fusion.2.refs_0_) | copy-start | bytes 3538948
  119.2 21.3 %collective-permute-start.10 = (bf16[64,120,128]{2,1,0:T(8,128)(2,1)}, bf16[64,120,128]{2,1,0:T(8,128)(2,1)}, u32[]{:S(2)}, u32[]{:S(2)}) collective-permute-start(bf16[64,120,128]{2,1,0:T(8,128)(2,1)} %all-to-all-done.2.keys_ref), channel_id=1, source_target_pairs={{0,1},{1,0},{2,3},{3,2},{4,5},{5,4},{6,7},{7,6},{8,9},{9,8},{10,11... | collective-permute-start | bytes 5898248 | tf_op jit(solution)/shard_map/ppermute | solution.py:49
  122.4 56.9 %collective-permute-start.11 = (bf16[4,384,128]{2,1,0:T(8,128)(2,1)S(1)}, bf16[4,384,128]{2,1,0:T(8,128)(2,1)}, u32[]{:S(2)}, u32[]{:S(2)}) collective-permute-start(bf16[4,384,128]{2,1,0:T(8,128)(2,1)S(1)} %slice.259), channel_id=1, source_target_pairs={{0,1},{1,0},{2,3},{3,2},{4,5},{5,4},{6,7},{7,6},{8,9},{9,8},{10,11... | collective-permute-start | bytes 1179656 | tf_op jit(solution)/shard_map/ppermute | solution.py:49
  155.4 5.9 %copy-start.2 = (bf16[1024,256]{1,0:T(8,128)(2,1)S(1)}, bf16[1024,256]{1,0:T(8,128)(2,1)}, u32[]{:S(2)}) copy-start(bf16[1024,256]{1,0:T(8,128)(2,1)} %param.27) | copy-start | bytes 1572868
  155.4 17.9 %all-to-all-start.3 = ((bf16[4,272,384]{2,1,0:T(8,128)(2,1)}), bf16[4,272,384]{2,1,0:T(8,128)(2,1)S(1)}, u32[]{:S(2)}, u32[]{:S(2)}) async-start(bf16[4,272,384]{2,1,0:T(8,128)(2,1)} %attend_last.1), calls=%async_computation.3 | async-start | bytes 1671168 | tf_op jit(solution)/shard_map/all_to_all | solution.py:40
  175.7 16.6 %all-to-all-start.4 = ((bf16[8,384,128]{2,1,0:T(8,128)(2,1)}), bf16[8,384,128]{2,1,0:T(8,128)(2,1)S(1)}, u32[]{:S(2)}, u32[]{:S(2)}) async-start(bf16[8,384,128]{2,1,0:T(8,128)(2,1)} %broadcast_in_dim.96), calls=%async_computation.4 | async-start | bytes 1572864 | tf_op jit(solution)/shard_map/all_to_all | solution.py:40

commit v4 on v3

--- a/solution.py
+++ b/solution.py
@@ -16,9 +16,11 @@
 KV_RANK = 256
 HEAD = 64
 WINDOW = 128
-SP = ("z", "y")
+SP = ("z", "yh", "yl")
+Y = ("yh", "yl")
+SAME_PARITY = ("z", "yh")
 TP = ("x", "c")
-SP_TP = ("z", "y", "x", "c")
+SP_TP = ("z", "yh", "yl", "x", "c")
 
 NORM_EPS = 1e-06
 ROPE_BASE = 10000.0
@@ -52,6 +54,11 @@
 def from_x(value, step):
     count = lax.axis_size("x")
     return lax.ppermute(value, "x", [(i, (i + step) % count) for i in range(count)])
+
+
+def from_y(value, step):
+    count = lax.axis_size(Y)
+    return lax.ppermute(value, Y, [(i, (i + step) % count) for i in range(count)])
 
 
 def to_float(values):
@@ -83,7 +90,8 @@
     ).astype(jnp.bfloat16)
 
 
-def attend_body(where_ref, keys_ref, *refs, first, last):
+def attend_body(where_ref, *refs, n_parts, first, last):
+    key_refs, refs = refs[:n_parts], refs[n_parts:]
     if first:
         (sent_ref, up_ref, o_ref, m_ref, l_ref, q_ref, kc_ref) = refs
         for h in range(HEADS_CORE):
@@ -95,33 +103,44 @@
                 preferred_element_type=jnp.float32,
             ).astype(jnp.bfloat16)
             q_ref[rows, KV_RANK:] = sent_ref[h, :, NOPE : 2 * LANES]
-    elif last:
-        (q_ref, o_in, m_in, l_in, out_ref, o_ref, m_ref, l_ref, kc_ref) = refs
-    block = where_ref[0]
-    key_rank = where_ref[1]
-    if first:
         o_ref[...] = jnp.zeros_like(o_ref)
         m_ref[...] = jnp.full(m_ref.shape, MASKED_VALUE, jnp.float32)
         l_ref[...] = jnp.zeros_like(l_ref)
     else:
+        if last:
+            (q_ref, o_in, m_in, l_in, out_ref, o_ref, m_ref, l_ref, kc_ref) = refs
+        else:
+            (q_ref, o_in, m_in, l_in, o_ref, m_ref, l_ref, kc_ref) = refs
         o_ref[...] = o_in[...]
         m_ref[...] = m_in[...]
         l_ref[...] = l_in[...]
+    block = where_ref[0]
+    parity = where_ref[1]
     n_keys = CHUNK * OWN
 
-    def chunk_step(index, masked):
+    def load_keys(keys_ref, index):
         part = keys_ref[pl.ds(index * CHUNK, CHUNK)]
-        k0 = part[:, :OWN].reshape(n_keys, LANES)
-        k1 = part[:, OWN : 2 * OWN].reshape(n_keys, LANES)
         tail = part[:, 2 * OWN :]
         turned = jnp.concatenate([tail[..., ROPE:], tail[..., :ROPE]], axis=-1)
-        kr = jnp.concatenate([tail, turned], axis=1).reshape(n_keys, LANES)
-        kc_ref[:, :LANES] = k0
-        kc_ref[:, LANES : 2 * LANES] = k1
-        kc_ref[:, 2 * LANES :] = kr
+        kc_ref[:, :LANES] = part[:, :OWN].reshape(n_keys, LANES)
+        kc_ref[:, LANES : 2 * LANES] = part[:, OWN : 2 * OWN].reshape(n_keys, LANES)
+        kc_ref[:, 2 * LANES :] = jnp.concatenate([tail, turned], axis=1).reshape(n_keys, LANES)
+
+    def load_part(part, index):
+        if n_parts == 1:
+            load_keys(key_refs[0], index)
+        for i in range(n_parts if n_parts > 1 else 0):
+
+            @pl.when(part == i)
+            def _(i=i):
+                load_keys(key_refs[i], index)
+
+    def chunk_step(part, index, masked):
+        load_part(part, index)
         if masked:
             row = lax.broadcasted_iota(jnp.int32, (n_keys, 1), 0)
-            key_pos = (index * CHUNK + row // OWN) * ROWS + key_rank * OWN + row % OWN
+            source = 2 * (index * CHUNK + row // OWN) + parity
+            key_pos = source * ROWS + where_ref[2 + part] * OWN + row % OWN
 
         def scores_of(tile):
             return lax.dot_general(
@@ -145,7 +164,10 @@
             m_ref[tile] = new
             l_ref[tile] = l_ref[tile] * alpha + jnp.sum(p, axis=0, keepdims=True)
             o_ref[tile] = o_ref[tile] * alpha + lax.dot_general(
-                kc_ref[:, : 2 * LANES], p.astype(jnp.bfloat16), (((0,), (0,)), ((), ())), preferred_element_type=jnp.float32
+                kc_ref[:, : 2 * LANES],
+                p.astype(jnp.bfloat16),
+                (((0,), (0,)), ((), ())),
+                preferred_element_type=jnp.float32,
             )
 
         s = scores_of(0)
@@ -154,13 +176,31 @@
             absorb(tile, s)
             s = ahead
 
-    def full_step(index, carry):
-        chunk_step(index, False)
+    n_chunks = SOURCES // 2 // CHUNK
+    n_full = (block - parity + 1) // (2 * CHUNK)
+
+    def full_step(step, carry):
+        if n_parts == 1:
+            chunk_step(0, step, False)
+        else:
+            part = (step >= n_full).astype(jnp.int32)
+            chunk_step(part, step - part * n_full, False)
         return carry
 
-    n_full = block // CHUNK
-    lax.fori_loop(0, n_full, full_step, 0)
-    chunk_step(n_full, True)
+    lax.fori_loop(0, n_full * n_parts, full_step, 0)
+
+    @pl.when(n_full < n_chunks)
+    def _():
+        if n_parts == 1:
+            chunk_step(0, n_full, True)
+        else:
+
+            def masked_step(part, carry):
+                chunk_step(part, n_full, True)
+                return carry
+
+            lax.fori_loop(0, n_parts, masked_step, 0)
+
     if last:
         whole = jnp.concatenate([o_ref[t] for t in range(TILES)], axis=1).astype(jnp.bfloat16)
         m = jnp.concatenate([m_ref[t] for t in range(TILES)], axis=1)
@@ -177,7 +217,7 @@
             out_ref[h, KV_RANK:] = stats[:, h * ROWS : (h + 1) * ROWS]
 
 
-def attend(where, keys, queries, state):
+def attend(where, parts, queries, state, last):
     state_shapes = (
         jax.ShapeDtypeStruct((TILES, KV_RANK, QTILE), jnp.float32),
         jax.ShapeDtypeStruct((TILES, 1, QTILE), jnp.float32),
@@ -187,24 +227,27 @@
     smem = pl.BlockSpec(memory_space=pltpu.SMEM)
     vmem = pl.BlockSpec(memory_space=pltpu.VMEM)
     scratch = [pltpu.VMEM((CHUNK * OWN, 3 * LANES), jnp.bfloat16)]
+    out_shape = state_shapes
     if first:
         out_shape = (*state_shapes, jax.ShapeDtypeStruct((QROWS, 3 * LANES), jnp.bfloat16))
-        operands = (where, keys, *queries)
+        operands = (where, *parts, *queries)
     else:
+        operands = (where, *parts, queries, *state)
+    if last:
         out_shape = jax.ShapeDtypeStruct((HEADS_CORE, KV_RANK + STAT_ROWS, ROWS), jnp.bfloat16)
-        operands = (where, keys, queries, *state)
         scratch = [pltpu.VMEM(s.shape, s.dtype) for s in state_shapes] + scratch
-    flops = 2 * QROWS * SOURCES * OWN * (3 * LANES + KV_RANK)
+    n_keys = SOURCES // 2 * OWN * len(parts)
     return pl.pallas_call(
-        functools.partial(attend_body, first=first, last=not first),
+        functools.partial(attend_body, n_parts=len(parts), first=first, last=last),
         out_shape=out_shape,
         in_specs=[smem] + [vmem] * (len(operands) - 1),
         out_specs=jax.tree.map(lambda _: vmem, out_shape),
         scratch_shapes=scratch,
         cost_estimate=pl.CostEstimate(
-            flops=flops, transcendentals=QROWS * SOURCES * OWN, bytes_accessed=6000000
+            flops=2 * QROWS * n_keys * (3 * LANES + KV_RANK),
+            transcendentals=QROWS * n_keys,
+            bytes_accessed=6000000,
         ),
-        name="attend_first" if first else "attend_last",
     )(*operands)
 
 
@@ -244,71 +287,36 @@
             placed = lax.dynamic_update_index_in_dim(placed, value, at, 0)
         return placed
 
-    def by_core(values):
-        return tuple(
-            lax.dynamic_index_in_dim(values, rank, 0, keepdims=False)
-            for rank in (c_rank, 1 - c_rank)
-        )
-
-    down = jnp.concatenate([latent_down, rope_down], axis=1)
-    width = down.shape[1] // x_count
-    down = lax.dynamic_slice_in_dim(down, x_rank * width, width, 1)
-    rest = LANES - width
-    low, high = (down[:16], down[16:])
-    bottom = jnp.concatenate([high[:8, rest:], high[8:, rest:]], axis=1)
-    bottom = jnp.pad(bottom, ((0, 0), (0, LANES - bottom.shape[1])))
-    down = jnp.concatenate([jnp.concatenate([low, high[:, :rest]], axis=1), bottom], axis=0)
+    half = rope_down.shape[0] // 2
+    down = jnp.concatenate(
+        [
+            latent_down[:, :LANES],
+            latent_down[:, LANES:],
+            jnp.concatenate([rope_down[:half], rope_down[half:]], axis=1),
+        ],
+        axis=0,
+    )
     down = to_everyone(down, SP)
-    left = width - rest
-    ends = jnp.concatenate([down[:, 16:, :left], down[:, 16:, left : 2 * left]], axis=1)
-    high = jnp.concatenate([down[:, :16, width:], ends], axis=2)
-    down = jnp.stack([down[:, :16, :width], high], axis=1).reshape(-1, width)
+    rope_tiles = down[:, 4 * half :]
+    down_rope = jnp.stack([rope_tiles[:, :, :ROPE], rope_tiles[:, :, ROPE:]], axis=1)
+    down_rope = down_rope.reshape(-1, ROPE)
+    down_latent = jnp.concatenate([down[:, : 2 * half], down[:, 2 * half : 4 * half]], axis=2)
+    down_latent = down_latent.reshape(-1, KV_RANK)
 
     normed = norm_rows(inputs, norm_gain)
     kv_weights = jnp.concatenate([swa_key, swa_value], axis=1)
     mine = by_x(normed)
-    mine = lax.optimization_barrier(mine)
-    kv_weights_other = from_core(kv_weights)
-
-    latent = jnp.dot(mine.reshape(-1, mine.shape[2]), down, preferred_element_type=jnp.float32)
-    latent = latent.astype(jnp.bfloat16).reshape(x_count, own_rows, width)
-    latent = exchange(latent, "x")
-    tail_rows = mine[x_count // 2 :].reshape(2 * own_rows, -1)
-    tail = jnp.concatenate(
-        [
-            jnp.dot(tail_rows, weights, preferred_element_type=jnp.float32)
-            for weights in (kv_weights, kv_weights_other)
-        ],
-        axis=1,
-    ).astype(jnp.bfloat16)
-    count = lax.axis_size(SP)
-    before = lax.ppermute(tail, SP, [(i, i + 1) for i in range(count - 1)])
-    latent = jnp.transpose(latent, (1, 0, 2)).reshape(own_rows, KV_RANK + ROPE)
-    keys_latent = norm_rows(latent[:, :KV_RANK], latent_gain)
-    keys_rope = rotate(latent[:, KV_RANK:], own_pos)
-    packed = jnp.concatenate(
-        [
-            keys_latent[:, :LANES],
-            keys_latent[:, LANES:],
-            jnp.concatenate([keys_rope[: OWN // 2], keys_rope[OWN // 2 :]], axis=1),
-        ],
-        axis=0,
-    )
-    packed, mine, before = lax.optimization_barrier((packed, mine, before))
-    keys_own = to_everyone(packed, SP)
-
     other = from_core(mine)
     pieces = jnp.zeros((x_count, 2, *mine.shape[1:]), jnp.bfloat16)
     pieces = lax.dynamic_update_index_in_dim(pieces, mine, c_rank, 1)
     pieces = lax.dynamic_update_index_in_dim(pieces, other, 1 - c_rank, 1)
     pieces = pieces.reshape(ROWS, -1)
-    before_other = from_core(before[:, LANES:])
     swa_kv = jnp.dot(pieces, kv_weights, preferred_element_type=jnp.float32)
     swa_kv = swa_kv.astype(jnp.bfloat16)
-    before_both = jnp.stack([before[:, :LANES], before_other])
-    rows_0, rows_1 = by_core(before_both)
-    before = jnp.concatenate([rows_1[3 * OWN - WINDOW : OWN], rows_0[OWN:], rows_1[OWN:]], axis=0)
-
+    count = lax.axis_size(SP)
+    before = lax.ppermute(
+        swa_kv[ROWS - WINDOW :], SP, [(i, i + 1) for i in range(count - 1)]
+    )
     queries = jnp.dot(pieces, mla_query, preferred_element_type=jnp.float32)
     queries = queries.astype(jnp.bfloat16)
     query = jnp.concatenate(
@@ -319,6 +327,21 @@
         ],
         axis=1,
     )
+
+    latent = jnp.dot(normed, down_latent, preferred_element_type=jnp.float32)
+    rope_raw = jnp.dot(normed, down_rope, preferred_element_type=jnp.float32)
+    keys_latent = norm_rows(latent.astype(jnp.bfloat16), latent_gain)
+    keys_rope = rotate(rope_raw.astype(jnp.bfloat16), own_pos)
+    packed = jnp.concatenate(
+        [
+            keys_latent[:, :LANES],
+            keys_latent[:, LANES:],
+            jnp.concatenate([keys_rope[: OWN // 2], keys_rope[OWN // 2 :]], axis=1),
+        ],
+        axis=0,
+    )
+    packed, pieces, swa_kv, before = lax.optimization_barrier((packed, pieces, swa_kv, before))
+    keys_own = to_everyone(packed, SAME_PARITY)
 
     swa_q = jnp.dot(pieces, swa_query, preferred_element_type=jnp.float32)
     swa_q = swa_q.astype(jnp.bfloat16)
@@ -346,17 +369,33 @@
     sent = jnp.concatenate([query, swa_out], axis=1)
     sent = by_x(sent)
     swa_x = sent[:, :, 2 * LANES :]
-    up_heads = lax.dynamic_index_in_dim(
-        key_up.reshape(KV_RANK, x_count, 2, NOPE), c_rank, 2, keepdims=False
-    )
-    up_heads = jnp.transpose(up_heads, (1, 0, 2))
-    keys_own, sent, up_heads, swa_x = lax.optimization_barrier((keys_own, sent, up_heads, swa_x))
+    swa_other = from_core(swa_x)
+    up_heads = jnp.stack(
+        [lax.dynamic_slice_in_dim(key_up, (2 * x + c_rank) * NOPE, NOPE, 1) for x in range(x_count)]
+    )
+    parity = lax.axis_index("yl")
+    rank_other = tp_rank + 1 - 2 * c_rank
+    where = [
+        jnp.stack(entries).astype(jnp.int32)
+        for entries in (
+            (block, parity, tp_rank),
+            (block, parity, rank_other),
+            (block, 1 - parity, tp_rank, rank_other),
+        )
+    ]
+    keys_own, sent, up_heads, swa_x, where = lax.optimization_barrier(
+        (keys_own, sent, up_heads, swa_x, where)
+    )
+    half = keys_own.shape[0] // 2
+    low = from_y(keys_own[:half], 1)
+    high = from_y(keys_own[half:], -1)
     keys_other = from_core(keys_own)
-    swa_other = from_core(swa_x)
-    rank_own = jnp.stack([block, tp_rank]).astype(jnp.int32)
-    rank_other = jnp.stack([block, tp_rank + 1 - 2 * c_rank]).astype(jnp.int32)
-    *state, q_all = attend(rank_own, keys_own, (sent, up_heads), None)
-    partial = attend(rank_other, keys_other, q_all, state)
+    *state, q_all = attend(where[0], (keys_own,), (sent, up_heads), None, False)
+    far_own = jnp.concatenate([low, high], axis=0)
+    far_own, state = lax.optimization_barrier((far_own, state))
+    far_other = from_core(far_own)
+    state = attend(where[1], (keys_other,), q_all, state, False)
+    partial = attend(where[2], (far_own, far_other), q_all, state, True)
     parts = exchange(partial, "x")
     per_head = out_swa.reshape(x_count, 2, 2 * HEAD, -1)
     from_swa = jnp.zeros((ROWS, out_swa.shape[1]), jnp.float32)
@@ -384,7 +423,7 @@
 
 
 def solution(mesh):
-    split = Mesh(mesh.devices.reshape(8, 8, 4, 2), SP_TP)
+    split = Mesh(mesh.devices.reshape(8, 4, 2, 4, 2), SP_TP)
     placed = (
         P(SP_TP, None),
         P(),

time: 197 us -> 193 us (0.980)
  the two profiles are of different devices: /device:TPU:384 before, /device:TPU:1 now
where the time goes in v4:
time: 193 us; the launch traced here: 190 us
  starting transfers between devices  78.8 us (41%)
  waiting for transfers between devices  47.4 us (25%)
  Pallas kernels  24.1 us (12%)
  matrix products  17.5 us (9%)
  local copies, waits for them, and re-layouts  11.5 us (6%)
  other arithmetic  9.81 us (5%)
    all_to_all x4, waiting for transfers between devices, exchange(): return lax.all_to_all(array, axis, split_axis=0, concat_axis=0, tiled=True)  33.5 us
    all_to_all x4, starting transfers between devices, exchange(): return lax.all_to_all(array, axis, split_axis=0, concat_axis=0, tiled=True)  31.8 us
    pallas_call x3, Pallas kernels, attend(): pl.pallas_call(functools.partial(attend_body, n_parts=len(parts), first=f...  24.1 us
    ppermute x6, starting transfers between devices, from_x(): lax.ppermute(value, 'x', [(i, (i + step) % count) for i in range(count)])  19.8 us
    ppermute x4, starting transfers between devices, from_core(): return lax.ppermute(value, 'c', [(0, 1), (1, 0)])  12.8 us
    ppermute x2, starting transfers between devices, from_y(): lax.ppermute(value, Y, [(i, (i + step) % count) for i in range(count)])  11.2 us
    dot_general x8, matrix products, layer(): jnp.dot(values[x], weights[x], preferred_element_type=jnp.float32)  10.8 us
    ppermute x6, waiting for transfers between devices, from_x(): lax.ppermute(value, 'x', [(i, (i + step) % count) for i in range(count)])  10.1 us
  transfers between devices with their start and end apart: 17, of which 8 were waited for; matrix products, arithmetic and copies ran while one was open for 14% of the time, Pallas kernels for 7%

profile of v4, /device:TPU:1, one launch (start us, length us, event | category | flops | bytes accessed | tf_op | source)
XLA Modules:
  0.0 189.9 jit_solution(3389441240365760692)
XLA Ops:
  0.0 1.1 fusion.12
  1.3 1.1 bitcast_dynamic-update-slice_fusion.9
  2.3 3.9 %collective-permute-start = (bf16[48,2048]{1,0:T(8,128)(2,1)S(1)}, bf16[48,2048]{1,0:T(8,128)(2,1)}, u32[]{:S(2)}, u32[]{:S(2)}) collective-permute-start(bf16[48,2048]{1,0:T(8,128)(2,1)S(1)} %get-tuple-element.52), channel_id=1, source_target_pairs={{0,2},{2,4},{4,6},{6,0},{1,3},{3,5},{5,7},{7,1},{8,10},{10,12},{12... | collective-permute-start | bytes 589832 | tf_op jit(solution)/shard_map/ppermute | solution.py:56
  6.3 4.4 %collective-permute-start.1 = (bf16[48,2048]{1,0:T(8,128)(2,1)S(1)}, bf16[48,2048]{1,0:T(8,128)(2,1)S(1)}, u32[]{:S(2)}, u32[]{:S(2)}) collective-permute-start(bf16[48,2048]{1,0:T(8,128)(2,1)S(1)} %get-tuple-element.52), channel_id=1, source_target_pairs={{0,4},{2,6},{4,0},{6,2},{1,5},{3,7},{5,1},{7,3},{8,12},{10,14},{12... | collective-permute-start | bytes 589832 | tf_op jit(solution)/shard_map/ppermute | solution.py:56
  10.7 3.1 %collective-permute-start.2 = (bf16[48,2048]{1,0:T(8,128)(2,1)S(1)}, bf16[48,2048]{1,0:T(8,128)(2,1)S(1)}, u32[]{:S(2)}, u32[]{:S(2)}) collective-permute-start(bf16[48,2048]{1,0:T(8,128)(2,1)S(1)} %get-tuple-element.52), channel_id=1, source_target_pairs={{0,6},{2,0},{4,2},{6,4},{1,7},{3,1},{5,3},{7,5},{8,14},{10,8},{12,... | collective-permute-start | bytes 589832 | tf_op jit(solution)/shard_map/ppermute | solution.py:56
  13.9 1.3 broadcast_in_dim.78
  15.1 16.4 %all-to-all-start = ((bf16[64,80,128]{2,1,0:T(8,128)(2,1)}), bf16[64,80,128]{2,1,0:T(8,128)(2,1)S(1)}, u32[]{:S(2)}, u32[]{:S(2)}) async-start(bf16[64,80,128]{2,1,0:T(8,128)(2,1)} %broadcast_in_dim.78), calls=%async_computation | async-start | bytes 2621440 | tf_op jit(solution)/shard_map/all_to_all | solution.py:42
  32.5 1.0 dynamic-slice_bitcast_fusion.19
  35.2 3.7 %collective-permute-start.3 = (bf16[4,48,2048]{2,1,0:T(8,128)(2,1)S(1)}, bf16[4,48,2048]{2,1,0:T(8,128)(2,1)S(1)}, u32[]{:S(2)}, u32[]{:S(2)}) collective-permute-start(bf16[4,48,2048]{2,1,0:T(8,128)(2,1)S(1)} %bitcast_dynamic-update-slice_fusion.6), channel_id=1, source_target_pairs={{0,1},{1,0},{2,3},{3,2},{4,5},{5,4},{6,7},{7,6},{8,9},{9,8},{10,11... | collective-permute-start | bytes 2359304 | tf_op jit(solution)/shard_map/ppermute | solution.py:51
  38.9 1.0 fusion.8
  42.9 3.2 %collective-permute-start.4 = (bf16[128,128]{1,0:T(8,128)(2,1)S(1)}, bf16[128,128]{1,0:T(8,128)(2,1)S(1)}, u32[]{:S(2)}, u32[]{:S(2)}) collective-permute-start(bf16[128,128]{1,0:T(8,128)(2,1)S(1)} %slice.211), channel_id=1, source_target_pairs={{0,8},{8,16},{16,24},{24,32},{32,40},{40,48},{48,56},{56,64},{64,7... | collective-permute-start | bytes 98312 | tf_op jit(solution)/shard_map/ppermute | solution.py:317
  47.0 16.5 %all-to-all-done = bf16[64,80,128]{2,1,0:T(8,128)(2,1)S(1)} async-done(((bf16[64,80,128]{2,1,0:T(8,128)(2,1)}), bf16[64,80,128]{2,1,0:T(8,128)(2,1)S(1)}, u32[]{:S(2)}, u32[]{:S(2)}) %all-to-all-start) | async-done | bytes 1310752 | tf_op jit(solution)/shard_map/all_to_all | solution.py:42
  65.8 1.1 broadcast_in_dim.87
  66.9 7.4 %all-to-all-start.1 = ((bf16[32,120,128]{2,1,0:T(8,128)(2,1)}), bf16[32,120,128]{2,1,0:T(8,128)(2,1)S(1)}, u32[]{:S(2)}, u32[]{:S(2)}) async-start(bf16[32,120,128]{2,1,0:T(8,128)(2,1)} %broadcast_in_dim.87), calls=%async_computation.1 | async-start | bytes 1966080 | tf_op jit(solution)/shard_map/all_to_all | solution.py:42
  74.3 1.6 constant_dynamic-update-slice_fusion
  75.9 1.7 convolution_convert_fusion.2
  79.5 2.2 %collective-permute-start.5 = (bf16[384,384]{1,0:T(8,128)(2,1)S(1)}, bf16[384,384]{1,0:T(8,128)(2,1)S(1)}, u32[]{:S(2)}, u32[]{:S(2)}) collective-permute-start(bf16[384,384]{1,0:T(8,128)(2,1)S(1)} %concatenate.42), channel_id=1, source_target_pairs={{0,2},{2,4},{4,6},{6,0},{1,3},{3,5},{5,7},{7,1},{8,10},{10,12},{12... | collective-permute-start | bytes 884744 | tf_op jit(solution)/shard_map/ppermute | solution.py:56
  82.3 3.1 %collective-permute-start.6 = (bf16[384,384]{1,0:T(8,128)(2,1)S(1)}, bf16[384,384]{1,0:T(8,128)(2,1)S(1)}, u32[]{:S(2)}, u32[]{:S(2)}) collective-permute-start(bf16[384,384]{1,0:T(8,128)(2,1)S(1)} %concatenate.42), channel_id=1, source_target_pairs={{0,4},{2,6},{4,0},{6,2},{1,5},{3,7},{5,1},{7,3},{8,12},{10,14},{12... | collective-permute-start | bytes 884744 | tf_op jit(solution)/shard_map/ppermute | solution.py:56
  85.3 3.1 %collective-permute-start.7 = (bf16[384,384]{1,0:T(8,128)(2,1)S(1)}, bf16[384,384]{1,0:T(8,128)(2,1)S(1)}, u32[]{:S(2)}, u32[]{:S(2)}) collective-permute-start(bf16[384,384]{1,0:T(8,128)(2,1)S(1)} %concatenate.42), channel_id=1, source_target_pairs={{0,6},{2,0},{4,2},{6,4},{1,7},{3,1},{5,3},{7,5},{8,14},{10,8},{12,... | collective-permute-start | bytes 884744 | tf_op jit(solution)/shard_map/ppermute | solution.py:56
  88.7 6.0 %collective-permute-done.6 = bf16[384,384]{1,0:T(8,128)(2,1)S(1)} collective-permute-done((bf16[384,384]{1,0:T(8,128)(2,1)S(1)}, bf16[384,384]{1,0:T(8,128)(2,1)S(1)}, u32[]{:S(2)}, u32[]{:S(2)}) %collective-permute-start.6) | collective-permute-done | bytes 294944 | tf_op jit(solution)/shard_map/ppermute | solution.py:56
  94.8 4.1 %collective-permute-done.7 = bf16[384,384]{1,0:T(8,128)(2,1)S(1)} collective-permute-done((bf16[384,384]{1,0:T(8,128)(2,1)S(1)}, bf16[384,384]{1,0:T(8,128)(2,1)S(1)}, u32[]{:S(2)}, u32[]{:S(2)}) %collective-permute-start.7) | collective-permute-done | bytes 294944 | tf_op jit(solution)/shard_map/ppermute | solution.py:56
  99.0 1.3 fusion.73
  100.3 9.3 %collective-permute-start.8 = (bf16[16,120,128]{2,1,0:T(8,128)(2,1)}, bf16[16,120,128]{2,1,0:T(8,128)(2,1)}, u32[]{:S(2)}, u32[]{:S(2)}) collective-permute-start(bf16[16,120,128]{2,1,0:T(8,128)(2,1)} %get-tuple-element.57), channel_id=1, source_target_pairs={{0,8},{8,16},{16,24},{24,32},{32,40},{40,48},{48,56},{56,0},{1,9},... | collective-permute-start | bytes 1474568 | tf_op jit(solution)/shard_map/ppermute | solution.py:61
  109.6 1.9 %collective-permute-start.9 = (bf16[16,120,128]{2,1,0:T(8,128)(2,1)}, bf16[16,120,128]{2,1,0:T(8,128)(2,1)}, u32[]{:S(2)}, u32[]{:S(2)}) collective-permute-start(bf16[16,120,128]{2,1,0:T(8,128)(2,1)} %get-tuple-element.58), channel_id=1, source_target_pairs={{0,56},{8,0},{16,8},{24,16},{32,24},{40,32},{48,40},{56,48},{1,57}... | collective-permute-start | bytes 1474568 | tf_op jit(solution)/shard_map/ppermute | solution.py:61
  111.5 3.2 %collective-permute-start.11 = (bf16[32,120,128]{2,1,0:T(8,128)(2,1)S(1)}, bf16[32,120,128]{2,1,0:T(8,128)(2,1)}, u32[]{:S(2)}, u32[]{:S(2)}) collective-permute-start(bf16[32,120,128]{2,1,0:T(8,128)(2,1)S(1)} %all-to-all-done.1.refs_0_), channel_id=1, source_target_pairs={{0,1},{1,0},{2,3},{3,2},{4,5},{5,4},{6,7},{7,6},{8,9},{9,8},{10,11... | collective-permute-start | bytes 2949128 | tf_op jit(solution)/shard_map/ppermute | solution.py:51
  114.7 7.1 %shard_map.136 = (f32[3,256,512]{2,1,0:T(8,128)}, f32[3,1,512]{2,1,0:T(1,128)}, f32[3,1,512]{2,1,0:T(1,128)}, bf16[1536,384]{1,0:T(8,128)(2,1)}) custom-call(s32[3]{0:T(128)} %get-tuple-element.33.where_ref, bf16[32,120,128]{2,1,0:T(8,128)(2,1)} %copy-done.3, bf16[4,384,384]{2,1,0:T(8,128)(2,1)} %copy-done.4, bf16[4,256,128]{2,1,0:T(8,128)(2,1)} %pad_maximum_fusion.3.refs_2_), custom_call_target="tpu_custom_call" | custom-call | flops 3019898880 | bytes 6000000 | tf_op jit(solution)/shard_map/pallas_call | solution.py:240
  121.8 1.5 collective-permute-done.9
  123.3 2.3 %pad_maximum_fusion.1.refs_0_ = bf16[32,120,128]{2,1,0:T(8,128)(2,1)} fusion(bf16[16,120,128]{2,1,0:T(8,128)(2,1)} %collective-permute-done.9, bf16[16,120,128]{2,1,0:T(8,128)(2,1)} %collective-permute-done.8), kind=kLoop, calls=%fused_computation.26 | loop fusion | flops 491520 | bytes 1966080 | tf_op jit(solution)/shard_map/concatenate | solution.py:394
  125.6 4.0 %collective-permute-start.10 = (bf16[32,120,128]{2,1,0:T(8,128)(2,1)}, bf16[32,120,128]{2,1,0:T(8,128)(2,1)}, u32[]{:S(2)}, u32[]{:S(2)}) collective-permute-start(bf16[32,120,128]{2,1,0:T(8,128)(2,1)} %pad_maximum_fusion.1.refs_0_), channel_id=1, source_target_pairs={{0,1},{1,0},{2,3},{3,2},{4,5},{5,4},{6,7},{7,6},{8,9},{9,8},{10,11... | collective-permute-start | bytes 2949128 | tf_op jit(solution)/shard_map/ppermute | solution.py:51
  129.6 1.9 %collective-permute-start.12 = (bf16[4,384,128]{2,1,0:T(8,128)(2,1)S(1)}, bf16[4,384,128]{2,1,0:T(8,128)(2,1)S(1)}, u32[]{:S(2)}, u32[]{:S(2)}) collective-permute-start(bf16[4,384,128]{2,1,0:T(8,128)(2,1)S(1)} %slice.218), channel_id=1, source_target_pairs={{0,1},{1,0},{2,3},{3,2},{4,5},{5,4},{6,7},{7,6},{8,9},{9,8},{10,11... | collective-permute-start | bytes 1179656 | tf_op jit(solution)/shard_map/ppermute | solution.py:51
  131.6 1.7 collective-permute-done.12
  133.2 1.1 fusion.23
  134.3 6.6 %shard_map.137 = (f32[3,256,512]{2,1,0:T(8,128)}, f32[3,1,512]{2,1,0:T(1,128)}, f32[3,1,512]{2,1,0:T(1,128)}) custom-call(s32[3]{0:T(128)} %get-tuple-element.41.where_ref, bf16[32,120,128]{2,1,0:T(8,128)(2,1)} %collective-permute-done.11.refs_0_, bf16[1536,384]{1,0:T(8,128)(2,1)} %get-tuple-element.40.refs_1_.refs_2_, ...), custom_call_target="tpu_custom_call" | custom-call | flops 3019898880 | bytes 6000000 | tf_op jit(solution)/shard_map/pallas_call | solution.py:240
  140.9 10.4 %shard_map.138 = bf16[4,272,384]{2,1,0:T(8,128)(2,1)} custom-call(s32[4]{0:T(128)} %pad_add_fusion.3.where_ref, bf16[32,120,128]{2,1,0:T(8,128)(2,1)} %pad_maximum_fusion.1.refs_0_, bf16[32,120,128]{2,1,0:T(8,128)(2,1)} %collective-permute-done.10.refs_1_, bf16[1536,384]{1,0:T(8,128)(2,1)} %get-tuple-element.40.refs_1_.refs_2_, ...), custom_call_target="tpu_custom_call" | custom-call | flops 6039797760 | bytes 6000000 | tf_op jit(solution)/shard_map/pallas_call | solution.py:240
  151.3 3.5 %all-to-all-start.2 = ((bf16[4,272,384]{2,1,0:T(8,128)(2,1)}), bf16[4,272,384]{2,1,0:T(8,128)(2,1)S(1)}, u32[]{:S(2)}, u32[]{:S(2)}) async-start(bf16[4,272,384]{2,1,0:T(8,128)(2,1)} %shard_map.138), calls=%async_computation.2 | async-start | bytes 1671168 | tf_op jit(solution)/shard_map/all_to_all | solution.py:42
  154.8 1.0 fusion.24
  155.9 1.1 fusion.25
  157.0 1.8 fusion.29
  158.8 8.8 %all-to-all-done.2 = bf16[4,272,384]{2,1,0:T(8,128)(2,1)S(1)} async-done(((bf16[4,272,384]{2,1,0:T(8,128)(2,1)}), bf16[4,272,384]{2,1,0:T(8,128)(2,1)S(1)}, u32[]{:S(2)}, u32[]{:S(2)}) %all-to-all-start.2) | async-done | bytes 835616 | tf_op jit(solution)/shard_map/all_to_all | solution.py:42
  167.9 1.1 convolution_convert_fusion.4
  169.0 1.0 broadcast_in_dim.96
  170.0 4.4 %all-to-all-start.3 = ((bf16[8,384,128]{2,1,0:T(8,128)(2,1)}), bf16[8,384,128]{2,1,0:T(8,128)(2,1)S(1)}, u32[]{:S(2)}, u32[]{:S(2)}) async-start(bf16[8,384,128]{2,1,0:T(8,128)(2,1)} %broadcast_in_dim.96), calls=%async_computation.3 | async-start | bytes 1572864 | tf_op jit(solution)/shard_map/all_to_all | solution.py:42
  174.5 1.2 convolution_add_fusion.3
  175.7 1.0 convolution_add_fusion.2
  176.8 1.8 convolution_add_fusion.1
  178.5 8.1 %all-to-all-done.3 = bf16[8,384,128]{2,1,0:T(8,128)(2,1)S(1)} async-done(((bf16[8,384,128]{2,1,0:T(8,128)(2,1)}), bf16[8,384,128]{2,1,0:T(8,128)(2,1)S(1)}, u32[]{:S(2)}, u32[]{:S(2)}) %all-to-all-start.3) | async-done | bytes 786464 | tf_op jit(solution)/shard_map/all_to_all | solution.py:42
  186.7 1.4 convolution_bitcast_fusion
  188.1 1.8 fusion.6
  (108 shorter events, 11.8 us)
Async XLA Ops:
  0.0 40.9 %copy-start = (bf16[2048,192]{0,1:T(8,128)(2,1)S(1)}, bf16[2048,192]{0,1:T(8,128)(2,1)}, u32[]{:S(2)}) copy-start(bf16[2048,192]{0,1:T(8,128)(2,1)} %param.19) | copy-start | bytes 2359300
  0.0 13.7 %copy-start.10 = (bf16[32,256]{1,0:T(8,128)(2,1)S(1)}, bf16[32,256]{1,0:T(8,128)(2,1)}, u32[]{:S(2)}) copy-start(bf16[32,256]{1,0:T(8,128)(2,1)} %param.16) | copy-start | bytes 49156
  0.0 13.7 %copy-start.12 = (bf16[32,64]{1,0:T(8,128)(2,1)S(1)}, bf16[32,64]{1,0:T(8,128)(2,1)}, u32[]{:S(2)}) copy-start(bf16[32,64]{1,0:T(8,128)(2,1)} %param.17) | copy-start | bytes 12292
  2.3 31.8 %collective-permute-start = (bf16[48,2048]{1,0:T(8,128)(2,1)S(1)}, bf16[48,2048]{1,0:T(8,128)(2,1)}, u32[]{:S(2)}, u32[]{:S(2)}) collective-permute-start(bf16[48,2048]{1,0:T(8,128)(2,1)S(1)} %get-tuple-element.52), channel_id=1, source_target_pairs={{0,2},{2,4},{4,6},{6,0},{1,3},{3,5},{5,7},{7,1},{8,10},{10,12},{12... | collective-permute-start | bytes 589832 | tf_op jit(solution)/shard_map/ppermute | solution.py:56
  6.3 28.8 %collective-permute-start.1 = (bf16[48,2048]{1,0:T(8,128)(2,1)S(1)}, bf16[48,2048]{1,0:T(8,128)(2,1)S(1)}, u32[]{:S(2)}, u32[]{:S(2)}) collective-permute-start(bf16[48,2048]{1,0:T(8,128)(2,1)S(1)} %get-tuple-element.52), channel_id=1, source_target_pairs={{0,4},{2,6},{4,0},{6,2},{1,5},{3,7},{5,1},{7,3},{8,12},{10,14},{12... | collective-permute-start | bytes 589832 | tf_op jit(solution)/shard_map/ppermute | solution.py:56
  10.7 24.5 %collective-permute-start.2 = (bf16[48,2048]{1,0:T(8,128)(2,1)S(1)}, bf16[48,2048]{1,0:T(8,128)(2,1)S(1)}, u32[]{:S(2)}, u32[]{:S(2)}) collective-permute-start(bf16[48,2048]{1,0:T(8,128)(2,1)S(1)} %get-tuple-element.52), channel_id=1, source_target_pairs={{0,6},{2,0},{4,2},{6,4},{1,7},{3,1},{5,3},{7,5},{8,14},{10,8},{12,... | collective-permute-start | bytes 589832 | tf_op jit(solution)/shard_map/ppermute | solution.py:56
  15.1 16.6 %copy-start.16 = (f32[16]{0:T(128)S(1)}, f32[16]{0:T(128)}, u32[]{:S(2)}) copy-start(f32[16]{0:T(128)} %param.25) | copy-start | bytes 196
  15.1 48.4 %all-to-all-start = ((bf16[64,80,128]{2,1,0:T(8,128)(2,1)}), bf16[64,80,128]{2,1,0:T(8,128)(2,1)S(1)}, u32[]{:S(2)}, u32[]{:S(2)}) async-start(bf16[64,80,128]{2,1,0:T(8,128)(2,1)} %broadcast_in_dim.78), calls=%async_computation | async-start | bytes 2621440 | tf_op jit(solution)/shard_map/all_to_all | solution.py:42
  35.2 5.6 %collective-permute-start.3 = (bf16[4,48,2048]{2,1,0:T(8,128)(2,1)S(1)}, bf16[4,48,2048]{2,1,0:T(8,128)(2,1)S(1)}, u32[]{:S(2)}, u32[]{:S(2)}) collective-permute-start(bf16[4,48,2048]{2,1,0:T(8,128)(2,1)S(1)} %bitcast_dynamic-update-slice_fusion.6), channel_id=1, source_target_pairs={{0,1},{1,0},{2,3},{3,2},{4,5},{5,4},{6,7},{7,6},{8,9},{9,8},{10,11... | collective-permute-start | bytes 2359304 | tf_op jit(solution)/shard_map/ppermute | solution.py:51
  40.9 1.1 copy-start.1
  40.9 1.1 copy-start.14
  40.9 1.4 copy-start.15
  41.5 4.7 %copy-start.7 = (bf16[384,192]{1,0:T(8,128)(2,1)}, bf16[384,192]{1,0:T(8,128)(2,1)S(1)}, u32[]{:S(2)}) copy-start(bf16[384,192]{1,0:T(8,128)(2,1)S(1)} %convolution_convert_fusion) | copy-start | bytes 442372
  42.9 20.9 %copy-start.9 = (bf16[384,128]{1,0:T(8,128)(2,1)}, bf16[384,128]{1,0:T(8,128)(2,1)S(1)}, u32[]{:S(2)}) copy-start(bf16[384,128]{1,0:T(8,128)(2,1)S(1)} %convolution_convert_fusion.3) | copy-start | bytes 294916
  42.9 22.3 %collective-permute-start.4 = (bf16[128,128]{1,0:T(8,128)(2,1)S(1)}, bf16[128,128]{1,0:T(8,128)(2,1)S(1)}, u32[]{:S(2)}, u32[]{:S(2)}) collective-permute-start(bf16[128,128]{1,0:T(8,128)(2,1)S(1)} %slice.211), channel_id=1, source_target_pairs={{0,8},{8,16},{16,24},{24,32},{32,40},{40,48},{48,56},{56,64},{64,7... | collective-permute-start | bytes 98312 | tf_op jit(solution)/shard_map/ppermute | solution.py:317
  63.6 0.7 copy-start.13
  65.8 10.1 %copy-start.2 = (bf16[4,2,48,2048]{3,2,1,0:T(8,128)(2,1)S(1)}, bf16[4,2,48,2048]{3,2,1,0:T(8,128)(2,1)}, u32[]{:S(2)}) copy-start(bf16[4,2,48,2048]{3,2,1,0:T(8,128)(2,1)} %copy-done.1) | copy-start | bytes 4718596
  66.9 32.1 %all-to-all-start.1 = ((bf16[32,120,128]{2,1,0:T(8,128)(2,1)}), bf16[32,120,128]{2,1,0:T(8,128)(2,1)S(1)}, u32[]{:S(2)}, u32[]{:S(2)}) async-start(bf16[32,120,128]{2,1,0:T(8,128)(2,1)} %broadcast_in_dim.87), calls=%async_computation.1 | async-start | bytes 1966080 | tf_op jit(solution)/shard_map/all_to_all | solution.py:42
  74.3 3.3 %copy-start.8 = (pred[384,512]{0,1:T(8,128)(4,1)S(1)}, pred[384,512]{0,1:T(8,128)(4,1)}, u32[]{:S(2)}) copy-start(pred[384,512]{0,1:T(8,128)(4,1)} %fusion.8) | copy-start | bytes 589828
  75.9 1.7 copy-start.11
  78.4 0.9 slice-start
  79.5 9.2 %collective-permute-start.5 = (bf16[384,384]{1,0:T(8,128)(2,1)S(1)}, bf16[384,384]{1,0:T(8,128)(2,1)S(1)}, u32[]{:S(2)}, u32[]{:S(2)}) collective-permute-start(bf16[384,384]{1,0:T(8,128)(2,1)S(1)} %concatenate.42), channel_id=1, source_target_pairs={{0,2},{2,4},{4,6},{6,0},{1,3},{3,5},{5,7},{7,1},{8,10},{10,12},{12... | collective-permute-start | bytes 884744 | tf_op jit(solution)/shard_map/ppermute | solution.py:56
  82.3 12.5 %collective-permute-start.6 = (bf16[384,384]{1,0:T(8,128)(2,1)S(1)}, bf16[384,384]{1,0:T(8,128)(2,1)S(1)}, u32[]{:S(2)}, u32[]{:S(2)}) collective-permute-start(bf16[384,384]{1,0:T(8,128)(2,1)S(1)} %concatenate.42), channel_id=1, source_target_pairs={{0,4},{2,6},{4,0},{6,2},{1,5},{3,7},{5,1},{7,3},{8,12},{10,14},{12... | collective-permute-start | bytes 884744 | tf_op jit(solution)/shard_map/ppermute | solution.py:56
  85.3 13.5 %collective-permute-start.7 = (bf16[384,384]{1,0:T(8,128)(2,1)S(1)}, bf16[384,384]{1,0:T(8,128)(2,1)S(1)}, u32[]{:S(2)}, u32[]{:S(2)}) collective-permute-start(bf16[384,384]{1,0:T(8,128)(2,1)S(1)} %concatenate.42), channel_id=1, source_target_pairs={{0,6},{2,0},{4,2},{6,4},{1,7},{3,1},{5,3},{7,5},{8,14},{10,8},{12,... | collective-permute-start | bytes 884744 | tf_op jit(solution)/shard_map/ppermute | solution.py:56
  98.9 15.8 %copy-start.4 = (bf16[4,384,384]{2,1,0:T(8,128)(2,1)}, bf16[4,384,384]{2,1,0:T(8,128)(2,1)S(1)}, u32[]{:S(2)}) copy-start(bf16[4,384,384]{2,1,0:T(8,128)(2,1)S(1)} %bitcast_dynamic-update-slice_fusion.2.refs_1_) | copy-start | bytes 3538948
  99.0 15.7 %copy-start.3 = (bf16[32,120,128]{2,1,0:T(8,128)(2,1)}, bf16[32,120,128]{2,1,0:T(8,128)(2,1)S(1)}, u32[]{:S(2)}) copy-start(bf16[32,120,128]{2,1,0:T(8,128)(2,1)S(1)} %all-to-all-done.1.refs_0_) | copy-start | bytes 2949124
  100.3 21.5 %collective-permute-start.8 = (bf16[16,120,128]{2,1,0:T(8,128)(2,1)}, bf16[16,120,128]{2,1,0:T(8,128)(2,1)}, u32[]{:S(2)}, u32[]{:S(2)}) collective-permute-start(bf16[16,120,128]{2,1,0:T(8,128)(2,1)} %get-tuple-element.57), channel_id=1, source_target_pairs={{0,8},{8,16},{16,24},{24,32},{32,40},{40,48},{48,56},{56,0},{1,9},... | collective-permute-start | bytes 1474568 | tf_op jit(solution)/shard_map/ppermute | solution.py:61
  109.6 13.7 %collective-permute-start.9 = (bf16[16,120,128]{2,1,0:T(8,128)(2,1)}, bf16[16,120,128]{2,1,0:T(8,128)(2,1)}, u32[]{:S(2)}, u32[]{:S(2)}) collective-permute-start(bf16[16,120,128]{2,1,0:T(8,128)(2,1)} %get-tuple-element.58), channel_id=1, source_target_pairs={{0,56},{8,0},{16,8},{24,16},{32,24},{40,32},{48,40},{56,48},{1,57}... | collective-permute-start | bytes 1474568 | tf_op jit(solution)/shard_map/ppermute | solution.py:61
  111.5 22.8 %collective-permute-start.11 = (bf16[32,120,128]{2,1,0:T(8,128)(2,1)S(1)}, bf16[32,120,128]{2,1,0:T(8,128)(2,1)}, u32[]{:S(2)}, u32[]{:S(2)}) collective-permute-start(bf16[32,120,128]{2,1,0:T(8,128)(2,1)S(1)} %all-to-all-done.1.refs_0_), channel_id=1, source_target_pairs={{0,1},{1,0},{2,3},{3,2},{4,5},{5,4},{6,7},{7,6},{8,9},{9,8},{10,11... | collective-permute-start | bytes 2949128 | tf_op jit(solution)/shard_map/ppermute | solution.py:51
  125.6 15.4 %collective-permute-start.10 = (bf16[32,120,128]{2,1,0:T(8,128)(2,1)}, bf16[32,120,128]{2,1,0:T(8,128)(2,1)}, u32[]{:S(2)}, u32[]{:S(2)}) collective-permute-start(bf16[32,120,128]{2,1,0:T(8,128)(2,1)} %pad_maximum_fusion.1.refs_0_), channel_id=1, source_target_pairs={{0,1},{1,0},{2,3},{3,2},{4,5},{5,4},{6,7},{7,6},{8,9},{9,8},{10,11... | collective-permute-start | bytes 2949128 | tf_op jit(solution)/shard_map/ppermute | solution.py:51
  129.6 3.6 %collective-permute-start.12 = (bf16[4,384,128]{2,1,0:T(8,128)(2,1)S(1)}, bf16[4,384,128]{2,1,0:T(8,128)(2,1)S(1)}, u32[]{:S(2)}, u32[]{:S(2)}) collective-permute-start(bf16[4,384,128]{2,1,0:T(8,128)(2,1)S(1)} %slice.218), channel_id=1, source_target_pairs={{0,1},{1,0},{2,3},{3,2},{4,5},{5,4},{6,7},{7,6},{8,9},{9,8},{10,11... | collective-permute-start | bytes 1179656 | tf_op jit(solution)/shard_map/ppermute | solution.py:51
  133.2 21.6 %copy-start.6 = (bf16[4,384,128]{2,1,0:T(8,128)(2,1)}, bf16[4,384,128]{2,1,0:T(8,128)(2,1)S(1)}, u32[]{:S(2)}) copy-start(bf16[4,384,128]{2,1,0:T(8,128)(2,1)S(1)} %collective-permute-done.12) | copy-start | bytes 1179652
  151.3 16.2 %all-to-all-start.2 = ((bf16[4,272,384]{2,1,0:T(8,128)(2,1)}), bf16[4,272,384]{2,1,0:T(8,128)(2,1)S(1)}, u32[]{:S(2)}, u32[]{:S(2)}) async-start(bf16[4,272,384]{2,1,0:T(8,128)(2,1)} %shard_map.138), calls=%async_computation.2 | async-start | bytes 1671168 | tf_op jit(solution)/shard_map/all_to_all | solution.py:42
  170.0 16.6 %all-to-all-start.3 = ((bf16[8,384,128]{2,1,0:T(8,128)(2,1)}), bf16[8,384,128]{2,1,0:T(8,128)(2,1)S(1)}, u32[]{:S(2)}, u32[]{:S(2)}) async-start(bf16[8,384,128]{2,1,0:T(8,128)(2,1)} %broadcast_in_dim.96), calls=%async_computation.3 | async-start | bytes 1572864 | tf_op jit(solution)/shard_map/all_to_all | solution.py:42
  178.5 9.5 %copy-start.5 = (f32[384,256]{1,0:T(8,128)S(1)}, f32[384,256]{1,0:T(8,128)}, u32[]{:S(2)}) copy-start(f32[384,256]{1,0:T(8,128)} %convolution_add_fusion.1) | copy-start | bytes 1179652

commit v5 on v4

--- a/solution.py
+++ b/solution.py
@@ -219,9 +219,9 @@
 
 def attend(where, parts, queries, state, last):
     state_shapes = (
-        jax.ShapeDtypeStruct((TILES, KV_RANK, QTILE), jnp.float32),
-        jax.ShapeDtypeStruct((TILES, 1, QTILE), jnp.float32),
-        jax.ShapeDtypeStruct((TILES, 1, QTILE), jnp.float32),
+        pltpu.VMEM((TILES, KV_RANK, QTILE), jnp.float32),
+        pltpu.VMEM((TILES, 1, QTILE), jnp.float32),
+        pltpu.VMEM((TILES, 1, QTILE), jnp.float32),
     )
     first = state is None
     smem = pl.BlockSpec(memory_space=pltpu.SMEM)
@@ -229,13 +229,18 @@
     scratch = [pltpu.VMEM((CHUNK * OWN, 3 * LANES), jnp.bfloat16)]
     out_shape = state_shapes
     if first:
-        out_shape = (*state_shapes, jax.ShapeDtypeStruct((QROWS, 3 * LANES), jnp.bfloat16))
+        out_shape = (*state_shapes, pltpu.VMEM((QROWS, 3 * LANES), jnp.bfloat16))
         operands = (where, *parts, *queries)
     else:
         operands = (where, *parts, queries, *state)
     if last:
         out_shape = jax.ShapeDtypeStruct((HEADS_CORE, KV_RANK + STAT_ROWS, ROWS), jnp.bfloat16)
-        scratch = [pltpu.VMEM(s.shape, s.dtype) for s in state_shapes] + scratch
+        scratch = list(state_shapes) + scratch
+    if not first:
+        operands = operands[: 1 + len(parts)] + tuple(
+            pltpu.with_memory_space_constraint(value, pltpu.VMEM)
+            for value in operands[1 + len(parts) :]
+        )
     n_keys = SOURCES // 2 * OWN * len(parts)
     return pl.pallas_call(
         functools.partial(attend_body, n_parts=len(parts), first=first, last=last),
@@ -243,12 +248,83 @@
         in_specs=[smem] + [vmem] * (len(operands) - 1),
         out_specs=jax.tree.map(lambda _: vmem, out_shape),
         scratch_shapes=scratch,
+        compiler_params=pltpu.CompilerParams(vmem_limit_bytes=24 * 1024 * 1024),
         cost_estimate=pl.CostEstimate(
             flops=2 * QROWS * n_keys * (3 * LANES + KV_RANK),
             transcendentals=QROWS * n_keys,
             bytes_accessed=6000000,
         ),
     )(*operands)
+
+
+def joined_body(low_ref, high_ref, out_ref):
+    half = low_ref.shape[0]
+    out_ref[:half] = low_ref[...]
+    out_ref[half:] = high_ref[...]
+
+
+def joined(low, high):
+    vmem = pl.BlockSpec(memory_space=pltpu.VMEM)
+    return pl.pallas_call(
+        joined_body,
+        out_shape=jax.ShapeDtypeStruct((2 * low.shape[0], *low.shape[1:]), low.dtype),
+        in_specs=[vmem, vmem],
+        out_specs=vmem,
+        compiler_params=pltpu.CompilerParams(vmem_limit_bytes=8 * 1024 * 1024),
+        name="joined",
+    )(low, high)
+
+
+def windowed_body(where_ref, sink_ref, rows_ref, before_ref, query_ref, out_ref):
+    out_ref[:, : 2 * LANES] = query_ref[...]
+    for tile in range(ROWS // WINDOW):
+        here = rows_ref[tile * WINDOW : (tile + 1) * WINDOW]
+        if tile == 0:
+            behind = before_ref[...]
+        else:
+            behind = rows_ref[(tile - 1) * WINDOW : tile * WINDOW, LANES:]
+        both = jnp.concatenate([behind, here[:, LANES:]], axis=0)
+        row = lax.broadcasted_iota(jnp.int32, (WINDOW, 2 * WINDOW), 0)
+        col = lax.broadcasted_iota(jnp.int32, (WINDOW, 2 * WINDOW), 1)
+        allowed = (col > row) & (col <= row + WINDOW)
+        if tile == 0:
+            allowed = allowed & ((col >= WINDOW) | (where_ref[0] > 0))
+        outs = []
+        for h in range(LANES // HEAD):
+            scores = lax.dot_general(
+                here[:, h * HEAD : (h + 1) * HEAD],
+                both[:, :HEAD],
+                (((1,), (1,)), ((), ())),
+                preferred_element_type=jnp.float32,
+            ) * HEAD ** (-0.5)
+            scores = jnp.where(allowed, scores, MASKED_VALUE)
+            sink = jnp.full((WINDOW, 1), sink_ref[where_ref[2] * (LANES // HEAD) + h])
+            row_max = jnp.maximum(jnp.max(scores, axis=1, keepdims=True), sink)
+            raw = jnp.exp(scores - row_max)
+            total = jnp.sum(raw, axis=1, keepdims=True) + jnp.exp(sink - row_max)
+            weights = (raw / total).astype(jnp.bfloat16)
+            outs.append(jnp.dot(weights, both[:, HEAD:], preferred_element_type=jnp.float32))
+        out_ref[tile * WINDOW : (tile + 1) * WINDOW, 2 * LANES :] = jnp.concatenate(
+            outs, axis=1
+        ).astype(jnp.bfloat16)
+
+
+def windowed(where, sink_logits, rows, before, query):
+    smem = pl.BlockSpec(memory_space=pltpu.SMEM)
+    vmem = pl.BlockSpec(memory_space=pltpu.VMEM)
+    return pl.pallas_call(
+        windowed_body,
+        out_shape=jax.ShapeDtypeStruct((ROWS, 3 * LANES), jnp.bfloat16),
+        in_specs=[smem, smem, vmem, vmem, vmem],
+        out_specs=vmem,
+        compiler_params=pltpu.CompilerParams(vmem_limit_bytes=16 * 1024 * 1024),
+        cost_estimate=pl.CostEstimate(
+            flops=4 * ROWS * 2 * WINDOW * LANES,
+            transcendentals=ROWS * 4 * WINDOW,
+            bytes_accessed=1000000,
+        ),
+        name="windowed",
+    )(where, sink_logits, rows, before, query)
 
 
 def layer(
@@ -275,7 +351,6 @@
     offset = block * ROWS
     own_pos = offset + tp_rank * own_rows + jnp.arange(own_rows, dtype=jnp.int32)
     block_pos = offset + jnp.arange(ROWS, dtype=jnp.int32)
-    heads_swa = swa_query.shape[1] // HEAD
 
     x_count = lax.axis_size("x")
 
@@ -304,18 +379,18 @@
     down_latent = down_latent.reshape(-1, KV_RANK)
 
     normed = norm_rows(inputs, norm_gain)
-    kv_weights = jnp.concatenate([swa_key, swa_value], axis=1)
+    swa_weights = jnp.concatenate([swa_query, swa_key, swa_value], axis=1)
     mine = by_x(normed)
     other = from_core(mine)
     pieces = jnp.zeros((x_count, 2, *mine.shape[1:]), jnp.bfloat16)
     pieces = lax.dynamic_update_index_in_dim(pieces, mine, c_rank, 1)
     pieces = lax.dynamic_update_index_in_dim(pieces, other, 1 - c_rank, 1)
     pieces = pieces.reshape(ROWS, -1)
-    swa_kv = jnp.dot(pieces, kv_weights, preferred_element_type=jnp.float32)
-    swa_kv = swa_kv.astype(jnp.bfloat16)
+    swa_rows = jnp.dot(pieces, swa_weights, preferred_element_type=jnp.float32)
+    swa_rows = swa_rows.astype(jnp.bfloat16)
     count = lax.axis_size(SP)
     before = lax.ppermute(
-        swa_kv[ROWS - WINDOW :], SP, [(i, i + 1) for i in range(count - 1)]
+        swa_rows[ROWS - WINDOW :, LANES:], SP, [(i, i + 1) for i in range(count - 1)]
     )
     queries = jnp.dot(pieces, mla_query, preferred_element_type=jnp.float32)
     queries = queries.astype(jnp.bfloat16)
@@ -340,36 +415,6 @@
         ],
         axis=0,
     )
-    packed, pieces, swa_kv, before = lax.optimization_barrier((packed, pieces, swa_kv, before))
-    keys_own = to_everyone(packed, SAME_PARITY)
-
-    swa_q = jnp.dot(pieces, swa_query, preferred_element_type=jnp.float32)
-    swa_q = swa_q.astype(jnp.bfloat16)
-    window = jnp.concatenate([before, swa_kv], axis=0)
-    window_keys, window_values = window[:, :HEAD], window[:, HEAD:]
-    scores = jnp.einsum(
-        "tgd,sd->gts",
-        swa_q.reshape(ROWS, heads_swa, HEAD),
-        window_keys,
-        preferred_element_type=jnp.float32,
-    ) * HEAD ** (-0.5)
-    key_pos = offset - WINDOW + jnp.arange(WINDOW + ROWS, dtype=jnp.int32)
-    distance = block_pos[:, None] - key_pos[None, :]
-    allowed = (distance >= 0) & (distance < WINDOW) & (key_pos[None, :] >= 0)
-    scores = jnp.where(allowed, scores, MASKED_VALUE)
-    sink = lax.dynamic_slice_in_dim(sink_logits, tp_rank * heads_swa, heads_swa, 0)
-    sink = sink.reshape(heads_swa, 1, 1)
-    row_max = jnp.maximum(jnp.max(scores, axis=-1, keepdims=True), sink)
-    raw = jnp.exp(scores - row_max)
-    weights = (
-        raw / (jnp.sum(raw, axis=-1, keepdims=True) + jnp.exp(sink - row_max))
-    ).astype(jnp.bfloat16)
-    swa_out = jnp.einsum("gts,sd->tgd", weights, window_values, preferred_element_type=jnp.float32)
-    swa_out = swa_out.astype(jnp.bfloat16).reshape(ROWS, heads_swa * HEAD)
-    sent = jnp.concatenate([query, swa_out], axis=1)
-    sent = by_x(sent)
-    swa_x = sent[:, :, 2 * LANES :]
-    swa_other = from_core(swa_x)
     up_heads = jnp.stack(
         [lax.dynamic_slice_in_dim(key_up, (2 * x + c_rank) * NOPE, NOPE, 1) for x in range(x_count)]
     )
@@ -383,6 +428,15 @@
             (block, 1 - parity, tp_rank, rank_other),
         )
     ]
+    packed, swa_rows, before, query, up_heads, where = lax.optimization_barrier(
+        (packed, swa_rows, before, query, up_heads, where)
+    )
+    keys_own = to_everyone(packed, SAME_PARITY)
+
+    sent = windowed(where[0], sink_logits, swa_rows, before, query)
+    sent = by_x(sent)
+    swa_x = sent[:, :, 2 * LANES :]
+    swa_other = from_core(swa_x)
     keys_own, sent, up_heads, swa_x, where = lax.optimization_barrier(
         (keys_own, sent, up_heads, swa_x, where)
     )
@@ -391,8 +445,7 @@
     high = from_y(keys_own[half:], -1)
     keys_other = from_core(keys_own)
     *state, q_all = attend(where[0], (keys_own,), (sent, up_heads), None, False)
-    far_own = jnp.concatenate([low, high], axis=0)
-    far_own, state = lax.optimization_barrier((far_own, state))
+    far_own = joined(low, high)
     far_other = from_core(far_own)
     state = attend(where[1], (keys_other,), q_all, state, False)
     partial = attend(where[2], (far_own, far_other), q_all, state, True)

time: 193 us -> 194 us (level)
  the two profiles are of different devices: /device:TPU:1 before, /device:TPU:320 now
where the time goes in v5:
time: 194 us; the launch traced here: 192 us
  starting transfers between devices  68.4 us (35%)
  waiting for transfers between devices  60.5 us (31%)
  Pallas kernels  32.1 us (17%)
  matrix products  14.5 us (7%)
  local copies, waits for them, and re-layouts  11.5 us (6%)
  other arithmetic  4.53 us (2%)
    all_to_all x4, waiting for transfers between devices, exchange(): return lax.all_to_all(array, axis, split_axis=0, concat_axis=0, tiled=True)  42.3 us
    pallas_call x3, Pallas kernels, attend(): pl.pallas_call(functools.partial(attend_body, n_parts=len(parts), first=f...  29.4 us
    all_to_all x4, starting transfers between devices, exchange(): return lax.all_to_all(array, axis, split_axis=0, concat_axis=0, tiled=True)  28 us
    ppermute x6, starting transfers between devices, from_x(): lax.ppermute(value, 'x', [(i, (i + step) % count) for i in range(count)])  20.4 us
    dot_general x8, matrix products, layer(): jnp.dot(values[x], weights[x], preferred_element_type=jnp.float32)  10.2 us
    ppermute x6, waiting for transfers between devices, from_x(): lax.ppermute(value, 'x', [(i, (i + step) % count) for i in range(count)])  9.07 us
    ppermute x2, starting transfers between devices, from_y(): lax.ppermute(value, Y, [(i, (i + step) % count) for i in range(count)])  8.52 us
    ppermute x4, starting transfers between devices, from_core(): return lax.ppermute(value, 'c', [(0, 1), (1, 0)])  8.16 us
  transfers between devices with their start and end apart: 17, of which 9 were waited for; matrix products, arithmetic and copies ran while one was open for 11% of the time, Pallas kernels for 9%

profile of v5, /device:TPU:320, one launch (start us, length us, event | category | flops | bytes accessed | tf_op | source)
XLA Modules:
  0.0 192.4 jit_solution(4009780124443615201)
XLA Ops:
  0.0 1.1 fusion.11
  1.3 1.1 bitcast_dynamic-update-slice_fusion.9
  2.3 3.4 %collective-permute-start = (bf16[48,2048]{1,0:T(8,128)(2,1)S(1)}, bf16[48,2048]{1,0:T(8,128)(2,1)}, u32[]{:S(2)}, u32[]{:S(2)}) collective-permute-start(bf16[48,2048]{1,0:T(8,128)(2,1)S(1)} %get-tuple-element.52), channel_id=1, source_target_pairs={{0,2},{2,4},{4,6},{6,0},{1,3},{3,5},{5,7},{7,1},{8,10},{10,12},{12... | collective-permute-start | bytes 589832 | tf_op jit(solution)/shard_map/ppermute | solution.py:56
  5.8 4.6 %collective-permute-start.1 = (bf16[48,2048]{1,0:T(8,128)(2,1)S(1)}, bf16[48,2048]{1,0:T(8,128)(2,1)}, u32[]{:S(2)}, u32[]{:S(2)}) collective-permute-start(bf16[48,2048]{1,0:T(8,128)(2,1)S(1)} %get-tuple-element.52), channel_id=1, source_target_pairs={{0,4},{2,6},{4,0},{6,2},{1,5},{3,7},{5,1},{7,3},{8,12},{10,14},{12... | collective-permute-start | bytes 589832 | tf_op jit(solution)/shard_map/ppermute | solution.py:56
  10.4 3.3 %collective-permute-start.2 = (bf16[48,2048]{1,0:T(8,128)(2,1)S(1)}, bf16[48,2048]{1,0:T(8,128)(2,1)S(1)}, u32[]{:S(2)}, u32[]{:S(2)}) collective-permute-start(bf16[48,2048]{1,0:T(8,128)(2,1)S(1)} %get-tuple-element.52), channel_id=1, source_target_pairs={{0,6},{2,0},{4,2},{6,4},{1,7},{3,1},{5,3},{7,5},{8,14},{10,8},{12,... | collective-permute-start | bytes 589832 | tf_op jit(solution)/shard_map/ppermute | solution.py:56
  13.9 1.2 broadcast_in_dim.65
  15.1 12.6 %all-to-all-start = ((bf16[64,80,128]{2,1,0:T(8,128)(2,1)}), bf16[64,80,128]{2,1,0:T(8,128)(2,1)}, u32[]{:S(2)}, u32[]{:S(2)}) async-start(bf16[64,80,128]{2,1,0:T(8,128)(2,1)} %broadcast_in_dim.65), calls=%async_computation | async-start | bytes 2621440 | tf_op jit(solution)/shard_map/all_to_all | solution.py:42
  30.6 1.9 collective-permute-start.3
  32.6 1.0 dynamic-slice_bitcast_fusion.19
  36.6 3.4 %collective-permute-start.4 = (bf16[128,128]{1,0:T(8,128)(2,1)S(1)}, bf16[128,128]{1,0:T(8,128)(2,1)S(1)}, u32[]{:S(2)}, u32[]{:S(2)}) collective-permute-start(bf16[128,128]{1,0:T(8,128)(2,1)S(1)} %slice.203), channel_id=1, source_target_pairs={{0,8},{8,16},{16,24},{24,32},{32,40},{40,48},{48,56},{56,64},{64,7... | collective-permute-start | bytes 98312 | tf_op jit(solution)/shard_map/ppermute | solution.py:392
  40.9 18.8 %all-to-all-done = bf16[64,80,128]{2,1,0:T(8,128)(2,1)} async-done(((bf16[64,80,128]{2,1,0:T(8,128)(2,1)}), bf16[64,80,128]{2,1,0:T(8,128)(2,1)}, u32[]{:S(2)}, u32[]{:S(2)}) %all-to-all-start) | async-done | bytes 1310752 | tf_op jit(solution)/shard_map/all_to_all | solution.py:42
  59.7 1.3 fusion.70
  61.7 1.2 slice_bitcast_fusion.1
  63.6 1.1 broadcast_in_dim.75
  64.7 8.3 %all-to-all-start.1 = ((bf16[32,120,128]{2,1,0:T(8,128)(2,1)}), bf16[32,120,128]{2,1,0:T(8,128)(2,1)S(1)}, u32[]{:S(2)}, u32[]{:S(2)}) async-start(bf16[32,120,128]{2,1,0:T(8,128)(2,1)} %broadcast_in_dim.75), calls=%async_computation.1 | async-start | bytes 1966080 | tf_op jit(solution)/shard_map/all_to_all | solution.py:42
  73.1 1.6 windowed.1
  74.7 2.5 %collective-permute-start.5 = (bf16[384,384]{1,0:T(8,128)(2,1)S(1)}, bf16[384,384]{1,0:T(8,128)(2,1)S(1)}, u32[]{:S(2)}, u32[]{:S(2)}) collective-permute-start(bf16[384,384]{1,0:T(8,128)(2,1)S(1)} %windowed.1), channel_id=1, source_target_pairs={{0,2},{2,4},{4,6},{6,0},{1,3},{3,5},{5,7},{7,1},{8,10},{10,12},{12... | collective-permute-start | bytes 884744 | tf_op jit(solution)/shard_map/ppermute | solution.py:56
  77.2 3.1 %collective-permute-start.6 = (bf16[384,384]{1,0:T(8,128)(2,1)S(1)}, bf16[384,384]{1,0:T(8,128)(2,1)S(1)}, u32[]{:S(2)}, u32[]{:S(2)}) collective-permute-start(bf16[384,384]{1,0:T(8,128)(2,1)S(1)} %windowed.1), channel_id=1, source_target_pairs={{0,4},{2,6},{4,0},{6,2},{1,5},{3,7},{5,1},{7,3},{8,12},{10,14},{12... | collective-permute-start | bytes 884744 | tf_op jit(solution)/shard_map/ppermute | solution.py:56
  80.4 3.4 %collective-permute-start.7 = (bf16[384,384]{1,0:T(8,128)(2,1)S(1)}, bf16[384,384]{1,0:T(8,128)(2,1)S(1)}, u32[]{:S(2)}, u32[]{:S(2)}) collective-permute-start(bf16[384,384]{1,0:T(8,128)(2,1)S(1)} %windowed.1), channel_id=1, source_target_pairs={{0,6},{2,0},{4,2},{6,4},{1,7},{3,1},{5,3},{7,5},{8,14},{10,8},{12,... | collective-permute-start | bytes 884744 | tf_op jit(solution)/shard_map/ppermute | solution.py:56
  83.9 6.7 %collective-permute-done.5 = bf16[384,384]{1,0:T(8,128)(2,1)S(1)} collective-permute-done((bf16[384,384]{1,0:T(8,128)(2,1)S(1)}, bf16[384,384]{1,0:T(8,128)(2,1)S(1)}, u32[]{:S(2)}, u32[]{:S(2)}) %collective-permute-start.5) | collective-permute-done | bytes 294944 | tf_op jit(solution)/shard_map/ppermute | solution.py:56
  90.7 2.4 %collective-permute-done.7 = bf16[384,384]{1,0:T(8,128)(2,1)S(1)} collective-permute-done((bf16[384,384]{1,0:T(8,128)(2,1)S(1)}, bf16[384,384]{1,0:T(8,128)(2,1)S(1)}, u32[]{:S(2)}, u32[]{:S(2)}) %collective-permute-start.7) | collective-permute-done | bytes 294944 | tf_op jit(solution)/shard_map/ppermute | solution.py:56
  94.0 3.4 %all-to-all-done.1.refs_0_ = bf16[32,120,128]{2,1,0:T(8,128)(2,1)S(1)} async-done(((bf16[32,120,128]{2,1,0:T(8,128)(2,1)}), bf16[32,120,128]{2,1,0:T(8,128)(2,1)S(1)}, u32[]{:S(2)}, u32[]{:S(2)}) %all-to-all-start.1) | async-done | bytes 983072 | tf_op jit(solution)/shard_map/all_to_all | solution.py:42
  97.5 6.6 %collective-permute-start.8 = (bf16[16,120,128]{2,1,0:T(8,128)(2,1)S(1)}, bf16[16,120,128]{2,1,0:T(8,128)(2,1)S(1)}, u32[]{:S(2)}, u32[]{:S(2)}) collective-permute-start(bf16[16,120,128]{2,1,0:T(8,128)(2,1)S(1)} %get-tuple-element.58), channel_id=1, source_target_pairs={{0,8},{8,16},{16,24},{24,32},{32,40},{40,48},{48,56},{56,0},{1,9},... | collective-permute-start | bytes 1474568 | tf_op jit(solution)/shard_map/ppermute | solution.py:61
  104.1 1.9 collective-permute-start.9
  106.1 1.9 collective-permute-start.11
  108.0 2.4 %collective-permute-start.12 = (bf16[4,384,128]{2,1,0:T(8,128)(2,1)}, bf16[4,384,128]{2,1,0:T(8,128)(2,1)}, u32[]{:S(2)}, u32[]{:S(2)}) collective-permute-start(bf16[4,384,128]{2,1,0:T(8,128)(2,1)} %slice.208), channel_id=1, source_target_pairs={{0,1},{1,0},{2,3},{3,2},{4,5},{5,4},{6,7},{7,6},{8,9},{9,8},{10,11... | collective-permute-start | bytes 1179656 | tf_op jit(solution)/shard_map/ppermute | solution.py:51
  110.4 4.2 %collective-permute-done.8.low_ref = bf16[16,120,128]{2,1,0:T(8,128)(2,1)S(1)} collective-permute-done((bf16[16,120,128]{2,1,0:T(8,128)(2,1)S(1)}, bf16[16,120,128]{2,1,0:T(8,128)(2,1)S(1)}, u32[]{:S(2)}, u32[]{:S(2)}) %collective-permute-start.8) | collective-permute-done | bytes 491552 | tf_op jit(solution)/shard_map/ppermute | solution.py:61
  114.6 3.9 %collective-permute-done.9.high_ref = bf16[16,120,128]{2,1,0:T(8,128)(2,1)S(1)} collective-permute-done((bf16[16,120,128]{2,1,0:T(8,128)(2,1)S(1)}, bf16[16,120,128]{2,1,0:T(8,128)(2,1)S(1)}, u32[]{:S(2)}, u32[]{:S(2)}) %collective-permute-start.9) | collective-permute-done | bytes 491552 | tf_op jit(solution)/shard_map/ppermute | solution.py:61
  118.5 1.1 joined.1.refs_0_
  119.6 1.9 collective-permute-start.10
  121.5 1.8 fusion.22
  123.4 7.1 %shard_map.136 = (f32[3,256,512]{2,1,0:T(8,128)S(1)}, f32[3,1,512]{2,1,0:T(1,128)S(1)}, f32[3,1,512]{2,1,0:T(1,128)S(1)}, bf16[1536,384]{1,0:T(8,128)(2,1)S(1)}) custom-call(s32[3]{0:T(128)S(1)} %get-tuple-element.37.where_ref, bf16[32,120,128]{2,1,0:T(8,128)(2,1)S(1)} %all-to-all-done.1.refs_0_, ...), custom_call_target="tpu_custom_call" | custom-call | flops 3019898880 | bytes 6000000 | tf_op jit(solution)/shard_map/pallas_call | solution.py:245
  130.5 7.2 %shard_map.137 = (f32[3,256,512]{2,1,0:T(8,128)S(1)}, f32[3,1,512]{2,1,0:T(1,128)S(1)}, f32[3,1,512]{2,1,0:T(1,128)S(1)}) custom-call(s32[3]{0:T(128)S(1)} %get-tuple-element.41.where_ref, bf16[32,120,128]{2,1,0:T(8,128)(2,1)} %collective-permute-done.11.refs_0_, bf16[1536,384]{1,0:T(8,128)(2,1)S(1)} %get-tuple-element.40.refs_1_.refs_2_, ...), custom_call_target="tpu_custom_call" | custom-call | flops 3019898880 | bytes 6000000 | tf_op jit(solution)/shard_map/pallas_call | solution.py:245
  137.7 15.1 %shard_map.138 = bf16[4,272,384]{2,1,0:T(8,128)(2,1)} custom-call(s32[4]{0:T(128)S(1)} %pad_add_fusion.3.where_ref, bf16[32,120,128]{2,1,0:T(8,128)(2,1)} %joined.1.refs_0_, bf16[32,120,128]{2,1,0:T(8,128)(2,1)} %collective-permute-done.10.refs_1_, bf16[1536,384]{1,0:T(8,128)(2,1)S(1)} %get-tuple-element.40.refs_1_.refs_2_, ...), custom_call_target="tpu_custom_call" | custom-call | flops 6039797760 | bytes 6000000 | tf_op jit(solution)/shard_map/pallas_call | solution.py:245
  152.8 3.5 %all-to-all-start.2 = ((bf16[4,272,384]{2,1,0:T(8,128)(2,1)}), bf16[4,272,384]{2,1,0:T(8,128)(2,1)S(1)}, u32[]{:S(2)}, u32[]{:S(2)}) async-start(bf16[4,272,384]{2,1,0:T(8,128)(2,1)} %shard_map.138), calls=%async_computation.2 | async-start | bytes 1671168 | tf_op jit(solution)/shard_map/all_to_all | solution.py:42
  156.3 1.1 fusion.23
  157.4 1.1 fusion.24
  158.5 1.1 fusion.28
  159.6 10.4 %all-to-all-done.2 = bf16[4,272,384]{2,1,0:T(8,128)(2,1)S(1)} async-done(((bf16[4,272,384]{2,1,0:T(8,128)(2,1)}), bf16[4,272,384]{2,1,0:T(8,128)(2,1)S(1)}, u32[]{:S(2)}, u32[]{:S(2)}) %all-to-all-start.2) | async-done | bytes 835616 | tf_op jit(solution)/shard_map/all_to_all | solution.py:42
  170.4 1.1 convolution_convert_fusion.2
  171.5 1.0 broadcast_in_dim.81
  172.5 3.5 %all-to-all-start.3 = ((bf16[8,384,128]{2,1,0:T(8,128)(2,1)}), bf16[8,384,128]{2,1,0:T(8,128)(2,1)S(1)}, u32[]{:S(2)}, u32[]{:S(2)}) async-start(bf16[8,384,128]{2,1,0:T(8,128)(2,1)} %broadcast_in_dim.81), calls=%async_computation.3 | async-start | bytes 1572864 | tf_op jit(solution)/shard_map/all_to_all | solution.py:42
  176.0 1.1 convolution_add_fusion.3
  177.2 1.1 convolution_add_fusion.2
  178.3 1.1 convolution_add_fusion.1
  179.4 9.7 %all-to-all-done.3 = bf16[8,384,128]{2,1,0:T(8,128)(2,1)S(1)} async-done(((bf16[8,384,128]{2,1,0:T(8,128)(2,1)}), bf16[8,384,128]{2,1,0:T(8,128)(2,1)S(1)}, u32[]{:S(2)}, u32[]{:S(2)}) %all-to-all-start.3) | async-done | bytes 786464 | tf_op jit(solution)/shard_map/all_to_all | solution.py:42
  189.1 1.4 convolution_bitcast_fusion
  190.5 1.8 fusion.5
  (82 shorter events, 9.7 us)
Async XLA Ops:
  0.0 34.8 %copy-start = (bf16[2048,192]{0,1:T(8,128)(2,1)S(1)}, bf16[2048,192]{0,1:T(8,128)(2,1)}, u32[]{:S(2)}) copy-start(bf16[2048,192]{0,1:T(8,128)(2,1)} %param.19) | copy-start | bytes 2359300
  0.0 13.7 %copy-start.5 = (bf16[32,256]{1,0:T(8,128)(2,1)S(1)}, bf16[32,256]{1,0:T(8,128)(2,1)}, u32[]{:S(2)}) copy-start(bf16[32,256]{1,0:T(8,128)(2,1)} %param.16) | copy-start | bytes 49156
  0.0 13.8 %copy-start.6 = (bf16[32,64]{1,0:T(8,128)(2,1)S(1)}, bf16[32,64]{1,0:T(8,128)(2,1)}, u32[]{:S(2)}) copy-start(bf16[32,64]{1,0:T(8,128)(2,1)} %param.17) | copy-start | bytes 12292
  2.3 26.3 %collective-permute-start = (bf16[48,2048]{1,0:T(8,128)(2,1)S(1)}, bf16[48,2048]{1,0:T(8,128)(2,1)}, u32[]{:S(2)}, u32[]{:S(2)}) collective-permute-start(bf16[48,2048]{1,0:T(8,128)(2,1)S(1)} %get-tuple-element.52), channel_id=1, source_target_pairs={{0,2},{2,4},{4,6},{6,0},{1,3},{3,5},{5,7},{7,1},{8,10},{10,12},{12... | collective-permute-start | bytes 589832 | tf_op jit(solution)/shard_map/ppermute | solution.py:56
  5.8 23.8 %collective-permute-start.1 = (bf16[48,2048]{1,0:T(8,128)(2,1)S(1)}, bf16[48,2048]{1,0:T(8,128)(2,1)}, u32[]{:S(2)}, u32[]{:S(2)}) collective-permute-start(bf16[48,2048]{1,0:T(8,128)(2,1)S(1)} %get-tuple-element.52), channel_id=1, source_target_pairs={{0,4},{2,6},{4,0},{6,2},{1,5},{3,7},{5,1},{7,3},{8,12},{10,14},{12... | collective-permute-start | bytes 589832 | tf_op jit(solution)/shard_map/ppermute | solution.py:56
  10.4 20.1 %collective-permute-start.2 = (bf16[48,2048]{1,0:T(8,128)(2,1)S(1)}, bf16[48,2048]{1,0:T(8,128)(2,1)S(1)}, u32[]{:S(2)}, u32[]{:S(2)}) collective-permute-start(bf16[48,2048]{1,0:T(8,128)(2,1)S(1)} %get-tuple-element.52), channel_id=1, source_target_pairs={{0,6},{2,0},{4,2},{6,4},{1,7},{3,1},{5,3},{7,5},{8,14},{10,8},{12,... | collective-permute-start | bytes 589832 | tf_op jit(solution)/shard_map/ppermute | solution.py:56
  15.1 12.7 %copy-start.3 = (bf16[2048,64]{0,1:T(8,128)(2,1)S(1)}, bf16[2048,64]{0,1:T(8,128)(2,1)}, u32[]{:S(2)}) copy-start(bf16[2048,64]{0,1:T(8,128)(2,1)} %param.23) | copy-start | bytes 786436
  15.1 13.0 %copy-start.4 = (bf16[2048,64]{0,1:T(8,128)(2,1)S(1)}, bf16[2048,64]{0,1:T(8,128)(2,1)}, u32[]{:S(2)}) copy-start(bf16[2048,64]{0,1:T(8,128)(2,1)} %param.24) | copy-start | bytes 786436
  15.1 44.5 %all-to-all-start = ((bf16[64,80,128]{2,1,0:T(8,128)(2,1)}), bf16[64,80,128]{2,1,0:T(8,128)(2,1)}, u32[]{:S(2)}, u32[]{:S(2)}) async-start(bf16[64,80,128]{2,1,0:T(8,128)(2,1)} %broadcast_in_dim.65), calls=%async_computation | async-start | bytes 2621440 | tf_op jit(solution)/shard_map/all_to_all | solution.py:42
  30.6 4.2 %collective-permute-start.3 = (bf16[4,48,2048]{2,1,0:T(8,128)(2,1)S(1)}, bf16[4,48,2048]{2,1,0:T(8,128)(2,1)S(1)}, u32[]{:S(2)}, u32[]{:S(2)}) collective-permute-start(bf16[4,48,2048]{2,1,0:T(8,128)(2,1)S(1)} %bitcast_dynamic-update-slice_fusion.6), channel_id=1, source_target_pairs={{0,1},{1,0},{2,3},{3,2},{4,5},{5,4},{6,7},{7,6},{8,9},{9,8},{10,11... | collective-permute-start | bytes 2359304 | tf_op jit(solution)/shard_map/ppermute | solution.py:51
  34.8 1.0 copy-start.8
  36.6 27.1 %collective-permute-start.4 = (bf16[128,128]{1,0:T(8,128)(2,1)S(1)}, bf16[128,128]{1,0:T(8,128)(2,1)S(1)}, u32[]{:S(2)}, u32[]{:S(2)}) collective-permute-start(bf16[128,128]{1,0:T(8,128)(2,1)S(1)} %slice.203), channel_id=1, source_target_pairs={{0,8},{8,16},{16,24},{24,32},{32,40},{40,48},{48,56},{56,64},{64,7... | collective-permute-start | bytes 98312 | tf_op jit(solution)/shard_map/ppermute | solution.py:392
  60.9 0.7 copy-start.7
  63.3 9.8 %copy-start.1 = (f32[16]{0:T(128)S(1)}, f32[16]{0:T(128)}, u32[]{:S(2)}) copy-start(f32[16]{0:T(128)} %sink_ref.1) | copy-start | bytes 196
  64.7 32.7 %all-to-all-start.1 = ((bf16[32,120,128]{2,1,0:T(8,128)(2,1)}), bf16[32,120,128]{2,1,0:T(8,128)(2,1)S(1)}, u32[]{:S(2)}, u32[]{:S(2)}) async-start(bf16[32,120,128]{2,1,0:T(8,128)(2,1)} %broadcast_in_dim.75), calls=%async_computation.1 | async-start | bytes 1966080 | tf_op jit(solution)/shard_map/all_to_all | solution.py:42
  74.7 15.9 %collective-permute-start.5 = (bf16[384,384]{1,0:T(8,128)(2,1)S(1)}, bf16[384,384]{1,0:T(8,128)(2,1)S(1)}, u32[]{:S(2)}, u32[]{:S(2)}) collective-permute-start(bf16[384,384]{1,0:T(8,128)(2,1)S(1)} %windowed.1), channel_id=1, source_target_pairs={{0,2},{2,4},{4,6},{6,0},{1,3},{3,5},{5,7},{7,1},{8,10},{10,12},{12... | collective-permute-start | bytes 884744 | tf_op jit(solution)/shard_map/ppermute | solution.py:56
  77.2 13.4 %collective-permute-start.6 = (bf16[384,384]{1,0:T(8,128)(2,1)S(1)}, bf16[384,384]{1,0:T(8,128)(2,1)S(1)}, u32[]{:S(2)}, u32[]{:S(2)}) collective-permute-start(bf16[384,384]{1,0:T(8,128)(2,1)S(1)} %windowed.1), channel_id=1, source_target_pairs={{0,4},{2,6},{4,0},{6,2},{1,5},{3,7},{5,1},{7,3},{8,12},{10,14},{12... | collective-permute-start | bytes 884744 | tf_op jit(solution)/shard_map/ppermute | solution.py:56
  80.4 12.7 %collective-permute-start.7 = (bf16[384,384]{1,0:T(8,128)(2,1)S(1)}, bf16[384,384]{1,0:T(8,128)(2,1)S(1)}, u32[]{:S(2)}, u32[]{:S(2)}) collective-permute-start(bf16[384,384]{1,0:T(8,128)(2,1)S(1)} %windowed.1), channel_id=1, source_target_pairs={{0,6},{2,0},{4,2},{6,4},{1,7},{3,1},{5,3},{7,5},{8,14},{10,8},{12,... | collective-permute-start | bytes 884744 | tf_op jit(solution)/shard_map/ppermute | solution.py:56
  97.5 17.1 %collective-permute-start.8 = (bf16[16,120,128]{2,1,0:T(8,128)(2,1)S(1)}, bf16[16,120,128]{2,1,0:T(8,128)(2,1)S(1)}, u32[]{:S(2)}, u32[]{:S(2)}) collective-permute-start(bf16[16,120,128]{2,1,0:T(8,128)(2,1)S(1)} %get-tuple-element.58), channel_id=1, source_target_pairs={{0,8},{8,16},{16,24},{24,32},{32,40},{40,48},{48,56},{56,0},{1,9},... | collective-permute-start | bytes 1474568 | tf_op jit(solution)/shard_map/ppermute | solution.py:61
  104.1 14.4 %collective-permute-start.9 = (bf16[16,120,128]{2,1,0:T(8,128)(2,1)S(1)}, bf16[16,120,128]{2,1,0:T(8,128)(2,1)S(1)}, u32[]{:S(2)}, u32[]{:S(2)}) collective-permute-start(bf16[16,120,128]{2,1,0:T(8,128)(2,1)S(1)} %get-tuple-element.57), channel_id=1, source_target_pairs={{0,56},{8,0},{16,8},{24,16},{32,24},{40,32},{48,40},{56,48},{1,57}... | collective-permute-start | bytes 1474568 | tf_op jit(solution)/shard_map/ppermute | solution.py:61
  106.1 24.4 %collective-permute-start.11 = (bf16[32,120,128]{2,1,0:T(8,128)(2,1)S(1)}, bf16[32,120,128]{2,1,0:T(8,128)(2,1)}, u32[]{:S(2)}, u32[]{:S(2)}) collective-permute-start(bf16[32,120,128]{2,1,0:T(8,128)(2,1)S(1)} %all-to-all-done.1.refs_0_), channel_id=1, source_target_pairs={{0,1},{1,0},{2,3},{3,2},{4,5},{5,4},{6,7},{7,6},{8,9},{9,8},{10,11... | collective-permute-start | bytes 2949128 | tf_op jit(solution)/shard_map/ppermute | solution.py:51
  108.0 13.5 %collective-permute-start.12 = (bf16[4,384,128]{2,1,0:T(8,128)(2,1)}, bf16[4,384,128]{2,1,0:T(8,128)(2,1)}, u32[]{:S(2)}, u32[]{:S(2)}) collective-permute-start(bf16[4,384,128]{2,1,0:T(8,128)(2,1)} %slice.208), channel_id=1, source_target_pairs={{0,1},{1,0},{2,3},{3,2},{4,5},{5,4},{6,7},{7,6},{8,9},{9,8},{10,11... | collective-permute-start | bytes 1179656 | tf_op jit(solution)/shard_map/ppermute | solution.py:51
  119.6 18.1 %collective-permute-start.10 = (bf16[32,120,128]{2,1,0:T(8,128)(2,1)}, bf16[32,120,128]{2,1,0:T(8,128)(2,1)}, u32[]{:S(2)}, u32[]{:S(2)}) collective-permute-start(bf16[32,120,128]{2,1,0:T(8,128)(2,1)} %joined.1.refs_0_), channel_id=1, source_target_pairs={{0,1},{1,0},{2,3},{3,2},{4,5},{5,4},{6,7},{7,6},{8,9},{9,8},{10,11... | collective-permute-start | bytes 2949128 | tf_op jit(solution)/shard_map/ppermute | solution.py:51
  152.8 17.2 %all-to-all-start.2 = ((bf16[4,272,384]{2,1,0:T(8,128)(2,1)}), bf16[4,272,384]{2,1,0:T(8,128)(2,1)S(1)}, u32[]{:S(2)}, u32[]{:S(2)}) async-start(bf16[4,272,384]{2,1,0:T(8,128)(2,1)} %shard_map.138), calls=%async_computation.2 | async-start | bytes 1671168 | tf_op jit(solution)/shard_map/all_to_all | solution.py:42
  172.5 16.6 %all-to-all-start.3 = ((bf16[8,384,128]{2,1,0:T(8,128)(2,1)}), bf16[8,384,128]{2,1,0:T(8,128)(2,1)S(1)}, u32[]{:S(2)}, u32[]{:S(2)}) async-start(bf16[8,384,128]{2,1,0:T(8,128)(2,1)} %broadcast_in_dim.81), calls=%async_computation.3 | async-start | bytes 1572864 | tf_op jit(solution)/shard_map/all_to_all | solution.py:42
  177.1 13.4 %copy-start.2 = (f32[384,256]{1,0:T(8,128)S(1)}, f32[384,256]{1,0:T(8,128)}, u32[]{:S(2)}) copy-start(f32[384,256]{1,0:T(8,128)} %fusion.22) | copy-start | bytes 1179652

commit v6 on v5

--- a/solution.py
+++ b/solution.py
@@ -275,15 +275,16 @@
     )(low, high)
 
 
-def windowed_body(where_ref, sink_ref, rows_ref, before_ref, query_ref, out_ref):
+def windowed_body(where_ref, sink_ref, q_ref, kv_ref, before_ref, query_ref, out_ref):
     out_ref[:, : 2 * LANES] = query_ref[...]
     for tile in range(ROWS // WINDOW):
-        here = rows_ref[tile * WINDOW : (tile + 1) * WINDOW]
+        q = q_ref[tile * WINDOW : (tile + 1) * WINDOW]
+        here = kv_ref[tile * WINDOW : (tile + 1) * WINDOW]
         if tile == 0:
             behind = before_ref[...]
         else:
-            behind = rows_ref[(tile - 1) * WINDOW : tile * WINDOW, LANES:]
-        both = jnp.concatenate([behind, here[:, LANES:]], axis=0)
+            behind = kv_ref[(tile - 1) * WINDOW : tile * WINDOW]
+        both = jnp.concatenate([behind, here], axis=0)
         row = lax.broadcasted_iota(jnp.int32, (WINDOW, 2 * WINDOW), 0)
         col = lax.broadcasted_iota(jnp.int32, (WINDOW, 2 * WINDOW), 1)
         allowed = (col > row) & (col <= row + WINDOW)
@@ -292,7 +293,7 @@
         outs = []
         for h in range(LANES // HEAD):
             scores = lax.dot_general(
-                here[:, h * HEAD : (h + 1) * HEAD],
+                q[:, h * HEAD : (h + 1) * HEAD],
                 both[:, :HEAD],
                 (((1,), (1,)), ((), ())),
                 preferred_element_type=jnp.float32,
@@ -309,13 +310,13 @@
         ).astype(jnp.bfloat16)
 
 
-def windowed(where, sink_logits, rows, before, query):
+def windowed(where, sink_logits, q, kv, before, query):
     smem = pl.BlockSpec(memory_space=pltpu.SMEM)
     vmem = pl.BlockSpec(memory_space=pltpu.VMEM)
     return pl.pallas_call(
         windowed_body,
         out_shape=jax.ShapeDtypeStruct((ROWS, 3 * LANES), jnp.bfloat16),
-        in_specs=[smem, smem, vmem, vmem, vmem],
+        in_specs=[smem, smem, vmem, vmem, vmem, vmem],
         out_specs=vmem,
         compiler_params=pltpu.CompilerParams(vmem_limit_bytes=16 * 1024 * 1024),
         cost_estimate=pl.CostEstimate(
@@ -324,7 +325,7 @@
             bytes_accessed=1000000,
         ),
         name="windowed",
-    )(where, sink_logits, rows, before, query)
+    )(where, sink_logits, q, kv, before, query)
 
 
 def layer(
@@ -362,51 +363,54 @@
             placed = lax.dynamic_update_index_in_dim(placed, value, at, 0)
         return placed
 
-    half = rope_down.shape[0] // 2
-    down = jnp.concatenate(
+    def by_core(values):
+        return tuple(
+            lax.dynamic_index_in_dim(values, rank, 0, keepdims=False)
+            for rank in (c_rank, 1 - c_rank)
+        )
+
+    def by_core(values):
+        return tuple(
+            lax.dynamic_index_in_dim(values, rank, 0, keepdims=False)
+            for rank in (c_rank, 1 - c_rank)
+        )
+
+    down = jnp.concatenate([latent_down, rope_down], axis=1)
+    width = down.shape[1] // x_count
+    down = lax.dynamic_slice_in_dim(down, x_rank * width, width, 1)
+    rest = LANES - width
+    low, high = (down[:16], down[16:])
+    bottom = jnp.concatenate([high[:8, rest:], high[8:, rest:]], axis=1)
+    bottom = jnp.pad(bottom, ((0, 0), (0, LANES - bottom.shape[1])))
+    down = jnp.concatenate([jnp.concatenate([low, high[:, :rest]], axis=1), bottom], axis=0)
+    down = to_everyone(down, SP)
+    left = width - rest
+    ends = jnp.concatenate([down[:, 16:, :left], down[:, 16:, left : 2 * left]], axis=1)
+    high = jnp.concatenate([down[:, :16, width:], ends], axis=2)
+    down = jnp.stack([down[:, :16, :width], high], axis=1).reshape(-1, width)
+
+    normed = norm_rows(inputs, norm_gain)
+    kv_weights = jnp.concatenate([swa_key, swa_value], axis=1)
+    mine = by_x(normed)
+    mine = lax.optimization_barrier(mine)
+    kv_weights_other = from_core(kv_weights)
+
+    latent = jnp.dot(mine.reshape(-1, mine.shape[2]), down, preferred_element_type=jnp.float32)
+    latent = latent.astype(jnp.bfloat16).reshape(x_count, own_rows, width)
+    latent = exchange(latent, "x")
+    tail_rows = mine[x_count // 2 :].reshape(2 * own_rows, -1)
+    tail = jnp.concatenate(
         [
-            latent_down[:, :LANES],
-            latent_down[:, LANES:],
-            jnp.concatenate([rope_down[:half], rope_down[half:]], axis=1),
-        ],
-        axis=0,
-    )
-    down = to_everyone(down, SP)
-    rope_tiles = down[:, 4 * half :]
-    down_rope = jnp.stack([rope_tiles[:, :, :ROPE], rope_tiles[:, :, ROPE:]], axis=1)
-    down_rope = down_rope.reshape(-1, ROPE)
-    down_latent = jnp.concatenate([down[:, : 2 * half], down[:, 2 * half : 4 * half]], axis=2)
-    down_latent = down_latent.reshape(-1, KV_RANK)
-
-    normed = norm_rows(inputs, norm_gain)
-    swa_weights = jnp.concatenate([swa_query, swa_key, swa_value], axis=1)
-    mine = by_x(normed)
-    other = from_core(mine)
-    pieces = jnp.zeros((x_count, 2, *mine.shape[1:]), jnp.bfloat16)
-    pieces = lax.dynamic_update_index_in_dim(pieces, mine, c_rank, 1)
-    pieces = lax.dynamic_update_index_in_dim(pieces, other, 1 - c_rank, 1)
-    pieces = pieces.reshape(ROWS, -1)
-    swa_rows = jnp.dot(pieces, swa_weights, preferred_element_type=jnp.float32)
-    swa_rows = swa_rows.astype(jnp.bfloat16)
-    count = lax.axis_size(SP)
-    before = lax.ppermute(
-        swa_rows[ROWS - WINDOW :, LANES:], SP, [(i, i + 1) for i in range(count - 1)]
-    )
-    queries = jnp.dot(pieces, mla_query, preferred_element_type=jnp.float32)
-    queries = queries.astype(jnp.bfloat16)
-    query = jnp.concatenate(
-        [
-            queries[:, :NOPE],
-            rotate(queries[:, NOPE:], block_pos),
-            jnp.zeros((ROWS, LANES - ROPE), jnp.bfloat16),
+            jnp.dot(tail_rows, weights, preferred_element_type=jnp.float32)
+            for weights in (kv_weights, kv_weights_other)
         ],
         axis=1,
-    )
-
-    latent = jnp.dot(normed, down_latent, preferred_element_type=jnp.float32)
-    rope_raw = jnp.dot(normed, down_rope, preferred_element_type=jnp.float32)
-    keys_latent = norm_rows(latent.astype(jnp.bfloat16), latent_gain)
-    keys_rope = rotate(rope_raw.astype(jnp.bfloat16), own_pos)
+    ).astype(jnp.bfloat16)
+    count = lax.axis_size(SP)
+    before = lax.ppermute(tail, SP, [(i, i + 1) for i in range(count - 1)])
+    latent = jnp.transpose(latent, (1, 0, 2)).reshape(own_rows, KV_RANK + ROPE)
+    keys_latent = norm_rows(latent[:, :KV_RANK], latent_gain)
+    keys_rope = rotate(latent[:, KV_RANK:], own_pos)
     packed = jnp.concatenate(
         [
             keys_latent[:, :LANES],
@@ -428,18 +432,35 @@
             (block, 1 - parity, tp_rank, rank_other),
         )
     ]
-    packed, swa_rows, before, query, up_heads, where = lax.optimization_barrier(
-        (packed, swa_rows, before, query, up_heads, where)
+    packed, mine, before, where = lax.optimization_barrier((packed, mine, before, where))
+    keys_own = to_everyone(packed, SAME_PARITY)
+
+    other = from_core(mine)
+    pieces = jnp.zeros((x_count, 2, *mine.shape[1:]), jnp.bfloat16)
+    pieces = lax.dynamic_update_index_in_dim(pieces, mine, c_rank, 1)
+    pieces = lax.dynamic_update_index_in_dim(pieces, other, 1 - c_rank, 1)
+    pieces = pieces.reshape(ROWS, -1)
+    before_other = from_core(before[:, LANES:])
+    before_both = jnp.stack([before[:, :LANES], before_other])
+    rows_0, rows_1 = by_core(before_both)
+    before = jnp.concatenate([rows_1[3 * OWN - WINDOW : OWN], rows_0[OWN:], rows_1[OWN:]], axis=0)
+    swa_kv = jnp.dot(pieces, kv_weights, preferred_element_type=jnp.float32)
+    swa_kv = swa_kv.astype(jnp.bfloat16)
+    swa_q = jnp.dot(pieces, swa_query, preferred_element_type=jnp.float32)
+    swa_q = swa_q.astype(jnp.bfloat16)
+    queries = jnp.dot(pieces, mla_query, preferred_element_type=jnp.float32)
+    queries = queries.astype(jnp.bfloat16)
+    query = jnp.concatenate(
+        [
+            queries[:, :NOPE],
+            rotate(queries[:, NOPE:], block_pos),
+            jnp.zeros((ROWS, LANES - ROPE), jnp.bfloat16),
+        ],
+        axis=1,
     )
-    keys_own = to_everyone(packed, SAME_PARITY)
-
-    sent = windowed(where[0], sink_logits, swa_rows, before, query)
+    sent = windowed(where[0], sink_logits, swa_q, swa_kv, before, query)
     sent = by_x(sent)
-    swa_x = sent[:, :, 2 * LANES :]
-    swa_other = from_core(swa_x)
-    keys_own, sent, up_heads, swa_x, where = lax.optimization_barrier(
-        (keys_own, sent, up_heads, swa_x, where)
-    )
+    keys_own, sent, up_heads, where = lax.optimization_barrier((keys_own, sent, up_heads, where))
     half = keys_own.shape[0] // 2
     low = from_y(keys_own[:half], 1)
     high = from_y(keys_own[half:], -1)
@@ -450,6 +471,8 @@
     state = attend(where[1], (keys_other,), q_all, state, False)
     partial = attend(where[2], (far_own, far_other), q_all, state, True)
     parts = exchange(partial, "x")
+    swa_x = lax.optimization_barrier(sent[:, :, 2 * LANES :])
+    swa_other = from_core(swa_x)
     per_head = out_swa.reshape(x_count, 2, 2 * HEAD, -1)
     from_swa = jnp.zeros((ROWS, out_swa.shape[1]), jnp.float32)
     for values, core in ((swa_x, c_rank), (swa_other, 1 - c_rank)):

time: 194 us -> 199 us (1.026)
  the two profiles are of different devices: /device:TPU:320 before, /device:TPU:280 now
where the time goes in v6:
time: 199 us; the launch traced here: 198 us
  starting transfers between devices  84.4 us (42%)
  waiting for transfers between devices  48.8 us (25%)
  Pallas kernels  32.3 us (16%)
  matrix products  16.5 us (8%)
  local copies, waits for them, and re-layouts  9.44 us (5%)
  other arithmetic  5.49 us (3%)
    all_to_all x5, starting transfers between devices, exchange(): return lax.all_to_all(array, axis, split_axis=0, concat_axis=0, tiled=True)  36.7 us
    all_to_all x5, waiting for transfers between devices, exchange(): return lax.all_to_all(array, axis, split_axis=0, concat_axis=0, tiled=True)  29.7 us
    pallas_call x3, Pallas kernels, attend(): pl.pallas_call(functools.partial(attend_body, n_parts=len(parts), first=f...  29.6 us
    ppermute x6, starting transfers between devices, from_x(): lax.ppermute(value, 'x', [(i, (i + step) % count) for i in range(count)])  23 us
    ppermute x6, starting transfers between devices, from_core(): return lax.ppermute(value, 'c', [(0, 1), (1, 0)])  12.5 us
    ppermute x2, waiting for transfers between devices, from_y(): lax.ppermute(value, Y, [(i, (i + step) % count) for i in range(count)])  10.7 us
    dot_general x8, matrix products, layer(): jnp.dot(values[x], weights[x], preferred_element_type=jnp.float32)  10.2 us
    ppermute x2, starting transfers between devices, from_y(): lax.ppermute(value, Y, [(i, (i + step) % count) for i in range(count)])  9.43 us
  transfers between devices with their start and end apart: 20, of which 8 were waited for; matrix products, arithmetic and copies ran while one was open for 12% of the time, Pallas kernels for 16%

profile of v6, /device:TPU:280, one launch (start us, length us, event | category | flops | bytes accessed | tf_op | source)
XLA Modules:
  0.0 197.8 jit_solution(13597167696120661154)
XLA Ops:
  0.0 1.2 fusion.6
  1.3 1.7 bitcast_dynamic-update-slice_fusion.9
  3.1 3.4 %collective-permute-start = (bf16[48,2048]{1,0:T(8,128)(2,1)}, bf16[48,2048]{1,0:T(8,128)(2,1)}, u32[]{:S(2)}, u32[]{:S(2)}) collective-permute-start(bf16[48,2048]{1,0:T(8,128)(2,1)} %get-tuple-element.46), channel_id=1, source_target_pairs={{0,2},{2,4},{4,6},{6,0},{1,3},{3,5},{5,7},{7,1},{8,10},{10,12},{12... | collective-permute-start | bytes 589832 | tf_op jit(solution)/shard_map/ppermute | solution.py:56
  6.5 4.6 %collective-permute-start.1 = (bf16[48,2048]{1,0:T(8,128)(2,1)}, bf16[48,2048]{1,0:T(8,128)(2,1)S(1)}, u32[]{:S(2)}, u32[]{:S(2)}) collective-permute-start(bf16[48,2048]{1,0:T(8,128)(2,1)} %get-tuple-element.46), channel_id=1, source_target_pairs={{0,4},{2,6},{4,0},{6,2},{1,5},{3,7},{5,1},{7,3},{8,12},{10,14},{12... | collective-permute-start | bytes 589832 | tf_op jit(solution)/shard_map/ppermute | solution.py:56
  11.1 3.3 %collective-permute-start.2 = (bf16[48,2048]{1,0:T(8,128)(2,1)}, bf16[48,2048]{1,0:T(8,128)(2,1)S(1)}, u32[]{:S(2)}, u32[]{:S(2)}) collective-permute-start(bf16[48,2048]{1,0:T(8,128)(2,1)} %get-tuple-element.46), channel_id=1, source_target_pairs={{0,6},{2,0},{4,2},{6,4},{1,7},{3,1},{5,3},{7,5},{8,14},{10,8},{12,... | collective-permute-start | bytes 589832 | tf_op jit(solution)/shard_map/ppermute | solution.py:56
  14.5 1.9 collective-permute-start.3
  17.6 12.8 %all-to-all-start = ((bf16[64,24,128]{2,1,0:T(8,128)(2,1)}), bf16[64,24,128]{2,1,0:T(8,128)(2,1)S(1)}, u32[]{:S(2)}, u32[]{:S(2)}) async-start(bf16[64,24,128]{2,1,0:T(8,128)(2,1)} %broadcast_in_dim.70), calls=%async_computation | async-start | bytes 786432 | tf_op jit(solution)/shard_map/all_to_all | solution.py:42
  33.3 1.3 convolution_convert_fusion.5
  34.6 7.5 %all-to-all-done = bf16[64,24,128]{2,1,0:T(8,128)(2,1)S(1)} async-done(((bf16[64,24,128]{2,1,0:T(8,128)(2,1)}), bf16[64,24,128]{2,1,0:T(8,128)(2,1)S(1)}, u32[]{:S(2)}, u32[]{:S(2)}) %all-to-all-start) | async-done | bytes 393248 | tf_op jit(solution)/shard_map/all_to_all | solution.py:42
  43.8 3.3 %all-to-all-start.1 = ((bf16[4,48,80]{2,1,0:T(8,128)(2,1)}), bf16[4,48,80]{2,1,0:T(8,128)(2,1)S(1)}, u32[]{:S(2)}, u32[]{:S(2)}) async-start(bf16[4,48,80]{2,1,0:T(8,128)(2,1)} %bitcast.9), calls=%async_computation.1 | async-start | bytes 98304 | tf_op jit(solution)/shard_map/all_to_all | solution.py:42
  47.1 2.7 %collective-permute-start.4 = (bf16[96,256]{1,0:T(8,128)(2,1)S(1)}, bf16[96,256]{1,0:T(8,128)(2,1)S(1)}, u32[]{:S(2)}, u32[]{:S(2)}) collective-permute-start(bf16[96,256]{1,0:T(8,128)(2,1)S(1)} %pad_maximum_fusion.2), channel_id=1, source_target_pairs={{0,8},{8,16},{16,24},{24,32},{32,40},{40,48},{48,56},{56,64},{64,7... | collective-permute-start | bytes 147464 | tf_op jit(solution)/shard_map/ppermute | solution.py:410
  49.8 2.8 %all-to-all-done.1 = bf16[4,48,80]{2,1,0:T(8,128)(2,1)S(1)} async-done(((bf16[4,48,80]{2,1,0:T(8,128)(2,1)}), bf16[4,48,80]{2,1,0:T(8,128)(2,1)S(1)}, u32[]{:S(2)}, u32[]{:S(2)}) %all-to-all-start.1) | async-done | bytes 30752 | tf_op jit(solution)/shard_map/all_to_all | solution.py:42
  53.3 1.9 collective-permute-start.5
  55.3 2.4 %collective-permute-start.6 = (bf16[96,128]{1,0:T(8,128)(2,1)S(1)}, bf16[96,128]{1,0:T(8,128)(2,1)S(1)}, u32[]{:S(2)}, u32[]{:S(2)}) collective-permute-start(bf16[96,128]{1,0:T(8,128)(2,1)S(1)} %get-tuple-element.60), channel_id=1, source_target_pairs={{0,1},{1,0},{2,3},{3,2},{4,5},{5,4},{6,7},{7,6},{8,9},{9,8},{10,11... | collective-permute-start | bytes 73736 | tf_op jit(solution)/shard_map/ppermute | solution.py:51
  57.7 1.1 broadcast_in_dim.71
  58.7 10.4 %all-to-all-start.2 = ((bf16[32,120,128]{2,1,0:T(8,128)(2,1)}), bf16[32,120,128]{2,1,0:T(8,128)(2,1)S(1)}, u32[]{:S(2)}, u32[]{:S(2)}) async-start(bf16[32,120,128]{2,1,0:T(8,128)(2,1)} %broadcast_in_dim.71), calls=%async_computation.2 | async-start | bytes 1966080 | tf_op jit(solution)/shard_map/all_to_all | solution.py:42
  69.5 1.2 bitcast_dynamic-update-slice_fusion.1
  74.0 1.6 windowed.1
  75.6 3.7 %collective-permute-start.7 = (bf16[384,384]{1,0:T(8,128)(2,1)S(1)}, bf16[384,384]{1,0:T(8,128)(2,1)S(1)}, u32[]{:S(2)}, u32[]{:S(2)}) collective-permute-start(bf16[384,384]{1,0:T(8,128)(2,1)S(1)} %windowed.1), channel_id=1, source_target_pairs={{0,2},{2,4},{4,6},{6,0},{1,3},{3,5},{5,7},{7,1},{8,10},{10,12},{12... | collective-permute-start | bytes 884744 | tf_op jit(solution)/shard_map/ppermute | solution.py:56
  79.4 4.6 %collective-permute-start.8 = (bf16[384,384]{1,0:T(8,128)(2,1)S(1)}, bf16[384,384]{1,0:T(8,128)(2,1)S(1)}, u32[]{:S(2)}, u32[]{:S(2)}) collective-permute-start(bf16[384,384]{1,0:T(8,128)(2,1)S(1)} %windowed.1), channel_id=1, source_target_pairs={{0,4},{2,6},{4,0},{6,2},{1,5},{3,7},{5,1},{7,3},{8,12},{10,14},{12... | collective-permute-start | bytes 884744 | tf_op jit(solution)/shard_map/ppermute | solution.py:56
  84.0 3.4 %collective-permute-start.9 = (bf16[384,384]{1,0:T(8,128)(2,1)S(1)}, bf16[384,384]{1,0:T(8,128)(2,1)S(1)}, u32[]{:S(2)}, u32[]{:S(2)}) collective-permute-start(bf16[384,384]{1,0:T(8,128)(2,1)S(1)} %windowed.1), channel_id=1, source_target_pairs={{0,6},{2,0},{4,2},{6,4},{1,7},{3,1},{5,3},{7,5},{8,14},{10,8},{12,... | collective-permute-start | bytes 884744 | tf_op jit(solution)/shard_map/ppermute | solution.py:56
  87.6 7.1 %collective-permute-done.8 = bf16[384,384]{1,0:T(8,128)(2,1)S(1)} collective-permute-done((bf16[384,384]{1,0:T(8,128)(2,1)S(1)}, bf16[384,384]{1,0:T(8,128)(2,1)S(1)}, u32[]{:S(2)}, u32[]{:S(2)}) %collective-permute-start.8) | collective-permute-done | bytes 294944 | tf_op jit(solution)/shard_map/ppermute | solution.py:56
  94.7 1.3 collective-permute-done.9
  96.2 7.5 %collective-permute-start.10 = (bf16[16,120,128]{2,1,0:T(8,128)(2,1)S(1)}, bf16[16,120,128]{2,1,0:T(8,128)(2,1)S(1)}, u32[]{:S(2)}, u32[]{:S(2)}) collective-permute-start(bf16[16,120,128]{2,1,0:T(8,128)(2,1)S(1)} %get-tuple-element.48), channel_id=1, source_target_pairs={{0,8},{8,16},{16,24},{24,32},{32,40},{40,48},{48,56},{56,0},{1,9},... | collective-permute-start | bytes 1474568 | tf_op jit(solution)/shard_map/ppermute | solution.py:61
  103.7 1.9 collective-permute-start.11
  105.6 1.9 collective-permute-start.13
  107.5 5.3 %collective-permute-done.10.low_ref = bf16[16,120,128]{2,1,0:T(8,128)(2,1)S(1)} collective-permute-done((bf16[16,120,128]{2,1,0:T(8,128)(2,1)S(1)}, bf16[16,120,128]{2,1,0:T(8,128)(2,1)S(1)}, u32[]{:S(2)}, u32[]{:S(2)}) %collective-permute-start.10) | collective-permute-done | bytes 491552 | tf_op jit(solution)/shard_map/ppermute | solution.py:61
  112.9 5.3 %collective-permute-done.11.high_ref = bf16[16,120,128]{2,1,0:T(8,128)(2,1)S(1)} collective-permute-done((bf16[16,120,128]{2,1,0:T(8,128)(2,1)S(1)}, bf16[16,120,128]{2,1,0:T(8,128)(2,1)S(1)}, u32[]{:S(2)}, u32[]{:S(2)}) %collective-permute-start.11) | collective-permute-done | bytes 491552 | tf_op jit(solution)/shard_map/ppermute | solution.py:61
  118.2 1.0 joined.1.refs_0_
  119.2 1.9 collective-permute-start.12
  122.0 2.4 %collective-permute-start.14 = (bf16[4,384,128]{2,1,0:T(8,128)(2,1)}, bf16[4,384,128]{2,1,0:T(8,128)(2,1)}, u32[]{:S(2)}, u32[]{:S(2)}) collective-permute-start(bf16[4,384,128]{2,1,0:T(8,128)(2,1)} %slice.217), channel_id=1, source_target_pairs={{0,1},{1,0},{2,3},{3,2},{4,5},{5,4},{6,7},{7,6},{8,9},{9,8},{10,11... | collective-permute-start | bytes 1179656 | tf_op jit(solution)/shard_map/ppermute | solution.py:51
  124.4 1.8 fusion.20
  126.2 7.2 %shard_map.136 = (f32[3,256,512]{2,1,0:T(8,128)S(1)}, f32[3,1,512]{2,1,0:T(1,128)S(1)}, f32[3,1,512]{2,1,0:T(1,128)S(1)}, bf16[1536,384]{1,0:T(8,128)(2,1)S(1)}) custom-call(s32[3]{0:T(128)S(1)} %get-tuple-element.32.where_ref, bf16[32,120,128]{2,1,0:T(8,128)(2,1)S(1)} %all-to-all-done.2.refs_0_, ...), custom_call_target="tpu_custom_call" | custom-call | flops 3019898880 | bytes 6000000 | tf_op jit(solution)/shard_map/pallas_call | solution.py:245
  133.4 7.3 %shard_map.137 = (f32[3,256,512]{2,1,0:T(8,128)S(1)}, f32[3,1,512]{2,1,0:T(1,128)S(1)}, f32[3,1,512]{2,1,0:T(1,128)S(1)}) custom-call(s32[3]{0:T(128)S(1)} %get-tuple-element.36.where_ref, bf16[32,120,128]{2,1,0:T(8,128)(2,1)} %collective-permute-done.13.refs_0_, bf16[1536,384]{1,0:T(8,128)(2,1)S(1)} %get-tuple-element.35.refs_1_.refs_2_, ...), custom_call_target="tpu_custom_call" | custom-call | flops 3019898880 | bytes 6000000 | tf_op jit(solution)/shard_map/pallas_call | solution.py:245
  140.7 15.2 %shard_map.138 = bf16[4,272,384]{2,1,0:T(8,128)(2,1)} custom-call(s32[4]{0:T(128)S(1)} %pad_add_fusion.3.where_ref, bf16[32,120,128]{2,1,0:T(8,128)(2,1)} %joined.1.refs_0_, bf16[32,120,128]{2,1,0:T(8,128)(2,1)} %collective-permute-done.12.refs_1_, bf16[1536,384]{1,0:T(8,128)(2,1)S(1)} %get-tuple-element.35.refs_1_.refs_2_, ...), custom_call_target="tpu_custom_call" | custom-call | flops 6039797760 | bytes 6000000 | tf_op jit(solution)/shard_map/pallas_call | solution.py:245
  155.9 6.7 %all-to-all-start.3 = ((bf16[4,272,384]{2,1,0:T(8,128)(2,1)}), bf16[4,272,384]{2,1,0:T(8,128)(2,1)S(1)}, u32[]{:S(2)}, u32[]{:S(2)}) async-start(bf16[4,272,384]{2,1,0:T(8,128)(2,1)} %shard_map.138), calls=%async_computation.3 | async-start | bytes 1671168 | tf_op jit(solution)/shard_map/all_to_all | solution.py:42
  162.6 1.1 convolution_add_fusion.3
  163.7 1.1 convolution_add_fusion.2
  164.8 1.1 convolution_add_fusion.1
  165.9 9.7 %all-to-all-done.3 = bf16[4,272,384]{2,1,0:T(8,128)(2,1)S(1)} async-done(((bf16[4,272,384]{2,1,0:T(8,128)(2,1)}), bf16[4,272,384]{2,1,0:T(8,128)(2,1)S(1)}, u32[]{:S(2)}, u32[]{:S(2)}) %all-to-all-start.3) | async-done | bytes 835616 | tf_op jit(solution)/shard_map/all_to_all | solution.py:42
  175.9 1.1 convolution_convert_fusion.3
  178.0 3.5 %all-to-all-start.4 = ((bf16[8,384,128]{2,1,0:T(8,128)(2,1)}), bf16[8,384,128]{2,1,0:T(8,128)(2,1)S(1)}, u32[]{:S(2)}, u32[]{:S(2)}) async-start(bf16[8,384,128]{2,1,0:T(8,128)(2,1)} %broadcast_in_dim.81), calls=%async_computation.4 | async-start | bytes 1572864 | tf_op jit(solution)/shard_map/all_to_all | solution.py:42
  181.6 1.1 fusion.17
  182.6 1.1 fusion.18
  183.7 1.1 fusion.19
  184.8 9.8 %all-to-all-done.4 = bf16[8,384,128]{2,1,0:T(8,128)(2,1)S(1)} async-done(((bf16[8,384,128]{2,1,0:T(8,128)(2,1)}), bf16[8,384,128]{2,1,0:T(8,128)(2,1)S(1)}, u32[]{:S(2)}, u32[]{:S(2)}) %all-to-all-start.4) | async-done | bytes 786464 | tf_op jit(solution)/shard_map/all_to_all | solution.py:42
  194.6 1.4 convolution_bitcast_fusion
  196.0 1.8 fusion.5
  (111 shorter events, 12.2 us)
Async XLA Ops:
  0.0 70.7 %copy-start = (bf16[2048,192]{0,1:T(8,128)(2,1)S(1)}, bf16[2048,192]{0,1:T(8,128)(2,1)}, u32[]{:S(2)}) copy-start(bf16[2048,192]{0,1:T(8,128)(2,1)} %param.19) | copy-start | bytes 2359300
  0.0 14.5 %copy-start.7 = (bf16[2048,64]{0,1:T(8,128)(2,1)S(1)}, bf16[2048,64]{0,1:T(8,128)(2,1)}, u32[]{:S(2)}) copy-start(bf16[2048,64]{0,1:T(8,128)(2,1)} %param.23) | copy-start | bytes 786436
  0.0 14.5 %copy-start.8 = (bf16[2048,64]{0,1:T(8,128)(2,1)S(1)}, bf16[2048,64]{0,1:T(8,128)(2,1)}, u32[]{:S(2)}) copy-start(bf16[2048,64]{0,1:T(8,128)(2,1)} %param.24) | copy-start | bytes 786436
  0.0 16.5 %copy-start.9 = (bf16[32,256]{1,0:T(8,128)(2,1)S(1)}, bf16[32,256]{1,0:T(8,128)(2,1)}, u32[]{:S(2)}) copy-start(bf16[32,256]{1,0:T(8,128)(2,1)} %param.16) | copy-start | bytes 49156
  0.0 16.5 %copy-start.10 = (bf16[32,64]{1,0:T(8,128)(2,1)S(1)}, bf16[32,64]{1,0:T(8,128)(2,1)}, u32[]{:S(2)}) copy-start(bf16[32,64]{1,0:T(8,128)(2,1)} %param.17) | copy-start | bytes 12292
  3.1 28.8 %collective-permute-start = (bf16[48,2048]{1,0:T(8,128)(2,1)}, bf16[48,2048]{1,0:T(8,128)(2,1)}, u32[]{:S(2)}, u32[]{:S(2)}) collective-permute-start(bf16[48,2048]{1,0:T(8,128)(2,1)} %get-tuple-element.46), channel_id=1, source_target_pairs={{0,2},{2,4},{4,6},{6,0},{1,3},{3,5},{5,7},{7,1},{8,10},{10,12},{12... | collective-permute-start | bytes 589832 | tf_op jit(solution)/shard_map/ppermute | solution.py:56
  6.5 26.4 %collective-permute-start.1 = (bf16[48,2048]{1,0:T(8,128)(2,1)}, bf16[48,2048]{1,0:T(8,128)(2,1)S(1)}, u32[]{:S(2)}, u32[]{:S(2)}) collective-permute-start(bf16[48,2048]{1,0:T(8,128)(2,1)} %get-tuple-element.46), channel_id=1, source_target_pairs={{0,4},{2,6},{4,0},{6,2},{1,5},{3,7},{5,1},{7,3},{8,12},{10,14},{12... | collective-permute-start | bytes 589832 | tf_op jit(solution)/shard_map/ppermute | solution.py:56
  11.1 21.8 %collective-permute-start.2 = (bf16[48,2048]{1,0:T(8,128)(2,1)}, bf16[48,2048]{1,0:T(8,128)(2,1)S(1)}, u32[]{:S(2)}, u32[]{:S(2)}) collective-permute-start(bf16[48,2048]{1,0:T(8,128)(2,1)} %get-tuple-element.46), channel_id=1, source_target_pairs={{0,6},{2,0},{4,2},{6,4},{1,7},{3,1},{5,3},{7,5},{8,14},{10,8},{12,... | collective-permute-start | bytes 589832 | tf_op jit(solution)/shard_map/ppermute | solution.py:56
  14.5 18.4 %copy-start.2 = (bf16[2048,128]{0,1:T(8,128)(2,1)}, bf16[2048,128]{0,1:T(8,128)(2,1)S(1)}, u32[]{:S(2)}) copy-start(bf16[2048,128]{0,1:T(8,128)(2,1)S(1)} %constant_dynamic-update-slice_fusion) | copy-start | bytes 1572868
  14.5 18.7 %collective-permute-start.3 = (bf16[2048,128]{0,1:T(8,128)(2,1)S(1)}, bf16[2048,128]{0,1:T(8,128)(2,1)}, u32[]{:S(2)}, u32[]{:S(2)}) collective-permute-start(bf16[2048,128]{0,1:T(8,128)(2,1)S(1)} %constant_dynamic-update-slice_fusion), channel_id=1, source_target_pairs={{0,1},{1,0},{2,3},{3,2},{4,5},{5,4},{6,7},{7,6},{8,9},{9,8},{10,11... | collective-permute-start | bytes 1572872 | tf_op jit(solution)/shard_map/ppermute | solution.py:51
  17.6 24.5 %all-to-all-start = ((bf16[64,24,128]{2,1,0:T(8,128)(2,1)}), bf16[64,24,128]{2,1,0:T(8,128)(2,1)S(1)}, u32[]{:S(2)}, u32[]{:S(2)}) async-start(bf16[64,24,128]{2,1,0:T(8,128)(2,1)} %broadcast_in_dim.70), calls=%async_computation | async-start | bytes 786432 | tf_op jit(solution)/shard_map/all_to_all | solution.py:42
  42.5 10.3 %copy-start.11 = (f32[256]{0:T(256)S(1)}, f32[256]{0:T(256)}, u32[]{:S(2)}) copy-start(f32[256]{0:T(256)} %param.18) | copy-start | bytes 3076
  43.8 8.8 %all-to-all-start.1 = ((bf16[4,48,80]{2,1,0:T(8,128)(2,1)}), bf16[4,48,80]{2,1,0:T(8,128)(2,1)S(1)}, u32[]{:S(2)}, u32[]{:S(2)}) async-start(bf16[4,48,80]{2,1,0:T(8,128)(2,1)} %bitcast.9), calls=%async_computation.1 | async-start | bytes 98304 | tf_op jit(solution)/shard_map/all_to_all | solution.py:42
  47.1 6.2 %collective-permute-start.4 = (bf16[96,256]{1,0:T(8,128)(2,1)S(1)}, bf16[96,256]{1,0:T(8,128)(2,1)S(1)}, u32[]{:S(2)}, u32[]{:S(2)}) collective-permute-start(bf16[96,256]{1,0:T(8,128)(2,1)S(1)} %pad_maximum_fusion.2), channel_id=1, source_target_pairs={{0,8},{8,16},{16,24},{24,32},{32,40},{40,48},{48,56},{56,64},{64,7... | collective-permute-start | bytes 147464 | tf_op jit(solution)/shard_map/ppermute | solution.py:410
  53.3 16.2 %collective-permute-start.5 = (bf16[4,48,2048]{2,1,0:T(8,128)(2,1)S(1)}, bf16[4,48,2048]{2,1,0:T(8,128)(2,1)}, u32[]{:S(2)}, u32[]{:S(2)}) collective-permute-start(bf16[4,48,2048]{2,1,0:T(8,128)(2,1)S(1)} %bitcast_dynamic-update-slice_fusion.6), channel_id=1, source_target_pairs={{0,1},{1,0},{2,3},{3,2},{4,5},{5,4},{6,7},{7,6},{8,9},{9,8},{10,11... | collective-permute-start | bytes 2359304 | tf_op jit(solution)/shard_map/ppermute | solution.py:51
  55.3 14.1 %collective-permute-start.6 = (bf16[96,128]{1,0:T(8,128)(2,1)S(1)}, bf16[96,128]{1,0:T(8,128)(2,1)S(1)}, u32[]{:S(2)}, u32[]{:S(2)}) collective-permute-start(bf16[96,128]{1,0:T(8,128)(2,1)S(1)} %get-tuple-element.60), channel_id=1, source_target_pairs={{0,1},{1,0},{2,3},{3,2},{4,5},{5,4},{6,7},{7,6},{8,9},{9,8},{10,11... | collective-permute-start | bytes 73736 | tf_op jit(solution)/shard_map/ppermute | solution.py:51
  58.7 37.3 %all-to-all-start.2 = ((bf16[32,120,128]{2,1,0:T(8,128)(2,1)}), bf16[32,120,128]{2,1,0:T(8,128)(2,1)S(1)}, u32[]{:S(2)}, u32[]{:S(2)}) async-start(bf16[32,120,128]{2,1,0:T(8,128)(2,1)} %broadcast_in_dim.71), calls=%async_computation.2 | async-start | bytes 1966080 | tf_op jit(solution)/shard_map/all_to_all | solution.py:42
  71.4 1.0 copy-start.3
  72.2 1.1 copy-start.6
  73.3 0.7 copy-start.1
  75.6 11.9 %collective-permute-start.7 = (bf16[384,384]{1,0:T(8,128)(2,1)S(1)}, bf16[384,384]{1,0:T(8,128)(2,1)S(1)}, u32[]{:S(2)}, u32[]{:S(2)}) collective-permute-start(bf16[384,384]{1,0:T(8,128)(2,1)S(1)} %windowed.1), channel_id=1, source_target_pairs={{0,2},{2,4},{4,6},{6,0},{1,3},{3,5},{5,7},{7,1},{8,10},{10,12},{12... | collective-permute-start | bytes 884744 | tf_op jit(solution)/shard_map/ppermute | solution.py:56
  79.4 15.3 %collective-permute-start.8 = (bf16[384,384]{1,0:T(8,128)(2,1)S(1)}, bf16[384,384]{1,0:T(8,128)(2,1)S(1)}, u32[]{:S(2)}, u32[]{:S(2)}) collective-permute-start(bf16[384,384]{1,0:T(8,128)(2,1)S(1)} %windowed.1), channel_id=1, source_target_pairs={{0,4},{2,6},{4,0},{6,2},{1,5},{3,7},{5,1},{7,3},{8,12},{10,14},{12... | collective-permute-start | bytes 884744 | tf_op jit(solution)/shard_map/ppermute | solution.py:56
  84.0 12.0 %collective-permute-start.9 = (bf16[384,384]{1,0:T(8,128)(2,1)S(1)}, bf16[384,384]{1,0:T(8,128)(2,1)S(1)}, u32[]{:S(2)}, u32[]{:S(2)}) collective-permute-start(bf16[384,384]{1,0:T(8,128)(2,1)S(1)} %windowed.1), channel_id=1, source_target_pairs={{0,6},{2,0},{4,2},{6,4},{1,7},{3,1},{5,3},{7,5},{8,14},{10,8},{12,... | collective-permute-start | bytes 884744 | tf_op jit(solution)/shard_map/ppermute | solution.py:56
  96.2 16.7 %collective-permute-start.10 = (bf16[16,120,128]{2,1,0:T(8,128)(2,1)S(1)}, bf16[16,120,128]{2,1,0:T(8,128)(2,1)S(1)}, u32[]{:S(2)}, u32[]{:S(2)}) collective-permute-start(bf16[16,120,128]{2,1,0:T(8,128)(2,1)S(1)} %get-tuple-element.48), channel_id=1, source_target_pairs={{0,8},{8,16},{16,24},{24,32},{32,40},{40,48},{48,56},{56,0},{1,9},... | collective-permute-start | bytes 1474568 | tf_op jit(solution)/shard_map/ppermute | solution.py:61
  103.7 14.5 %collective-permute-start.11 = (bf16[16,120,128]{2,1,0:T(8,128)(2,1)S(1)}, bf16[16,120,128]{2,1,0:T(8,128)(2,1)S(1)}, u32[]{:S(2)}, u32[]{:S(2)}) collective-permute-start(bf16[16,120,128]{2,1,0:T(8,128)(2,1)S(1)} %get-tuple-element.47), channel_id=1, source_target_pairs={{0,56},{8,0},{16,8},{24,16},{32,24},{40,32},{48,40},{56,48},{1,57}... | collective-permute-start | bytes 1474568 | tf_op jit(solution)/shard_map/ppermute | solution.py:61
  105.6 27.8 %collective-permute-start.13 = (bf16[32,120,128]{2,1,0:T(8,128)(2,1)S(1)}, bf16[32,120,128]{2,1,0:T(8,128)(2,1)}, u32[]{:S(2)}, u32[]{:S(2)}) collective-permute-start(bf16[32,120,128]{2,1,0:T(8,128)(2,1)S(1)} %all-to-all-done.2.refs_0_), channel_id=1, source_target_pairs={{0,1},{1,0},{2,3},{3,2},{4,5},{5,4},{6,7},{7,6},{8,9},{9,8},{10,11... | collective-permute-start | bytes 2949128 | tf_op jit(solution)/shard_map/ppermute | solution.py:51
  119.2 21.5 %collective-permute-start.12 = (bf16[32,120,128]{2,1,0:T(8,128)(2,1)}, bf16[32,120,128]{2,1,0:T(8,128)(2,1)}, u32[]{:S(2)}, u32[]{:S(2)}) collective-permute-start(bf16[32,120,128]{2,1,0:T(8,128)(2,1)} %joined.1.refs_0_), channel_id=1, source_target_pairs={{0,1},{1,0},{2,3},{3,2},{4,5},{5,4},{6,7},{7,6},{8,9},{9,8},{10,11... | collective-permute-start | bytes 2949128 | tf_op jit(solution)/shard_map/ppermute | solution.py:51
  122.0 59.6 %collective-permute-start.14 = (bf16[4,384,128]{2,1,0:T(8,128)(2,1)}, bf16[4,384,128]{2,1,0:T(8,128)(2,1)}, u32[]{:S(2)}, u32[]{:S(2)}) collective-permute-start(bf16[4,384,128]{2,1,0:T(8,128)(2,1)} %slice.217), channel_id=1, source_target_pairs={{0,1},{1,0},{2,3},{3,2},{4,5},{5,4},{6,7},{7,6},{8,9},{9,8},{10,11... | collective-permute-start | bytes 1179656 | tf_op jit(solution)/shard_map/ppermute | solution.py:51
  155.9 6.7 %copy-start.4 = (f32[384,256]{1,0:T(8,128)S(1)}, f32[384,256]{1,0:T(8,128)}, u32[]{:S(2)}) copy-start(f32[384,256]{1,0:T(8,128)} %fusion.20) | copy-start | bytes 1179652
  155.9 6.7 %copy-start.5 = (bf16[1024,256]{1,0:T(8,128)(2,1)S(1)}, bf16[1024,256]{1,0:T(8,128)(2,1)}, u32[]{:S(2)}) copy-start(bf16[1024,256]{1,0:T(8,128)(2,1)} %param.27) | copy-start | bytes 1572868
  155.9 19.7 %all-to-all-start.3 = ((bf16[4,272,384]{2,1,0:T(8,128)(2,1)}), bf16[4,272,384]{2,1,0:T(8,128)(2,1)S(1)}, u32[]{:S(2)}, u32[]{:S(2)}) async-start(bf16[4,272,384]{2,1,0:T(8,128)(2,1)} %shard_map.138), calls=%async_computation.3 | async-start | bytes 1671168 | tf_op jit(solution)/shard_map/all_to_all | solution.py:42
  178.0 16.6 %all-to-all-start.4 = ((bf16[8,384,128]{2,1,0:T(8,128)(2,1)}), bf16[8,384,128]{2,1,0:T(8,128)(2,1)S(1)}, u32[]{:S(2)}, u32[]{:S(2)}) async-start(bf16[8,384,128]{2,1,0:T(8,128)(2,1)} %broadcast_in_dim.81), calls=%async_computation.4 | async-start | bytes 1572864 | tf_op jit(solution)/shard_map/all_to_all | solution.py:42

commit v7 on v5

--- a/solution.py
+++ b/solution.py
@@ -435,11 +435,7 @@
 
     sent = windowed(where[0], sink_logits, swa_rows, before, query)
     sent = by_x(sent)
-    swa_x = sent[:, :, 2 * LANES :]
-    swa_other = from_core(swa_x)
-    keys_own, sent, up_heads, swa_x, where = lax.optimization_barrier(
-        (keys_own, sent, up_heads, swa_x, where)
-    )
+    keys_own, sent, up_heads, where = lax.optimization_barrier((keys_own, sent, up_heads, where))
     half = keys_own.shape[0] // 2
     low = from_y(keys_own[:half], 1)
     high = from_y(keys_own[half:], -1)
@@ -450,6 +446,8 @@
     state = attend(where[1], (keys_other,), q_all, state, False)
     partial = attend(where[2], (far_own, far_other), q_all, state, True)
     parts = exchange(partial, "x")
+    swa_x = lax.optimization_barrier(sent[:, :, 2 * LANES :])
+    swa_other = from_core(swa_x)
     per_head = out_swa.reshape(x_count, 2, 2 * HEAD, -1)
     from_swa = jnp.zeros((ROWS, out_swa.shape[1]), jnp.float32)
     for values, core in ((swa_x, c_rank), (swa_other, 1 - c_rank)):

time: 194 us -> 197 us (1.015)
  waiting for transfers between devices: 60.5 us -> 63.3 us
    ppermute x2, waiting for transfers between devices: 8.15 us -> 10.6 us  [from_y(): lax.ppermute(value, Y, [(i, (i + step) % count) for i in range(count)])]
  transfers between devices with their start and end apart: 17 -> 17, of which waited for: 9 -> 9; matrix products, arithmetic and copies ran while one was open for 11% -> 12% of each run, Pallas kernels for 9% -> 16%
where the time goes in v7:
time: 197 us; the launch traced here: 195 us
  starting transfers between devices  68.5 us (35%)
  waiting for transfers between devices  63.3 us (32%)
  Pallas kernels  32.1 us (16%)
  matrix products  14.5 us (7%)
  local copies, waits for them, and re-layouts  11.5 us (6%)
  other arithmetic  4.53 us (2%)
    all_to_all x4, waiting for transfers between devices, exchange(): return lax.all_to_all(array, axis, split_axis=0, concat_axis=0, tiled=True)  42.7 us
    pallas_call x3, Pallas kernels, attend(): pl.pallas_call(functools.partial(attend_body, n_parts=len(parts), first=f...  29.4 us
    all_to_all x4, starting transfers between devices, exchange(): return lax.all_to_all(array, axis, split_axis=0, concat_axis=0, tiled=True)  28.1 us
    ppermute x6, starting transfers between devices, from_x(): lax.ppermute(value, 'x', [(i, (i + step) % count) for i in range(count)])  20.4 us
    ppermute x2, waiting for transfers between devices, from_y(): lax.ppermute(value, Y, [(i, (i + step) % count) for i in range(count)])  10.6 us
    dot_general x8, matrix products, layer(): jnp.dot(values[x], weights[x], preferred_element_type=jnp.float32)  10.2 us
    ppermute x6, waiting for transfers between devices, from_x(): lax.ppermute(value, 'x', [(i, (i + step) % count) for i in range(count)])  9.06 us
    ppermute x2, starting transfers between devices, from_y(): lax.ppermute(value, Y, [(i, (i + step) % count) for i in range(count)])  8.52 us
  transfers between devices with their start and end apart: 17, of which 9 were waited for; matrix products, arithmetic and copies ran while one was open for 12% of the time, Pallas kernels for 16%

profile of v7, /device:TPU:320, one launch (start us, length us, event | category | flops | bytes accessed | tf_op | source)
XLA Modules:
  0.0 195.2 jit_solution(6396004473635082672)
XLA Ops:
  0.0 1.1 fusion.11
  1.3 1.1 bitcast_dynamic-update-slice_fusion.9
  2.3 3.4 %collective-permute-start = (bf16[48,2048]{1,0:T(8,128)(2,1)S(1)}, bf16[48,2048]{1,0:T(8,128)(2,1)}, u32[]{:S(2)}, u32[]{:S(2)}) collective-permute-start(bf16[48,2048]{1,0:T(8,128)(2,1)S(1)} %get-tuple-element.50), channel_id=1, source_target_pairs={{0,2},{2,4},{4,6},{6,0},{1,3},{3,5},{5,7},{7,1},{8,10},{10,12},{12... | collective-permute-start | bytes 589832 | tf_op jit(solution)/shard_map/ppermute | solution.py:56
  5.8 4.6 %collective-permute-start.1 = (bf16[48,2048]{1,0:T(8,128)(2,1)S(1)}, bf16[48,2048]{1,0:T(8,128)(2,1)}, u32[]{:S(2)}, u32[]{:S(2)}) collective-permute-start(bf16[48,2048]{1,0:T(8,128)(2,1)S(1)} %get-tuple-element.50), channel_id=1, source_target_pairs={{0,4},{2,6},{4,0},{6,2},{1,5},{3,7},{5,1},{7,3},{8,12},{10,14},{12... | collective-permute-start | bytes 589832 | tf_op jit(solution)/shard_map/ppermute | solution.py:56
  10.4 3.3 %collective-permute-start.2 = (bf16[48,2048]{1,0:T(8,128)(2,1)S(1)}, bf16[48,2048]{1,0:T(8,128)(2,1)S(1)}, u32[]{:S(2)}, u32[]{:S(2)}) collective-permute-start(bf16[48,2048]{1,0:T(8,128)(2,1)S(1)} %get-tuple-element.50), channel_id=1, source_target_pairs={{0,6},{2,0},{4,2},{6,4},{1,7},{3,1},{5,3},{7,5},{8,14},{10,8},{12,... | collective-permute-start | bytes 589832 | tf_op jit(solution)/shard_map/ppermute | solution.py:56
  13.9 1.2 broadcast_in_dim.65
  15.1 12.6 %all-to-all-start = ((bf16[64,80,128]{2,1,0:T(8,128)(2,1)}), bf16[64,80,128]{2,1,0:T(8,128)(2,1)}, u32[]{:S(2)}, u32[]{:S(2)}) async-start(bf16[64,80,128]{2,1,0:T(8,128)(2,1)} %broadcast_in_dim.65), calls=%async_computation | async-start | bytes 2621440 | tf_op jit(solution)/shard_map/all_to_all | solution.py:42
  30.6 1.9 collective-permute-start.3
  32.6 1.0 dynamic-slice_bitcast_fusion.19
  36.6 3.4 %collective-permute-start.4 = (bf16[128,128]{1,0:T(8,128)(2,1)S(1)}, bf16[128,128]{1,0:T(8,128)(2,1)S(1)}, u32[]{:S(2)}, u32[]{:S(2)}) collective-permute-start(bf16[128,128]{1,0:T(8,128)(2,1)S(1)} %slice.203), channel_id=1, source_target_pairs={{0,8},{8,16},{16,24},{24,32},{32,40},{40,48},{48,56},{56,64},{64,7... | collective-permute-start | bytes 98312 | tf_op jit(solution)/shard_map/ppermute | solution.py:392
  40.9 18.8 %all-to-all-done = bf16[64,80,128]{2,1,0:T(8,128)(2,1)} async-done(((bf16[64,80,128]{2,1,0:T(8,128)(2,1)}), bf16[64,80,128]{2,1,0:T(8,128)(2,1)}, u32[]{:S(2)}, u32[]{:S(2)}) %all-to-all-start) | async-done | bytes 1310752 | tf_op jit(solution)/shard_map/all_to_all | solution.py:42
  59.6 1.3 fusion.62
  61.7 1.2 slice_bitcast_fusion.1
  63.6 1.1 broadcast_in_dim.75
  64.7 8.3 %all-to-all-start.1 = ((bf16[32,120,128]{2,1,0:T(8,128)(2,1)}), bf16[32,120,128]{2,1,0:T(8,128)(2,1)S(1)}, u32[]{:S(2)}, u32[]{:S(2)}) async-start(bf16[32,120,128]{2,1,0:T(8,128)(2,1)} %broadcast_in_dim.75), calls=%async_computation.1 | async-start | bytes 1966080 | tf_op jit(solution)/shard_map/all_to_all | solution.py:42
  73.1 1.6 windowed.1
  74.7 2.5 %collective-permute-start.5 = (bf16[384,384]{1,0:T(8,128)(2,1)S(1)}, bf16[384,384]{1,0:T(8,128)(2,1)S(1)}, u32[]{:S(2)}, u32[]{:S(2)}) collective-permute-start(bf16[384,384]{1,0:T(8,128)(2,1)S(1)} %windowed.1), channel_id=1, source_target_pairs={{0,2},{2,4},{4,6},{6,0},{1,3},{3,5},{5,7},{7,1},{8,10},{10,12},{12... | collective-permute-start | bytes 884744 | tf_op jit(solution)/shard_map/ppermute | solution.py:56
  77.2 3.1 %collective-permute-start.6 = (bf16[384,384]{1,0:T(8,128)(2,1)S(1)}, bf16[384,384]{1,0:T(8,128)(2,1)S(1)}, u32[]{:S(2)}, u32[]{:S(2)}) collective-permute-start(bf16[384,384]{1,0:T(8,128)(2,1)S(1)} %windowed.1), channel_id=1, source_target_pairs={{0,4},{2,6},{4,0},{6,2},{1,5},{3,7},{5,1},{7,3},{8,12},{10,14},{12... | collective-permute-start | bytes 884744 | tf_op jit(solution)/shard_map/ppermute | solution.py:56
  80.3 3.4 %collective-permute-start.7 = (bf16[384,384]{1,0:T(8,128)(2,1)S(1)}, bf16[384,384]{1,0:T(8,128)(2,1)S(1)}, u32[]{:S(2)}, u32[]{:S(2)}) collective-permute-start(bf16[384,384]{1,0:T(8,128)(2,1)S(1)} %windowed.1), channel_id=1, source_target_pairs={{0,6},{2,0},{4,2},{6,4},{1,7},{3,1},{5,3},{7,5},{8,14},{10,8},{12,... | collective-permute-start | bytes 884744 | tf_op jit(solution)/shard_map/ppermute | solution.py:56
  83.9 6.7 %collective-permute-done.5 = bf16[384,384]{1,0:T(8,128)(2,1)S(1)} collective-permute-done((bf16[384,384]{1,0:T(8,128)(2,1)S(1)}, bf16[384,384]{1,0:T(8,128)(2,1)S(1)}, u32[]{:S(2)}, u32[]{:S(2)}) %collective-permute-start.5) | collective-permute-done | bytes 294944 | tf_op jit(solution)/shard_map/ppermute | solution.py:56
  90.7 2.4 %collective-permute-done.7 = bf16[384,384]{1,0:T(8,128)(2,1)S(1)} collective-permute-done((bf16[384,384]{1,0:T(8,128)(2,1)S(1)}, bf16[384,384]{1,0:T(8,128)(2,1)S(1)}, u32[]{:S(2)}, u32[]{:S(2)}) %collective-permute-start.7) | collective-permute-done | bytes 294944 | tf_op jit(solution)/shard_map/ppermute | solution.py:56
  93.1 4.3 %all-to-all-done.1.refs_0_ = bf16[32,120,128]{2,1,0:T(8,128)(2,1)S(1)} async-done(((bf16[32,120,128]{2,1,0:T(8,128)(2,1)}), bf16[32,120,128]{2,1,0:T(8,128)(2,1)S(1)}, u32[]{:S(2)}, u32[]{:S(2)}) %all-to-all-start.1) | async-done | bytes 983072 | tf_op jit(solution)/shard_map/all_to_all | solution.py:42
  97.5 6.6 %collective-permute-start.8 = (bf16[16,120,128]{2,1,0:T(8,128)(2,1)S(1)}, bf16[16,120,128]{2,1,0:T(8,128)(2,1)S(1)}, u32[]{:S(2)}, u32[]{:S(2)}) collective-permute-start(bf16[16,120,128]{2,1,0:T(8,128)(2,1)S(1)} %get-tuple-element.56), channel_id=1, source_target_pairs={{0,8},{8,16},{16,24},{24,32},{32,40},{40,48},{48,56},{56,0},{1,9},... | collective-permute-start | bytes 1474568 | tf_op jit(solution)/shard_map/ppermute | solution.py:61
  104.1 1.9 collective-permute-start.9
  106.0 1.9 collective-permute-start.11
  108.0 6.7 %collective-permute-done.8.low_ref = bf16[16,120,128]{2,1,0:T(8,128)(2,1)S(1)} collective-permute-done((bf16[16,120,128]{2,1,0:T(8,128)(2,1)S(1)}, bf16[16,120,128]{2,1,0:T(8,128)(2,1)S(1)}, u32[]{:S(2)}, u32[]{:S(2)}) %collective-permute-start.8) | collective-permute-done | bytes 491552 | tf_op jit(solution)/shard_map/ppermute | solution.py:61
  114.6 3.9 %collective-permute-done.9.high_ref = bf16[16,120,128]{2,1,0:T(8,128)(2,1)S(1)} collective-permute-done((bf16[16,120,128]{2,1,0:T(8,128)(2,1)S(1)}, bf16[16,120,128]{2,1,0:T(8,128)(2,1)S(1)}, u32[]{:S(2)}, u32[]{:S(2)}) %collective-permute-start.9) | collective-permute-done | bytes 491552 | tf_op jit(solution)/shard_map/ppermute | solution.py:61
  118.5 1.0 joined.1.refs_0_
  119.6 1.9 collective-permute-start.10
  122.3 2.4 %collective-permute-start.12 = (bf16[4,384,128]{2,1,0:T(8,128)(2,1)}, bf16[4,384,128]{2,1,0:T(8,128)(2,1)}, u32[]{:S(2)}, u32[]{:S(2)}) collective-permute-start(bf16[4,384,128]{2,1,0:T(8,128)(2,1)} %slice.176), channel_id=1, source_target_pairs={{0,1},{1,0},{2,3},{3,2},{4,5},{5,4},{6,7},{7,6},{8,9},{9,8},{10,11... | collective-permute-start | bytes 1179656 | tf_op jit(solution)/shard_map/ppermute | solution.py:51
  124.7 1.8 fusion.25
  126.5 7.1 %shard_map.136 = (f32[3,256,512]{2,1,0:T(8,128)S(1)}, f32[3,1,512]{2,1,0:T(1,128)S(1)}, f32[3,1,512]{2,1,0:T(1,128)S(1)}, bf16[1536,384]{1,0:T(8,128)(2,1)S(1)}) custom-call(s32[3]{0:T(128)S(1)} %get-tuple-element.36.where_ref, bf16[32,120,128]{2,1,0:T(8,128)(2,1)S(1)} %all-to-all-done.1.refs_0_, ...), custom_call_target="tpu_custom_call" | custom-call | flops 3019898880 | bytes 6000000 | tf_op jit(solution)/shard_map/pallas_call | solution.py:245
  133.7 7.2 %shard_map.137 = (f32[3,256,512]{2,1,0:T(8,128)S(1)}, f32[3,1,512]{2,1,0:T(1,128)S(1)}, f32[3,1,512]{2,1,0:T(1,128)S(1)}) custom-call(s32[3]{0:T(128)S(1)} %get-tuple-element.40.where_ref, bf16[32,120,128]{2,1,0:T(8,128)(2,1)} %collective-permute-done.11.refs_0_, bf16[1536,384]{1,0:T(8,128)(2,1)S(1)} %get-tuple-element.39.refs_1_.refs_2_, ...), custom_call_target="tpu_custom_call" | custom-call | flops 3019898880 | bytes 6000000 | tf_op jit(solution)/shard_map/pallas_call | solution.py:245
  140.9 15.1 %shard_map.138 = bf16[4,272,384]{2,1,0:T(8,128)(2,1)} custom-call(s32[4]{0:T(128)S(1)} %pad_add_fusion.3.where_ref, bf16[32,120,128]{2,1,0:T(8,128)(2,1)} %joined.1.refs_0_, bf16[32,120,128]{2,1,0:T(8,128)(2,1)} %collective-permute-done.10.refs_1_, bf16[1536,384]{1,0:T(8,128)(2,1)S(1)} %get-tuple-element.39.refs_1_.refs_2_, ...), custom_call_target="tpu_custom_call" | custom-call | flops 6039797760 | bytes 6000000 | tf_op jit(solution)/shard_map/pallas_call | solution.py:245
  156.0 3.6 %all-to-all-start.2 = ((bf16[4,272,384]{2,1,0:T(8,128)(2,1)}), bf16[4,272,384]{2,1,0:T(8,128)(2,1)S(1)}, u32[]{:S(2)}, u32[]{:S(2)}) async-start(bf16[4,272,384]{2,1,0:T(8,128)(2,1)} %shard_map.138), calls=%async_computation.2 | async-start | bytes 1671168 | tf_op jit(solution)/shard_map/all_to_all | solution.py:42
  159.7 1.1 convolution_add_fusion.3
  160.8 1.1 convolution_add_fusion.2
  161.9 1.1 convolution_add_fusion.1
  163.0 9.9 %all-to-all-done.2 = bf16[4,272,384]{2,1,0:T(8,128)(2,1)S(1)} async-done(((bf16[4,272,384]{2,1,0:T(8,128)(2,1)}), bf16[4,272,384]{2,1,0:T(8,128)(2,1)S(1)}, u32[]{:S(2)}, u32[]{:S(2)}) %all-to-all-start.2) | async-done | bytes 835616 | tf_op jit(solution)/shard_map/all_to_all | solution.py:42
  173.2 1.1 convolution_convert_fusion.2
  174.3 1.0 broadcast_in_dim.81
  175.4 3.5 %all-to-all-start.3 = ((bf16[8,384,128]{2,1,0:T(8,128)(2,1)}), bf16[8,384,128]{2,1,0:T(8,128)(2,1)S(1)}, u32[]{:S(2)}, u32[]{:S(2)}) async-start(bf16[8,384,128]{2,1,0:T(8,128)(2,1)} %broadcast_in_dim.81), calls=%async_computation.3 | async-start | bytes 1572864 | tf_op jit(solution)/shard_map/all_to_all | solution.py:42
  178.9 1.1 fusion.22
  180.0 1.1 fusion.23
  181.1 1.1 fusion.24
  182.2 9.8 %all-to-all-done.3 = bf16[8,384,128]{2,1,0:T(8,128)(2,1)S(1)} async-done(((bf16[8,384,128]{2,1,0:T(8,128)(2,1)}), bf16[8,384,128]{2,1,0:T(8,128)(2,1)S(1)}, u32[]{:S(2)}, u32[]{:S(2)}) %all-to-all-start.3) | async-done | bytes 786464 | tf_op jit(solution)/shard_map/all_to_all | solution.py:42
  192.0 1.4 convolution_bitcast_fusion
  193.4 1.8 fusion.5
  (84 shorter events, 9.7 us)
Async XLA Ops:
  0.0 34.8 %copy-start = (bf16[2048,192]{0,1:T(8,128)(2,1)S(1)}, bf16[2048,192]{0,1:T(8,128)(2,1)}, u32[]{:S(2)}) copy-start(bf16[2048,192]{0,1:T(8,128)(2,1)} %param.19) | copy-start | bytes 2359300
  0.0 13.7 %copy-start.6 = (bf16[32,256]{1,0:T(8,128)(2,1)S(1)}, bf16[32,256]{1,0:T(8,128)(2,1)}, u32[]{:S(2)}) copy-start(bf16[32,256]{1,0:T(8,128)(2,1)} %param.16) | copy-start | bytes 49156
  0.0 13.8 %copy-start.7 = (bf16[32,64]{1,0:T(8,128)(2,1)S(1)}, bf16[32,64]{1,0:T(8,128)(2,1)}, u32[]{:S(2)}) copy-start(bf16[32,64]{1,0:T(8,128)(2,1)} %param.17) | copy-start | bytes 12292
  2.3 26.3 %collective-permute-start = (bf16[48,2048]{1,0:T(8,128)(2,1)S(1)}, bf16[48,2048]{1,0:T(8,128)(2,1)}, u32[]{:S(2)}, u32[]{:S(2)}) collective-permute-start(bf16[48,2048]{1,0:T(8,128)(2,1)S(1)} %get-tuple-element.50), channel_id=1, source_target_pairs={{0,2},{2,4},{4,6},{6,0},{1,3},{3,5},{5,7},{7,1},{8,10},{10,12},{12... | collective-permute-start | bytes 589832 | tf_op jit(solution)/shard_map/ppermute | solution.py:56
  5.8 23.8 %collective-permute-start.1 = (bf16[48,2048]{1,0:T(8,128)(2,1)S(1)}, bf16[48,2048]{1,0:T(8,128)(2,1)}, u32[]{:S(2)}, u32[]{:S(2)}) collective-permute-start(bf16[48,2048]{1,0:T(8,128)(2,1)S(1)} %get-tuple-element.50), channel_id=1, source_target_pairs={{0,4},{2,6},{4,0},{6,2},{1,5},{3,7},{5,1},{7,3},{8,12},{10,14},{12... | collective-permute-start | bytes 589832 | tf_op jit(solution)/shard_map/ppermute | solution.py:56
  10.4 20.1 %collective-permute-start.2 = (bf16[48,2048]{1,0:T(8,128)(2,1)S(1)}, bf16[48,2048]{1,0:T(8,128)(2,1)S(1)}, u32[]{:S(2)}, u32[]{:S(2)}) collective-permute-start(bf16[48,2048]{1,0:T(8,128)(2,1)S(1)} %get-tuple-element.50), channel_id=1, source_target_pairs={{0,6},{2,0},{4,2},{6,4},{1,7},{3,1},{5,3},{7,5},{8,14},{10,8},{12,... | collective-permute-start | bytes 589832 | tf_op jit(solution)/shard_map/ppermute | solution.py:56
  15.1 12.7 %copy-start.4 = (bf16[2048,64]{0,1:T(8,128)(2,1)S(1)}, bf16[2048,64]{0,1:T(8,128)(2,1)}, u32[]{:S(2)}) copy-start(bf16[2048,64]{0,1:T(8,128)(2,1)} %param.23) | copy-start | bytes 786436
  15.1 13.0 %copy-start.5 = (bf16[2048,64]{0,1:T(8,128)(2,1)S(1)}, bf16[2048,64]{0,1:T(8,128)(2,1)}, u32[]{:S(2)}) copy-start(bf16[2048,64]{0,1:T(8,128)(2,1)} %param.24) | copy-start | bytes 786436
  15.1 44.5 %all-to-all-start = ((bf16[64,80,128]{2,1,0:T(8,128)(2,1)}), bf16[64,80,128]{2,1,0:T(8,128)(2,1)}, u32[]{:S(2)}, u32[]{:S(2)}) async-start(bf16[64,80,128]{2,1,0:T(8,128)(2,1)} %broadcast_in_dim.65), calls=%async_computation | async-start | bytes 2621440 | tf_op jit(solution)/shard_map/all_to_all | solution.py:42
  30.6 4.2 %collective-permute-start.3 = (bf16[4,48,2048]{2,1,0:T(8,128)(2,1)S(1)}, bf16[4,48,2048]{2,1,0:T(8,128)(2,1)S(1)}, u32[]{:S(2)}, u32[]{:S(2)}) collective-permute-start(bf16[4,48,2048]{2,1,0:T(8,128)(2,1)S(1)} %bitcast_dynamic-update-slice_fusion.6), channel_id=1, source_target_pairs={{0,1},{1,0},{2,3},{3,2},{4,5},{5,4},{6,7},{7,6},{8,9},{9,8},{10,11... | collective-permute-start | bytes 2359304 | tf_op jit(solution)/shard_map/ppermute | solution.py:51
  34.8 1.0 copy-start.9
  36.6 27.0 %collective-permute-start.4 = (bf16[128,128]{1,0:T(8,128)(2,1)S(1)}, bf16[128,128]{1,0:T(8,128)(2,1)S(1)}, u32[]{:S(2)}, u32[]{:S(2)}) collective-permute-start(bf16[128,128]{1,0:T(8,128)(2,1)S(1)} %slice.203), channel_id=1, source_target_pairs={{0,8},{8,16},{16,24},{24,32},{32,40},{40,48},{48,56},{56,64},{64,7... | collective-permute-start | bytes 98312 | tf_op jit(solution)/shard_map/ppermute | solution.py:392
  60.9 0.7 copy-start.8
  63.3 9.8 %copy-start.1 = (f32[16]{0:T(128)S(1)}, f32[16]{0:T(128)}, u32[]{:S(2)}) copy-start(f32[16]{0:T(128)} %sink_ref.1) | copy-start | bytes 196
  64.7 32.7 %all-to-all-start.1 = ((bf16[32,120,128]{2,1,0:T(8,128)(2,1)}), bf16[32,120,128]{2,1,0:T(8,128)(2,1)S(1)}, u32[]{:S(2)}, u32[]{:S(2)}) async-start(bf16[32,120,128]{2,1,0:T(8,128)(2,1)} %broadcast_in_dim.75), calls=%async_computation.1 | async-start | bytes 1966080 | tf_op jit(solution)/shard_map/all_to_all | solution.py:42
  74.7 15.9 %collective-permute-start.5 = (bf16[384,384]{1,0:T(8,128)(2,1)S(1)}, bf16[384,384]{1,0:T(8,128)(2,1)S(1)}, u32[]{:S(2)}, u32[]{:S(2)}) collective-permute-start(bf16[384,384]{1,0:T(8,128)(2,1)S(1)} %windowed.1), channel_id=1, source_target_pairs={{0,2},{2,4},{4,6},{6,0},{1,3},{3,5},{5,7},{7,1},{8,10},{10,12},{12... | collective-permute-start | bytes 884744 | tf_op jit(solution)/shard_map/ppermute | solution.py:56
  77.2 13.4 %collective-permute-start.6 = (bf16[384,384]{1,0:T(8,128)(2,1)S(1)}, bf16[384,384]{1,0:T(8,128)(2,1)S(1)}, u32[]{:S(2)}, u32[]{:S(2)}) collective-permute-start(bf16[384,384]{1,0:T(8,128)(2,1)S(1)} %windowed.1), channel_id=1, source_target_pairs={{0,4},{2,6},{4,0},{6,2},{1,5},{3,7},{5,1},{7,3},{8,12},{10,14},{12... | collective-permute-start | bytes 884744 | tf_op jit(solution)/shard_map/ppermute | solution.py:56
  80.3 12.7 %collective-permute-start.7 = (bf16[384,384]{1,0:T(8,128)(2,1)S(1)}, bf16[384,384]{1,0:T(8,128)(2,1)S(1)}, u32[]{:S(2)}, u32[]{:S(2)}) collective-permute-start(bf16[384,384]{1,0:T(8,128)(2,1)S(1)} %windowed.1), channel_id=1, source_target_pairs={{0,6},{2,0},{4,2},{6,4},{1,7},{3,1},{5,3},{7,5},{8,14},{10,8},{12,... | collective-permute-start | bytes 884744 | tf_op jit(solution)/shard_map/ppermute | solution.py:56
  97.5 17.1 %collective-permute-start.8 = (bf16[16,120,128]{2,1,0:T(8,128)(2,1)S(1)}, bf16[16,120,128]{2,1,0:T(8,128)(2,1)S(1)}, u32[]{:S(2)}, u32[]{:S(2)}) collective-permute-start(bf16[16,120,128]{2,1,0:T(8,128)(2,1)S(1)} %get-tuple-element.56), channel_id=1, source_target_pairs={{0,8},{8,16},{16,24},{24,32},{32,40},{40,48},{48,56},{56,0},{1,9},... | collective-permute-start | bytes 1474568 | tf_op jit(solution)/shard_map/ppermute | solution.py:61
  104.1 14.4 %collective-permute-start.9 = (bf16[16,120,128]{2,1,0:T(8,128)(2,1)S(1)}, bf16[16,120,128]{2,1,0:T(8,128)(2,1)S(1)}, u32[]{:S(2)}, u32[]{:S(2)}) collective-permute-start(bf16[16,120,128]{2,1,0:T(8,128)(2,1)S(1)} %get-tuple-element.55), channel_id=1, source_target_pairs={{0,56},{8,0},{16,8},{24,16},{32,24},{40,32},{48,40},{56,48},{1,57}... | collective-permute-start | bytes 1474568 | tf_op jit(solution)/shard_map/ppermute | solution.py:61
  106.0 27.6 %collective-permute-start.11 = (bf16[32,120,128]{2,1,0:T(8,128)(2,1)S(1)}, bf16[32,120,128]{2,1,0:T(8,128)(2,1)}, u32[]{:S(2)}, u32[]{:S(2)}) collective-permute-start(bf16[32,120,128]{2,1,0:T(8,128)(2,1)S(1)} %all-to-all-done.1.refs_0_), channel_id=1, source_target_pairs={{0,1},{1,0},{2,3},{3,2},{4,5},{5,4},{6,7},{7,6},{8,9},{9,8},{10,11... | collective-permute-start | bytes 2949128 | tf_op jit(solution)/shard_map/ppermute | solution.py:51
  119.6 21.4 %collective-permute-start.10 = (bf16[32,120,128]{2,1,0:T(8,128)(2,1)}, bf16[32,120,128]{2,1,0:T(8,128)(2,1)}, u32[]{:S(2)}, u32[]{:S(2)}) collective-permute-start(bf16[32,120,128]{2,1,0:T(8,128)(2,1)} %joined.1.refs_0_), channel_id=1, source_target_pairs={{0,1},{1,0},{2,3},{3,2},{4,5},{5,4},{6,7},{7,6},{8,9},{9,8},{10,11... | collective-permute-start | bytes 2949128 | tf_op jit(solution)/shard_map/ppermute | solution.py:51
  122.3 56.6 %collective-permute-start.12 = (bf16[4,384,128]{2,1,0:T(8,128)(2,1)}, bf16[4,384,128]{2,1,0:T(8,128)(2,1)}, u32[]{:S(2)}, u32[]{:S(2)}) collective-permute-start(bf16[4,384,128]{2,1,0:T(8,128)(2,1)} %slice.176), channel_id=1, source_target_pairs={{0,1},{1,0},{2,3},{3,2},{4,5},{5,4},{6,7},{7,6},{8,9},{9,8},{10,11... | collective-permute-start | bytes 1179656 | tf_op jit(solution)/shard_map/ppermute | solution.py:51
  156.0 3.6 %copy-start.2 = (f32[384,256]{1,0:T(8,128)S(1)}, f32[384,256]{1,0:T(8,128)}, u32[]{:S(2)}) copy-start(f32[384,256]{1,0:T(8,128)} %fusion.25) | copy-start | bytes 1179652
  156.0 3.7 %copy-start.3 = (bf16[1024,256]{1,0:T(8,128)(2,1)S(1)}, bf16[1024,256]{1,0:T(8,128)(2,1)}, u32[]{:S(2)}) copy-start(bf16[1024,256]{1,0:T(8,128)(2,1)} %param.27) | copy-start | bytes 1572868
  156.0 16.9 %all-to-all-start.2 = ((bf16[4,272,384]{2,1,0:T(8,128)(2,1)}), bf16[4,272,384]{2,1,0:T(8,128)(2,1)S(1)}, u32[]{:S(2)}, u32[]{:S(2)}) async-start(bf16[4,272,384]{2,1,0:T(8,128)(2,1)} %shard_map.138), calls=%async_computation.2 | async-start | bytes 1671168 | tf_op jit(solution)/shard_map/all_to_all | solution.py:42
  175.4 16.6 %all-to-all-start.3 = ((bf16[8,384,128]{2,1,0:T(8,128)(2,1)}), bf16[8,384,128]{2,1,0:T(8,128)(2,1)S(1)}, u32[]{:S(2)}, u32[]{:S(2)}) async-start(bf16[8,384,128]{2,1,0:T(8,128)(2,1)} %broadcast_in_dim.81), calls=%async_computation.3 | async-start | bytes 1572864 | tf_op jit(solution)/shard_map/all_to_all | solution.py:42
